TPU v7x, 256 devices: a 4x2x16 block of a 4x16x16 slice. The times are simulated.
256 devices in a mesh: grp: 2 (over y), sp: 32 (over z, core), tp: 4 (over x).
Axes of the slice: x: 4, y: 2, z: 16, core: 2. Of those that a mesh axis runs over, the one named last changes fastest.
The devices are a block of a 4x16x16 slice.
Arguments:
- resid: bfloat16 [12288, 2048], P(('grp', 'sp', 'tp')), parts along dimension 0, may hold values from -6 to 6
- queries: bfloat16 [12288, 1024], P(('grp', 'sp'), 'tp'), parts along dimension 0, may hold values from -64 to 64
- keys: bfloat16 [12288, 256], P(('grp', 'sp'), 'tp'), parts along dimension 0, may hold values from -64 to 64
- values: bfloat16 [12288, 256], P(('grp', 'sp'), 'tp'), parts along dimension 0, may hold values from -6 to 6
- doc_ids: int32 [12288], P(('grp', 'sp')), parts along dimension 0, may hold values from 0 to 15, never falling along the last dimension, each value on 1 to 768 neighbouring positions
- sink_logits: float32 [16], P('tp'), may hold values from 2 to 6
- out_proj: bfloat16 [1024, 2048], P('tp'), may hold values from -1.5 to 1.5
- norm1_gain: float32 [2048], replicated, may hold values from 0.1 to 1.9
- norm1_bias: float32 [2048], replicated, may hold values from -1.8 to 1.8
- route_ids: int32 [12288, 2], P(('grp', 'sp', 'tp')), parts along dimension 0, may hold values from 0 to 31, all different within a row; in each aligned block of 48 rows (0 to 47, 48 to 95, ...) at most 3 rows name the same one
- route_weights: float32 [12288, 2], P(('grp', 'sp', 'tp')), parts along dimension 0, may hold values from 0.25 to 1
- expert_gate: bfloat16 [32, 2048, 3072], P('sp', None, 'tp'), may hold values from -0.125 to 0.125
- expert_up: bfloat16 [32, 2048, 3072], P('sp', None, 'tp'), may hold values from -0.125 to 0.125
- expert_down: bfloat16 [32, 3072, 2048], P('sp', 'tp'), may hold values from -0.109375 to 0.109375
- norm2_gain: float32 [2048], replicated, may hold values from 0.1 to 1.9
- norm2_bias: float32 [2048], replicated, may hold values from -1.8 to 1.8
Outputs:
- mixed: bfloat16 [12288, 2048], P(('grp', 'sp', 'tp')), parts along dimension 0
There are 2 independent parts, one for each index of `grp`. A program takes and returns all parts, laid end to end along the dimension named above; an argument that names none is the same for every part. Nothing has to cross between parts.
Inputs may be any that keep to these rules, and one draw needn't show every extreme that they name: `route_ids`: among the rows of one device (aligned blocks of 48 tokens) no expert is named more than 3 times, a bound that some block reaches; a token's 2 experts differ.
All inputs are finite; a program needn't handle non-finite values.
Results may differ from a plain program's by a relative error of at most 0.012.
Values may be sent and summed in bfloat16 or wider, within the bound.
No kernel may reach another device: no remote copies, remote signals or barrier semaphores. Data moves between devices by JAX's collectives and lax.ppermute only.
A program may use at most 64 MiB of HBM per device.

v0:
```python
import functools

import jax
import jax.numpy as jnp
from jax import lax
from jax.experimental import pallas as pl
from jax.experimental.pallas import tpu as pltpu
from jax.sharding import PartitionSpec as P


HEAD_DIM = 64
WINDOW = 128
LANES = 128
NORM_EPSILON = 1e-05
RESIDUAL_SCALE = 1.4142135623730951
MASKED = -1e30
F32 = jnp.float32
BF16 = jnp.bfloat16


VMEM = pl.BlockSpec(memory_space=pltpu.VMEM)
HBM = pl.BlockSpec(memory_space=pltpu.HBM)


def mm(a, b):
    return jnp.dot(a, b, preferred_element_type=F32)


def mm_nt(a, b):
    return lax.dot_general(a, b, (((1,), (1,)), ((), ())), preferred_element_type=F32)


def call(body, out_shapes, *args, flops, specs=None, scratch=(), vmem=None):
    size = sum(a.size * a.dtype.itemsize for a in args)
    size += sum(s.size * s.dtype.itemsize for s in out_shapes)
    return pl.pallas_call(
        body,
        out_shape=out_shapes,
        in_specs=specs or [VMEM] * len(args),
        out_specs=[VMEM] * len(out_shapes),
        scratch_shapes=list(scratch),
        compiler_params=pltpu.CompilerParams(vmem_limit_bytes=vmem or 12 * 2**20),
        cost_estimate=pl.CostEstimate(flops=flops, bytes_accessed=size, transcendentals=0),
    )(*args)


def shape(dims, dtype):
    return jax.ShapeDtypeStruct(dims, dtype)


def layer_norm(values, gain, bias):
    centred = values - jnp.mean(values, -1, keepdims=True)
    variance = jnp.mean(centred * centred, -1, keepdims=True)
    return centred * lax.rsqrt(variance + NORM_EPSILON) * gain + bias


def first_body(count, *refs):
    sources, held, (head_ref, tail_ref, sems) = refs[:count], refs[count : 2 * count], refs[2 * count :]
    copies = [pltpu.make_async_copy(a, b, sems.at[i]) for i, (a, b) in enumerate(zip(sources, held))]
    for copy in copies:
        copy.start()
    for copy in copies[:3]:
        copy.wait()
    keys_ref, values_ref, docs_ref = held[:3]
    tokens = keys_ref.shape[1]
    docs = (docs_ref[...].astype(F32) + 1.0).astype(BF16)
    for ref, lo in ((head_ref, 0), (tail_ref, tokens - WINDOW)):
        cols = slice(lo, lo + WINDOW)
        ref[0:HEAD_DIM, :] = keys_ref[:, cols]
        ref[HEAD_DIM : 2 * HEAD_DIM, :] = values_ref[:, cols]
        ref[2 * HEAD_DIM :, :] = jnp.broadcast_to(docs[:, cols], (16, WINDOW))
    for copy in copies[3:]:
        copy.wait()


def attention_body(
    sink_ref, query_ref, keys_ref, values_ref, docs_ref, prev_ref, next_ref, proj_ref, out_ref, att_ref
):
    tokens = query_ref.shape[0]
    heads = query_ref.shape[1] // HEAD_DIM
    own_docs = docs_ref[...].astype(F32) + 1.0
    query_docs = jnp.broadcast_to(own_docs, (LANES, tokens)).T[:, 0:1]
    row = lax.broadcasted_iota(jnp.int32, (tokens, 1), 0)
    blocks = []
    for key, value, docs, first in (
        (prev_ref[0:HEAD_DIM, :], prev_ref[HEAD_DIM : 2 * HEAD_DIM, :], None, -WINDOW),
        (keys_ref[...], values_ref[...], own_docs, 0),
        (next_ref[0:HEAD_DIM, :], next_ref[HEAD_DIM : 2 * HEAD_DIM, :], None, tokens),
    ):
        if docs is None:
            ref = prev_ref if first < 0 else next_ref
            docs = ref[2 * HEAD_DIM :, :].astype(F32)[0:1, :]
        width = key.shape[1]
        place = first + lax.broadcasted_iota(jnp.int32, (1, width), 1)
        allowed = (jnp.abs(row - place) <= WINDOW) & (query_docs == docs)
        blocks.append((key, value, allowed))
    for h in range(heads):
        cols = slice(h * HEAD_DIM, (h + 1) * HEAD_DIM)
        query = query_ref[:, cols]
        sink = sink_ref[:, h : h + 1]
        scores = [
            jnp.where(allowed, mm(query, key) * HEAD_DIM ** (-0.5), MASKED)
            for key, _, allowed in blocks
        ]
        top = functools.reduce(jnp.maximum, [jnp.max(s, -1, keepdims=True) for s in scores])
        top = jnp.maximum(top, sink)
        raised = [
            jnp.where(allowed, jnp.exp(s - top), 0.0) for s, (_, _, allowed) in zip(scores, blocks)
        ]
        total = jnp.exp(sink - top) + sum(jnp.sum(r, -1, keepdims=True) for r in raised)
        scale = 1.0 / total
        result = sum(
            mm_nt((r * scale).astype(BF16), value) for r, (_, value, _) in zip(raised, blocks)
        )
        att_ref[:, cols] = result.astype(BF16)
    out_ref[...] = mm(att_ref[...], proj_ref[...]).astype(BF16)


def routing_rows(ids, experts, tokens):
    expert = lax.broadcasted_iota(jnp.int32, (experts, tokens), 0)
    named = jnp.zeros((experts, tokens), F32)
    for k in range(ids.shape[0]):
        named += (ids[k : k + 1, :] == expert).astype(F32)
    before = lax.broadcasted_iota(jnp.int32, (tokens, tokens), 0) < lax.broadcasted_iota(
        jnp.int32, (tokens, tokens), 1
    )
    rank = mm(named.astype(BF16), before.astype(BF16))
    return named, rank


def dispatch_body(
    experts, parts_ref, resid_ref, gain_ref, bias_ref, ids_ref, normed_ref, sent_ref, wide_ref
):
    tokens, width = resid_ref.shape
    tiles = width // LANES
    capacity = ids_ref.shape[0] * tokens // experts
    projected = sum(parts_ref[i].astype(F32) for i in range(parts_ref.shape[0]))
    pre_norm = RESIDUAL_SCALE * resid_ref[...].astype(F32) + projected.astype(BF16).astype(F32)
    normed = layer_norm(pre_norm, gain_ref[...], bias_ref[...]).astype(BF16)
    normed_ref[...] = normed
    named, rank = routing_rows(ids_ref[...], experts, tokens)
    for j in range(capacity):
        pick = jnp.where((named > 0.5) & (jnp.abs(rank - j) < 0.5), 1.0, 0.0).astype(BF16)
        rows = mm(pick, normed)
        for c in range(tiles):
            wide_ref[pl.ds(j * tiles + c, experts, stride=capacity * tiles), :] = rows[
                :, c * LANES : (c + 1) * LANES
            ]
    sent_ref[...] = wide_ref[...].astype(BF16)


def expert_body(count, *refs):
    row_refs, (gate_ref, up_ref, down_ref), refs = refs[:count], refs[count : count + 3], refs[count + 3 :]
    out_refs, (lhs, wide) = refs[:count], refs[count:]
    tiles = gate_ref.shape[0] // LANES
    rows = row_refs[0].shape[0] // tiles
    for b, ref in enumerate(row_refs):
        wide[b] = ref[...].astype(F32)
        for c in range(tiles):
            lhs[b * rows : (b + 1) * rows, c * LANES : (c + 1) * LANES] = wide.at[b][
                pl.ds(c, rows, stride=tiles), :
            ].astype(BF16)
    gate_act = mm(lhs[...], gate_ref[...])
    up_act = mm(lhs[...], up_ref[...])
    act = (gate_act / (1.0 + jnp.exp(-gate_act)) * up_act).astype(BF16)
    step = 4 * LANES
    for i in range(0, down_ref.shape[1], step):
        result = mm(act, down_ref[:, i : i + step])
        for t in range(0, step, LANES):
            for b in range(count):
                wide.at[b][pl.ds((i + t) // LANES, rows, stride=tiles), :] = result[
                    b * rows : (b + 1) * rows, t : t + LANES
                ]
    for b in range(count):
        out_refs[b][...] = wide[b].astype(BF16)


def total_body(kept_ref, left_1_ref, right_1_ref, left_2_ref, right_2_ref, out_ref):
    half = left_1_ref.shape[0]
    for part, left_ref, right_ref in ((0, left_1_ref, right_1_ref), (1, left_2_ref, right_2_ref)):
        rows = slice(part * half, (part + 1) * half)
        sides = left_ref[...].astype(F32) + right_ref[...].astype(F32)
        out_ref[rows, :] = (kept_ref[rows, :].astype(F32) + sides).astype(BF16)


def combine_body(
    experts, back_ref, normed_ref, ids_ref, weights_ref, gain_ref, bias_ref, out_ref, wide_ref, rows_ref
):
    tokens, width = normed_ref.shape
    tiles = width // LANES
    top = ids_ref.shape[1]
    capacity = top * tokens // experts
    wide_ref[...] = back_ref[...].astype(F32)
    expert = lax.broadcasted_iota(jnp.int32, (tokens, experts), 1)
    named = jnp.zeros((tokens, experts), F32)
    weighted = jnp.zeros((tokens, experts), F32)
    for k in range(top):
        hit = ids_ref[:, k : k + 1] == expert
        named += hit.astype(F32)
        weighted += jnp.where(hit, weights_ref[:, k : k + 1], 0.0)
    earlier = lax.broadcasted_iota(jnp.int32, (tokens, tokens), 1) < lax.broadcasted_iota(
        jnp.int32, (tokens, tokens), 0
    )
    rank = mm(earlier.astype(BF16), named.astype(BF16))
    moe_sum = 0.0
    for j in range(capacity):
        pick = jnp.where((named > 0.5) & (jnp.abs(rank - j) < 0.5), weighted, 0.0)
        for c in range(tiles):
            rows_ref[:, c * LANES : (c + 1) * LANES] = wide_ref[
                pl.ds(j * tiles + c, experts, stride=capacity * tiles), :
            ].astype(BF16)
        high = pick.astype(BF16)
        low = pick - high.astype(F32)
        middle = low.astype(BF16)
        last = (low - middle.astype(F32)).astype(BF16)
        rows = rows_ref[...]
        moe_sum = moe_sum + (mm(high, rows) + (mm(middle, rows) + mm(last, rows)))
    pre_final = RESIDUAL_SCALE * normed_ref[...].astype(F32) + moe_sum
    out_ref[...] = layer_norm(pre_final, gain_ref[...], bias_ref[...]).astype(BF16)


def per_device(
    resid,
    queries,
    keys,
    values,
    doc_ids,
    sink_logits,
    out_proj,
    norm1_gain,
    norm1_bias,
    route_ids,
    route_weights,
    expert_gate,
    expert_up,
    expert_down,
    norm2_gain,
    norm2_bias,
):
    tokens = queries.shape[0]
    own, width = resid.shape
    blocks, members = lax.axis_size("sp"), lax.axis_size("tp")
    experts = blocks
    capacity = route_ids.shape[1] * own // experts
    tiles = width // LANES
    packed = experts * capacity * tiles

    small = (keys.T, values.T, doc_ids.reshape(1, tokens), queries, out_proj, resid, sink_logits.reshape(1, -1))
    pack = shape((2 * HEAD_DIM + 16, WINDOW), BF16)
    keys_t, values_t, docs, queries, out_proj, resid, sinks, head, tail = call(
        functools.partial(first_body, len(small)),
        [shape(a.shape, a.dtype) for a in small] + [pack, pack],
        *[pltpu.with_memory_space_constraint(a, pltpu.HBM) for a in small],
        flops=10**5,
        specs=[HBM] * len(small),
        scratch=[pltpu.SemaphoreType.DMA((len(small),))],
    )
    previous = lax.ppermute(tail, "sp", [(i, i + 1) for i in range(blocks - 1)])
    following = lax.ppermute(head, "sp", [(i + 1, i) for i in range(blocks - 1)])
    (partial,) = call(
        attention_body,
        [shape((tokens, width), BF16)],
        sinks,
        queries,
        keys_t,
        values_t,
        docs,
        previous,
        following,
        out_proj,
        flops=10**9,
        scratch=[pltpu.VMEM(queries.shape, BF16)],
    )
    parts = lax.all_to_all(partial.reshape(members, own, width), "tp", 0, 0, tiled=True)
    normed, sent = call(
        functools.partial(dispatch_body, experts),
        [shape((own, width), BF16), shape((packed, LANES), BF16)],
        parts,
        resid,
        norm1_gain.reshape(1, -1),
        norm1_bias.reshape(1, -1),
        route_ids.T,
        flops=10**9,
        scratch=[pltpu.VMEM((packed, LANES), F32)],
    )
    arrived = lax.all_to_all(sent, "sp", 0, 0, tiled=True)

    def turned(array, by):
        return lax.ppermute(array, "tp", [(i, (i + by) % members) for i in range(members)])

    def expert_call(*row_sets):
        count, rows = len(row_sets), row_sets[0].shape[0]
        return call(
            functools.partial(expert_body, count),
            [shape((rows, LANES), BF16)] * count,
            *row_sets,
            expert_gate[0],
            expert_up[0],
            expert_down[0],
            flops=count * rows * 10**6,
            scratch=[
                pltpu.VMEM((count * rows // tiles, width), BF16),
                pltpu.VMEM((count, rows, LANES), F32),
            ],
        )

    half = packed // 2
    first, second = arrived[:half], arrived[half:]
    left_1, right_2 = turned(first, 1), turned(second, -1)
    left_2, right_1 = turned(second, 1), turned(first, -1)
    far_1, far_2 = turned(left_1, 1), turned(right_2, -1)
    (kept,) = expert_call(arrived)
    for_left_1, for_left_2, for_right_1, for_right_2 = expert_call(left_1, left_2, right_1, right_2)
    for_far_1, for_far_2 = expert_call(far_1, far_2)
    from_right_2 = turned(for_left_2, -1)
    from_left_1 = turned(for_right_1, 1)
    for_left_1 = for_left_1.astype(F32) + turned(for_far_1, -1).astype(F32)
    for_right_2 = for_right_2.astype(F32) + turned(for_far_2, 1).astype(F32)
    from_right_1 = turned(for_left_1.astype(BF16), -1)
    from_left_2 = turned(for_right_2.astype(BF16), 1)
    (summed,) = call(
        total_body,
        [shape((packed, LANES), BF16)],
        kept,
        from_left_1,
        from_right_1,
        from_left_2,
        from_right_2,
        flops=10**7,
    )
    back = lax.all_to_all(summed, "sp", 0, 0, tiled=True)
    (mixed,) = call(
        functools.partial(combine_body, experts),
        [shape((own, width), BF16)],
        back,
        normed,
        route_ids,
        route_weights,
        norm2_gain.reshape(1, -1),
        norm2_bias.reshape(1, -1),
        flops=10**9,
        scratch=[pltpu.VMEM((packed, LANES), F32), pltpu.VMEM((experts, width), BF16)],
    )
    return mixed


def solution(mesh):
    every = ("grp", "sp", "tp")
    group = ("grp", "sp")
    placed = (
        P(every, None),
        P(group, "tp"),
        P(group, "tp"),
        P(group, "tp"),
        P(group),
        P("tp"),
        P("tp", None),
        P(),
        P(),
        P(every, None),
        P(every, None),
        P("sp", None, "tp"),
        P("sp", None, "tp"),
        P("sp", "tp", None),
        P(),
        P(),
    )

    return jax.shard_map(
        per_device, mesh=mesh, in_specs=placed, out_specs=P(every, None), check_vma=False
    )
```

profile of v0, /device:TPU:40, one launch (start us, length us, event | category | flops | bytes accessed | tf_op | source)
XLA Modules:
  0.0 161.7 jit_solution(8285459583583430923)
XLA Ops:
  0.0 1.4 shard_map.154
  1.5 1.8 %collective-permute-start = (bf16[144,128]{1,0:T(8,128)(2,1)S(1)}, bf16[144,128]{1,0:T(8,128)(2,1)S(1)}, u32[]{:S(2)}, u32[]{:S(2)}) collective-permute-start(bf16[144,128]{1,0:T(8,128)(2,1)S(1)} %get-tuple-element.27), channel_id=1, source_target_pairs={{0,4},{4,8},{8,12},{12,16},{16,20},{20,24},{24,28},{28,32},{32,36}... | collective-permute-start | bytes 110600 | tf_op jit(solution)/shard_map/ppermute | solution.py:258
  3.3 1.3 collective-permute-start.1
  4.6 4.3 %collective-permute-done.1.next_ref = bf16[144,128]{1,0:T(8,128)(2,1)S(1)} collective-permute-done((bf16[144,128]{1,0:T(8,128)(2,1)S(1)}, bf16[144,128]{1,0:T(8,128)(2,1)S(1)}, u32[]{:S(2)}, u32[]{:S(2)}) %collective-permute-start.1) | collective-permute-done | bytes 36896 | tf_op jit(solution)/shard_map/ppermute | solution.py:259
  8.9 2.9 %shard_map.155 = bf16[192,2048]{1,0:T(8,128)(2,1)S(1)} custom-call(f32[1,4]{1,0:T(1,128)S(1)} %get-tuple-element.22.sink_ref, bf16[192,256]{1,0:T(8,128)(2,1)S(1)} %get-tuple-element.23.query_ref, bf16[64,192]{1,0:T(8,128)(2,1)S(1)} %get-tuple-element.24.keys_ref, bf16[64,192]{1,0:T(8,128)(2,1)S(1)} %get-tuple-element.25.values_ref, ...), custom_call_target="tpu_custom_call" | custom-call | flops 1000000000 | bytes 2056976 | tf_op jit(solution)/shard_map/pallas_call | solution.py:36
  11.8 16.9 %all_to_all.27.parts_ref = bf16[4,48,2048]{2,1,0:T(8,128)(2,1)S(1)} all-to-all(bf16[4,48,2048]{2,1,0:T(8,128)(2,1)S(1)} %bitcast.29), channel_id=1, replica_groups=mesh['grp'=2,'sp'=32,'tp'=4] {'tp'}, dimensions={0} | all-to-all | bytes 1572864 | tf_op jit(solution)/shard_map/all_to_all | solution.py:274
  28.8 0.8 shard_map.156
  29.5 52.8 %all_to_all.28 = bf16[32,48,128]{2,1,0:T(8,128)(2,1)S(1)} all-to-all(bf16[32,48,128]{2,1,0:T(8,128)(2,1)S(1)} %bitcast.31), channel_id=1, replica_groups=mesh['grp'=2,'sp'=32,'tp'=4] {'sp'}, dimensions={0} | all-to-all | bytes 786432 | tf_op jit(solution)/shard_map/all_to_all | solution.py:286
  82.3 0.7 collective-permute-start.2
  83.0 2.7 %collective-permute-start.5 = (bf16[768,128]{1,0:T(8,128)(2,1)S(1)}, bf16[768,128]{1,0:T(8,128)(2,1)S(1)}, u32[]{:S(2)}, u32[]{:S(2)}) collective-permute-start(bf16[768,128]{1,0:T(8,128)(2,1)S(1)} %bitcast.39), channel_id=1, source_target_pairs={{0,3},{1,0},{2,1},{3,2},{4,7},{5,4},{6,5},{7,6},{8,11},{9,8},{10,9... | collective-permute-start | bytes 589832 | tf_op jit(solution)/shard_map/ppermute | solution.py:289
  85.7 4.6 %collective-permute-done.2.refs_0_ = bf16[768,128]{1,0:T(8,128)(2,1)S(1)} collective-permute-done((bf16[768,128]{1,0:T(8,128)(2,1)S(1)}, bf16[768,128]{1,0:T(8,128)(2,1)S(1)}, u32[]{:S(2)}, u32[]{:S(2)}) %collective-permute-start.2) | collective-permute-done | bytes 196640 | tf_op jit(solution)/shard_map/ppermute | solution.py:289
  90.3 3.2 %collective-permute-start.8 = (bf16[768,128]{1,0:T(8,128)(2,1)S(1)}, bf16[768,128]{1,0:T(8,128)(2,1)S(1)}, u32[]{:S(2)}, u32[]{:S(2)}) collective-permute-start(bf16[768,128]{1,0:T(8,128)(2,1)S(1)} %collective-permute-done.5.refs_3_), channel_id=1, source_target_pairs={{0,3},{1,0},{2,1},{3,2},{4,7},{5,4},{6,5},{7,6},{8,11},{9,8},{10,9... | collective-permute-start | bytes 589832 | tf_op jit(solution)/shard_map/ppermute | solution.py:289
  93.5 3.2 %collective-permute-start.4 = (bf16[768,128]{1,0:T(8,128)(2,1)S(1)}, bf16[768,128]{1,0:T(8,128)(2,1)S(1)}, u32[]{:S(2)}, u32[]{:S(2)}) collective-permute-start(bf16[768,128]{1,0:T(8,128)(2,1)S(1)} %bitcast.38), channel_id=1, source_target_pairs={{0,3},{1,0},{2,1},{3,2},{4,7},{5,4},{6,5},{7,6},{8,11},{9,8},{10,9... | collective-permute-start | bytes 589832 | tf_op jit(solution)/shard_map/ppermute | solution.py:289
  96.8 2.0 %collective-permute-done.7.refs_0_ = bf16[768,128]{1,0:T(8,128)(2,1)S(1)} collective-permute-done((bf16[768,128]{1,0:T(8,128)(2,1)S(1)}, bf16[768,128]{1,0:T(8,128)(2,1)S(1)}, u32[]{:S(2)}, u32[]{:S(2)}) %collective-permute-start.7) | collective-permute-done | bytes 196640 | tf_op jit(solution)/shard_map/ppermute | solution.py:289
  98.8 2.0 %shard_map.159 = (bf16[768,128]{1,0:T(8,128)(2,1)S(1)}, bf16[768,128]{1,0:T(8,128)(2,1)S(1)}) custom-call(bf16[768,128]{1,0:T(8,128)(2,1)S(1)} %collective-permute-done.7.refs_0_, bf16[768,128]{1,0:T(8,128)(2,1)S(1)} %collective-permute-done.8.refs_1_, bf16[2048,768]{1,0:T(8,128)(2,1)S(1)} %bitcast.19, bf16[2048,768]{1,0:T(8,128)(2,1)S(1)} %bitcast.22, ...), custom_call_target="tpu_custom_call" | custom-call | flops 1536000000 | bytes 10223616 | tf_op jit(solution)/shard_map/pallas_call | solution.py:36
  100.8 3.6 %collective-permute-start.9 = (bf16[768,128]{1,0:T(8,128)(2,1)S(1)}, bf16[768,128]{1,0:T(8,128)(2,1)S(1)}, u32[]{:S(2)}, u32[]{:S(2)}) collective-permute-start(bf16[768,128]{1,0:T(8,128)(2,1)S(1)} %get-tuple-element.34), channel_id=1, source_target_pairs={{0,3},{1,0},{2,1},{3,2},{4,7},{5,4},{6,5},{7,6},{8,11},{9,8},{10,9... | collective-permute-start | bytes 589832 | tf_op jit(solution)/shard_map/ppermute | solution.py:289
  104.4 2.9 %shard_map.158 = (bf16[768,128]{1,0:T(8,128)(2,1)S(1)}, bf16[768,128]{1,0:T(8,128)(2,1)S(1)}, bf16[768,128]{1,0:T(8,128)(2,1)S(1)}, bf16[768,128]{1,0:T(8,128)(2,1)S(1)}) custom-call(bf16[768,128]{1,0:T(8,128)(2,1)S(1)} %collective-permute-done.2.refs_0_, bf16[768,128]{1,0:T(8,128)(2,1)S(1)} %collective-permute-done.3.refs_1_, ...), custom_call_target="tpu_custom_call" | custom-call | flops 3072000000 | bytes 11010048 | tf_op jit(solution)/shard_map/pallas_call | solution.py:36
  107.3 0.1 collective-permute-start.6
  107.4 3.2 %collective-permute-start.13 = (bf16[768,128]{1,0:T(8,128)(2,1)S(1)}, bf16[768,128]{1,0:T(8,128)(2,1)S(1)}, u32[]{:S(2)}, u32[]{:S(2)}) collective-permute-start(bf16[768,128]{1,0:T(8,128)(2,1)S(1)} %get-tuple-element.37), channel_id=1, source_target_pairs={{0,3},{1,0},{2,1},{3,2},{4,7},{5,4},{6,5},{7,6},{8,11},{9,8},{10,9... | collective-permute-start | bytes 589832 | tf_op jit(solution)/shard_map/ppermute | solution.py:289
  110.6 0.1 add_convert_fusion.1
  110.7 3.3 %collective-permute-start.10 = (bf16[768,128]{1,0:T(8,128)(2,1)S(1)}, bf16[768,128]{1,0:T(8,128)(2,1)S(1)}, u32[]{:S(2)}, u32[]{:S(2)}) collective-permute-start(bf16[768,128]{1,0:T(8,128)(2,1)S(1)} %add_convert_fusion.1), channel_id=1, source_target_pairs={{0,3},{1,0},{2,1},{3,2},{4,7},{5,4},{6,5},{7,6},{8,11},{9,8},{10,9... | collective-permute-start | bytes 589832 | tf_op jit(solution)/shard_map/ppermute | solution.py:289
  114.0 5.4 %collective-permute-done.11 = bf16[768,128]{1,0:T(8,128)(2,1)S(1)} collective-permute-done((bf16[768,128]{1,0:T(8,128)(2,1)S(1)}, bf16[768,128]{1,0:T(8,128)(2,1)S(1)}, u32[]{:S(2)}, u32[]{:S(2)}) %collective-permute-start.11) | collective-permute-done | bytes 196640 | tf_op jit(solution)/shard_map/ppermute | solution.py:289
  119.4 0.1 add_convert_fusion
  119.5 0.1 collective-permute-start.12
  119.7 2.0 %shard_map.157.kept_ref = bf16[1536,128]{1,0:T(8,128)(2,1)S(1)} custom-call(bf16[1536,128]{1,0:T(8,128)(2,1)S(1)} %bitcast.28, bf16[2048,768]{1,0:T(8,128)(2,1)S(1)} %bitcast.21, bf16[2048,768]{1,0:T(8,128)(2,1)S(1)} %bitcast.24, bf16[768,2048]{1,0:T(8,128)(2,1)S(1)} %bitcast.27), custom_call_target="tpu_custom_call" | custom-call | flops 1536000000 | bytes 10223616 | tf_op jit(solution)/shard_map/pallas_call | solution.py:36
  121.7 4.8 %collective-permute-done.12.left_2_ref = bf16[768,128]{1,0:T(8,128)(2,1)S(1)} collective-permute-done((bf16[768,128]{1,0:T(8,128)(2,1)S(1)}, bf16[768,128]{1,0:T(8,128)(2,1)S(1)}, u32[]{:S(2)}, u32[]{:S(2)}) %collective-permute-start.12) | collective-permute-done | bytes 196640 | tf_op jit(solution)/shard_map/ppermute | solution.py:289
  126.5 0.9 shard_map.160
  127.4 4.8 %all-to-all-start.2 = ((bf16[32,48,128]{2,1,0:T(8,128)(2,1)}), bf16[32,48,128]{2,1,0:T(8,128)(2,1)S(1)}, u32[]{:S(2)}, u32[]{:S(2)}) async-start(bf16[32,48,128]{2,1,0:T(8,128)(2,1)} %bitcast.15), calls=%async_computation.2 | async-start | bytes 786432 | tf_op jit(solution)/shard_map/all_to_all | solution.py:331
  132.2 0.1 copy.17.ids_ref
  132.3 0.1 copy.18.weights_ref
  132.4 27.5 %all-to-all-done.2 = bf16[32,48,128]{2,1,0:T(8,128)(2,1)S(1)} async-done(((bf16[32,48,128]{2,1,0:T(8,128)(2,1)}), bf16[32,48,128]{2,1,0:T(8,128)(2,1)S(1)}, u32[]{:S(2)}, u32[]{:S(2)}) %all-to-all-start.2) | async-done | bytes 393248 | tf_op jit(solution)/shard_map/all_to_all | solution.py:331
  159.8 1.8 %shard_map.161 = bf16[48,2048]{1,0:T(8,128)(2,1)} custom-call(bf16[1536,128]{1,0:T(8,128)(2,1)S(1)} %bitcast.30, bf16[48,2048]{1,0:T(8,128)(2,1)S(1)} %get-tuple-element.38.normed_ref, s32[48,2]{1,0:T(8,128)S(1)} %copy.17.ids_ref, f32[48,2]{1,0:T(8,128)S(1)} %copy.18.weights_ref, f32[1,2048]{1,0:T(1,128)S(1)} %bitcast.35, f32[1,2048]{1,0:T(1,128)S(1)} %bitcast.36), custom_call_target="tpu_custom_call" | custom-call | flops 1000000000 | bytes 803584 | tf_op jit(solution)/shard_map/pallas_call | solution.py:36
  (31 shorter events, 0.1 us)
Async XLA Ops:
  0.0 28.8 %copy-start.3 = (s32[48,2]{0,1:T(2,128)S(1)}, s32[48,2]{0,1:T(2,128)}, u32[]{:S(2)}) copy-start(s32[48,2]{0,1:T(2,128)} %param.25) | copy-start | bytes 1156
  0.0 28.8 %copy-start.4 = (f32[2048]{0:T(1024)S(1)}, f32[2048]{0:T(1024)}, u32[]{:S(2)}) copy-start(f32[2048]{0:T(1024)} %param.23) | copy-start | bytes 24580
  0.0 28.8 %copy-start.5 = (f32[2048]{0:T(1024)S(1)}, f32[2048]{0:T(1024)}, u32[]{:S(2)}) copy-start(f32[2048]{0:T(1024)} %param.24) | copy-start | bytes 24580
  1.5 3.2 %collective-permute-start = (bf16[144,128]{1,0:T(8,128)(2,1)S(1)}, bf16[144,128]{1,0:T(8,128)(2,1)S(1)}, u32[]{:S(2)}, u32[]{:S(2)}) collective-permute-start(bf16[144,128]{1,0:T(8,128)(2,1)S(1)} %get-tuple-element.27), channel_id=1, source_target_pairs={{0,4},{4,8},{8,12},{12,16},{16,20},{20,24},{24,28},{28,32},{32,36}... | collective-permute-start | bytes 110600 | tf_op jit(solution)/shard_map/ppermute | solution.py:258
  3.3 5.6 %collective-permute-start.1 = (bf16[144,128]{1,0:T(8,128)(2,1)S(1)}, bf16[144,128]{1,0:T(8,128)(2,1)S(1)}, u32[]{:S(2)}, u32[]{:S(2)}) collective-permute-start(bf16[144,128]{1,0:T(8,128)(2,1)S(1)} %get-tuple-element.28), channel_id=1, source_target_pairs={{4,0},{8,4},{12,8},{16,12},{20,16},{24,20},{28,24},{32,28},{36,32}... | collective-permute-start | bytes 110600 | tf_op jit(solution)/shard_map/ppermute | solution.py:259
  8.9 89.9 %copy-start.2 = (bf16[1,768,2048]{2,1,0:T(8,128)(2,1)S(1)}, bf16[1,768,2048]{2,1,0:T(8,128)(2,1)}, u32[]{:S(2)}) copy-start(bf16[1,768,2048]{2,1,0:T(8,128)(2,1)} %param.29) | copy-start | bytes 9437188
  11.8 87.0 %copy-start = (bf16[1,2048,768]{2,1,0:T(8,128)(2,1)S(1)}, bf16[1,2048,768]{2,1,0:T(8,128)(2,1)}, u32[]{:S(2)}) copy-start(bf16[1,2048,768]{2,1,0:T(8,128)(2,1)} %param.27) | copy-start | bytes 9437188
  11.8 87.0 %copy-start.1 = (bf16[1,2048,768]{2,1,0:T(8,128)(2,1)S(1)}, bf16[1,2048,768]{2,1,0:T(8,128)(2,1)}, u32[]{:S(2)}) copy-start(bf16[1,2048,768]{2,1,0:T(8,128)(2,1)} %param.28) | copy-start | bytes 9437188
  82.3 8.0 %collective-permute-start.2 = (bf16[768,128]{1,0:T(8,128)(2,1)S(1)}, bf16[768,128]{1,0:T(8,128)(2,1)S(1)}, u32[]{:S(2)}, u32[]{:S(2)}) collective-permute-start(bf16[768,128]{1,0:T(8,128)(2,1)S(1)} %bitcast.37), channel_id=1, source_target_pairs={{0,1},{1,2},{2,3},{3,0},{4,5},{5,6},{6,7},{7,4},{8,9},{9,10},{10,1... | collective-permute-start | bytes 589832 | tf_op jit(solution)/shard_map/ppermute | solution.py:289
  83.0 7.3 %collective-permute-start.5 = (bf16[768,128]{1,0:T(8,128)(2,1)S(1)}, bf16[768,128]{1,0:T(8,128)(2,1)S(1)}, u32[]{:S(2)}, u32[]{:S(2)}) collective-permute-start(bf16[768,128]{1,0:T(8,128)(2,1)S(1)} %bitcast.39), channel_id=1, source_target_pairs={{0,3},{1,0},{2,1},{3,2},{4,7},{5,4},{6,5},{7,6},{8,11},{9,8},{10,9... | collective-permute-start | bytes 589832 | tf_op jit(solution)/shard_map/ppermute | solution.py:289
  90.3 8.5 %collective-permute-start.7 = (bf16[768,128]{1,0:T(8,128)(2,1)S(1)}, bf16[768,128]{1,0:T(8,128)(2,1)S(1)}, u32[]{:S(2)}, u32[]{:S(2)}) collective-permute-start(bf16[768,128]{1,0:T(8,128)(2,1)S(1)} %collective-permute-done.2.refs_0_), channel_id=1, source_target_pairs={{0,1},{1,2},{2,3},{3,0},{4,5},{5,6},{6,7},{7,4},{8,9},{9,10},{10,1... | collective-permute-start | bytes 589832 | tf_op jit(solution)/shard_map/ppermute | solution.py:289
  90.3 8.5 %collective-permute-start.8 = (bf16[768,128]{1,0:T(8,128)(2,1)S(1)}, bf16[768,128]{1,0:T(8,128)(2,1)S(1)}, u32[]{:S(2)}, u32[]{:S(2)}) collective-permute-start(bf16[768,128]{1,0:T(8,128)(2,1)S(1)} %collective-permute-done.5.refs_3_), channel_id=1, source_target_pairs={{0,3},{1,0},{2,1},{3,2},{4,7},{5,4},{6,5},{7,6},{8,11},{9,8},{10,9... | collective-permute-start | bytes 589832 | tf_op jit(solution)/shard_map/ppermute | solution.py:289
  93.5 10.9 %collective-permute-start.3 = (bf16[768,128]{1,0:T(8,128)(2,1)S(1)}, bf16[768,128]{1,0:T(8,128)(2,1)S(1)}, u32[]{:S(2)}, u32[]{:S(2)}) collective-permute-start(bf16[768,128]{1,0:T(8,128)(2,1)S(1)} %bitcast.40), channel_id=1, source_target_pairs={{0,1},{1,2},{2,3},{3,0},{4,5},{5,6},{6,7},{7,4},{8,9},{9,10},{10,1... | collective-permute-start | bytes 589832 | tf_op jit(solution)/shard_map/ppermute | solution.py:289
  93.5 10.9 %collective-permute-start.4 = (bf16[768,128]{1,0:T(8,128)(2,1)S(1)}, bf16[768,128]{1,0:T(8,128)(2,1)S(1)}, u32[]{:S(2)}, u32[]{:S(2)}) collective-permute-start(bf16[768,128]{1,0:T(8,128)(2,1)S(1)} %bitcast.38), channel_id=1, source_target_pairs={{0,3},{1,0},{2,1},{3,2},{4,7},{5,4},{6,5},{7,6},{8,11},{9,8},{10,9... | collective-permute-start | bytes 589832 | tf_op jit(solution)/shard_map/ppermute | solution.py:289
  100.8 9.8 %collective-permute-start.9 = (bf16[768,128]{1,0:T(8,128)(2,1)S(1)}, bf16[768,128]{1,0:T(8,128)(2,1)S(1)}, u32[]{:S(2)}, u32[]{:S(2)}) collective-permute-start(bf16[768,128]{1,0:T(8,128)(2,1)S(1)} %get-tuple-element.34), channel_id=1, source_target_pairs={{0,3},{1,0},{2,1},{3,2},{4,7},{5,4},{6,5},{7,6},{8,11},{9,8},{10,9... | collective-permute-start | bytes 589832 | tf_op jit(solution)/shard_map/ppermute | solution.py:289
  107.3 14.4 %collective-permute-start.6 = (bf16[768,128]{1,0:T(8,128)(2,1)S(1)}, bf16[768,128]{1,0:T(8,128)(2,1)S(1)}, u32[]{:S(2)}, u32[]{:S(2)}) collective-permute-start(bf16[768,128]{1,0:T(8,128)(2,1)S(1)} %get-tuple-element.32), channel_id=1, source_target_pairs={{0,1},{1,2},{2,3},{3,0},{4,5},{5,6},{6,7},{7,4},{8,9},{9,10},{10,1... | collective-permute-start | bytes 589832 | tf_op jit(solution)/shard_map/ppermute | solution.py:289
  107.4 14.2 %collective-permute-start.13 = (bf16[768,128]{1,0:T(8,128)(2,1)S(1)}, bf16[768,128]{1,0:T(8,128)(2,1)S(1)}, u32[]{:S(2)}, u32[]{:S(2)}) collective-permute-start(bf16[768,128]{1,0:T(8,128)(2,1)S(1)} %get-tuple-element.37), channel_id=1, source_target_pairs={{0,3},{1,0},{2,1},{3,2},{4,7},{5,4},{6,5},{7,6},{8,11},{9,8},{10,9... | collective-permute-start | bytes 589832 | tf_op jit(solution)/shard_map/ppermute | solution.py:289
  110.6 8.8 %collective-permute-start.11 = (bf16[768,128]{1,0:T(8,128)(2,1)S(1)}, bf16[768,128]{1,0:T(8,128)(2,1)S(1)}, u32[]{:S(2)}, u32[]{:S(2)}) collective-permute-start(bf16[768,128]{1,0:T(8,128)(2,1)S(1)} %get-tuple-element.36), channel_id=1, source_target_pairs={{0,1},{1,2},{2,3},{3,0},{4,5},{5,6},{6,7},{7,4},{8,9},{9,10},{10,1... | collective-permute-start | bytes 589832 | tf_op jit(solution)/shard_map/ppermute | solution.py:289
  110.7 11.0 %collective-permute-start.10 = (bf16[768,128]{1,0:T(8,128)(2,1)S(1)}, bf16[768,128]{1,0:T(8,128)(2,1)S(1)}, u32[]{:S(2)}, u32[]{:S(2)}) collective-permute-start(bf16[768,128]{1,0:T(8,128)(2,1)S(1)} %add_convert_fusion.1), channel_id=1, source_target_pairs={{0,3},{1,0},{2,1},{3,2},{4,7},{5,4},{6,5},{7,6},{8,11},{9,8},{10,9... | collective-permute-start | bytes 589832 | tf_op jit(solution)/shard_map/ppermute | solution.py:289
  119.5 7.0 %collective-permute-start.12 = (bf16[768,128]{1,0:T(8,128)(2,1)S(1)}, bf16[768,128]{1,0:T(8,128)(2,1)S(1)}, u32[]{:S(2)}, u32[]{:S(2)}) collective-permute-start(bf16[768,128]{1,0:T(8,128)(2,1)S(1)} %add_convert_fusion), channel_id=1, source_target_pairs={{0,1},{1,2},{2,3},{3,0},{4,5},{5,6},{6,7},{7,4},{8,9},{9,10},{10,1... | collective-permute-start | bytes 589832 | tf_op jit(solution)/shard_map/ppermute | solution.py:289
  119.6 12.6 %copy-start.8 = (f32[48,2]{0,1:T(2,128)S(1)}, f32[48,2]{0,1:T(2,128)}, u32[]{:S(2)}) copy-start(f32[48,2]{0,1:T(2,128)} %param.26) | copy-start | bytes 1156
  119.6 40.2 %copy-start.6 = (f32[2048]{0:T(1024)S(1)}, f32[2048]{0:T(1024)}, u32[]{:S(2)}) copy-start(f32[2048]{0:T(1024)} %param.30) | copy-start | bytes 24580
  119.7 40.2 %copy-start.7 = (f32[2048]{0:T(1024)S(1)}, f32[2048]{0:T(1024)}, u32[]{:S(2)}) copy-start(f32[2048]{0:T(1024)} %param.31) | copy-start | bytes 24580
  127.4 32.5 %all-to-all-start.2 = ((bf16[32,48,128]{2,1,0:T(8,128)(2,1)}), bf16[32,48,128]{2,1,0:T(8,128)(2,1)S(1)}, u32[]{:S(2)}, u32[]{:S(2)}) async-start(bf16[32,48,128]{2,1,0:T(8,128)(2,1)} %bitcast.15), calls=%async_computation.2 | async-start | bytes 786432 | tf_op jit(solution)/shard_map/all_to_all | solution.py:331
where the time goes:
time: 163 us; the launch traced here: 162 us
  blocking collectives  69.7 us (43%)
  waiting for transfers between devices  48.6 us (30%)
  starting transfers between devices  28.2 us (17%)
  Pallas kernels  14.6 us (9%)
    all_to_all x1, blocking collectives, per_device(): arrived = lax.all_to_all(sent, 'sp', 0, 0, tiled=True)  52.8 us
    all_to_all x1, waiting for transfers between devices, per_device(): back = lax.all_to_all(summed, 'sp', 0, 0, tiled=True)  27.5 us
    ppermute x12, starting transfers between devices, turned(): lax.ppermute(array, 'tp', [(i, (i + by) % members) for i in range(members)])  20.2 us
    all_to_all x1, blocking collectives, per_device(): lax.all_to_all(partial.reshape(members, own, width), 'tp', 0, 0, tiled=True)  16.9 us
    ppermute x12, waiting for transfers between devices, turned(): lax.ppermute(array, 'tp', [(i, (i + by) % members) for i in range(members)])  16.9 us
    pallas_call x8, Pallas kernels, call(): pl.pallas_call(body, out_shape=out_shapes, in_specs=specs or [VMEM] * len...  14.6 us
    all_to_all x1, starting transfers between devices, per_device(): back = lax.all_to_all(summed, 'sp', 0, 0, tiled=True)  4.79 us
    ppermute x1, waiting for transfers between devices, per_device(): lax.ppermute(head, 'sp', [(i + 1, i) for i in range(blocks - 1)])  4.3 us
  transfers between devices with their start and end apart: 15, of which 6 were waited for; matrix products, arithmetic and copies ran while one was open for 0% of the time, Pallas kernels for 4%

commit v1 on v0

--- a/solution.py
+++ b/solution.py
@@ -5,6 +5,7 @@
 from jax import lax
 from jax.experimental import pallas as pl
 from jax.experimental.pallas import tpu as pltpu
+from jax.sharding import Mesh
 from jax.sharding import PartitionSpec as P
 
 
@@ -14,6 +15,7 @@
 NORM_EPSILON = 1e-05
 RESIDUAL_SCALE = 1.4142135623730951
 MASKED = -1e30
+SP = ("chip", "core")
 F32 = jnp.float32
 BF16 = jnp.bfloat16
 
@@ -28,6 +30,10 @@
 
 def mm_nt(a, b):
     return lax.dot_general(a, b, (((1,), (1,)), ((), ())), preferred_element_type=F32)
+
+
+def mm_tn(a, b):
+    return lax.dot_general(a, b, (((0,), (0,)), ((), ())), preferred_element_type=F32)
 
 
 def call(body, out_shapes, *args, flops, specs=None, scratch=(), vmem=None):
@@ -54,11 +60,12 @@
     return centred * lax.rsqrt(variance + NORM_EPSILON) * gain + bias
 
 
-def first_body(count, *refs):
-    sources, held, (head_ref, tail_ref, sems) = refs[:count], refs[count : 2 * count], refs[2 * count :]
+def first_body(count, core_ref, *refs):
+    sources, held, (head_ref, tail_ref, core_out_ref, sems) = refs[:count], refs[count : 2 * count], refs[2 * count :]
     copies = [pltpu.make_async_copy(a, b, sems.at[i]) for i, (a, b) in enumerate(zip(sources, held))]
     for copy in copies:
         copy.start()
+    core_out_ref[...] = core_ref[...]
     for copy in copies[:3]:
         copy.wait()
     keys_ref, values_ref, docs_ref = held[:3]
@@ -116,20 +123,34 @@
     out_ref[...] = mm(att_ref[...], proj_ref[...]).astype(BF16)
 
 
-def routing_rows(ids, experts, tokens):
-    expert = lax.broadcasted_iota(jnp.int32, (experts, tokens), 0)
+def routing_rows(ids, expert, weights=None):
+    experts, tokens = expert.shape
     named = jnp.zeros((experts, tokens), F32)
+    weighted = jnp.zeros((experts, tokens), F32)
     for k in range(ids.shape[0]):
-        named += (ids[k : k + 1, :] == expert).astype(F32)
+        hit = ids[k : k + 1, :] == expert
+        named += hit.astype(F32)
+        if weights is not None:
+            weighted += jnp.where(hit, weights[k : k + 1, :], 0.0)
     before = lax.broadcasted_iota(jnp.int32, (tokens, tokens), 0) < lax.broadcasted_iota(
         jnp.int32, (tokens, tokens), 1
     )
-    rank = mm(named.astype(BF16), before.astype(BF16))
-    return named, rank
+    rank = jnp.where(named > 0.5, mm(named.astype(BF16), before.astype(BF16)), -1.0)
+    return (named if weights is None else weighted), rank
 
 
 def dispatch_body(
-    experts, parts_ref, resid_ref, gain_ref, bias_ref, ids_ref, normed_ref, sent_ref, wide_ref
+    experts,
+    parts_ref,
+    resid_ref,
+    gain_ref,
+    bias_ref,
+    ids_ref,
+    core_ref,
+    normed_ref,
+    same_ref,
+    other_ref,
+    wide_ref,
 ):
     tokens, width = resid_ref.shape
     tiles = width // LANES
@@ -138,15 +159,29 @@
     pre_norm = RESIDUAL_SCALE * resid_ref[...].astype(F32) + projected.astype(BF16).astype(F32)
     normed = layer_norm(pre_norm, gain_ref[...], bias_ref[...]).astype(BF16)
     normed_ref[...] = normed
-    named, rank = routing_rows(ids_ref[...], experts, tokens)
+    chips = experts // 2
+    row = lax.broadcasted_iota(jnp.int32, (experts, tokens), 0)
+    core = jnp.broadcast_to(core_ref[:, 0:1], (experts, tokens))
+    expert = jnp.where(row < chips, 2 * row + core, 2 * (row - chips) + 1 - core)
+    named, rank = routing_rows(ids_ref[...], expert)
     for j in range(capacity):
-        pick = jnp.where((named > 0.5) & (jnp.abs(rank - j) < 0.5), 1.0, 0.0).astype(BF16)
+        pick = jnp.where(jnp.abs(rank - j) < 0.5, named, 0.0).astype(BF16)
         rows = mm(pick, normed)
         for c in range(tiles):
             wide_ref[pl.ds(j * tiles + c, experts, stride=capacity * tiles), :] = rows[
                 :, c * LANES : (c + 1) * LANES
             ]
-    sent_ref[...] = wide_ref[...].astype(BF16)
+    half = same_ref.shape[0]
+    same_ref[...] = wide_ref[0:half, :].astype(BF16)
+    other_ref[...] = wide_ref[half:, :].astype(BF16)
+
+
+def pair_body(same_ref, other_ref, core_ref, out_ref):
+    per_expert = same_ref.shape[1]
+    first_core = jnp.broadcast_to(core_ref[...], same_ref.shape) == 0
+    same, other = same_ref[...].astype(F32), other_ref[...].astype(F32)
+    out_ref[:, 0:per_expert, :] = jnp.where(first_core, same, other).astype(BF16)
+    out_ref[:, per_expert:, :] = jnp.where(first_core, other, same).astype(BF16)
 
 
 def expert_body(count, *refs):
@@ -188,23 +223,13 @@
 ):
     tokens, width = normed_ref.shape
     tiles = width // LANES
-    top = ids_ref.shape[1]
-    capacity = top * tokens // experts
+    capacity = ids_ref.shape[0] * tokens // experts
     wide_ref[...] = back_ref[...].astype(F32)
-    expert = lax.broadcasted_iota(jnp.int32, (tokens, experts), 1)
-    named = jnp.zeros((tokens, experts), F32)
-    weighted = jnp.zeros((tokens, experts), F32)
-    for k in range(top):
-        hit = ids_ref[:, k : k + 1] == expert
-        named += hit.astype(F32)
-        weighted += jnp.where(hit, weights_ref[:, k : k + 1], 0.0)
-    earlier = lax.broadcasted_iota(jnp.int32, (tokens, tokens), 1) < lax.broadcasted_iota(
-        jnp.int32, (tokens, tokens), 0
-    )
-    rank = mm(earlier.astype(BF16), named.astype(BF16))
+    expert = lax.broadcasted_iota(jnp.int32, (experts, tokens), 0)
+    weighted, rank = routing_rows(ids_ref[...], expert, weights_ref[...])
     moe_sum = 0.0
     for j in range(capacity):
-        pick = jnp.where((named > 0.5) & (jnp.abs(rank - j) < 0.5), weighted, 0.0)
+        pick = jnp.where(jnp.abs(rank - j) < 0.5, weighted, 0.0)
         for c in range(tiles):
             rows_ref[:, c * LANES : (c + 1) * LANES] = wide_ref[
                 pl.ds(j * tiles + c, experts, stride=capacity * tiles), :
@@ -214,7 +239,7 @@
         middle = low.astype(BF16)
         last = (low - middle.astype(F32)).astype(BF16)
         rows = rows_ref[...]
-        moe_sum = moe_sum + (mm(high, rows) + (mm(middle, rows) + mm(last, rows)))
+        moe_sum = moe_sum + (mm_tn(high, rows) + (mm_tn(middle, rows) + mm_tn(last, rows)))
     pre_final = RESIDUAL_SCALE * normed_ref[...].astype(F32) + moe_sum
     out_ref[...] = layer_norm(pre_final, gain_ref[...], bias_ref[...]).astype(BF16)
 
@@ -239,7 +264,7 @@
 ):
     tokens = queries.shape[0]
     own, width = resid.shape
-    blocks, members = lax.axis_size("sp"), lax.axis_size("tp")
+    blocks, members = lax.axis_size(SP), lax.axis_size("tp")
     experts = blocks
     capacity = route_ids.shape[1] * own // experts
     tiles = width // LANES
@@ -247,16 +272,18 @@
 
     small = (keys.T, values.T, doc_ids.reshape(1, tokens), queries, out_proj, resid, sink_logits.reshape(1, -1))
     pack = shape((2 * HEAD_DIM + 16, WINDOW), BF16)
-    keys_t, values_t, docs, queries, out_proj, resid, sinks, head, tail = call(
+    core = jnp.full((1, LANES), lax.axis_index("core"), jnp.int32)
+    keys_t, values_t, docs, queries, out_proj, resid, sinks, head, tail, core = call(
         functools.partial(first_body, len(small)),
-        [shape(a.shape, a.dtype) for a in small] + [pack, pack],
+        [shape(a.shape, a.dtype) for a in small] + [pack, pack, shape(core.shape, core.dtype)],
+        core,
         *[pltpu.with_memory_space_constraint(a, pltpu.HBM) for a in small],
         flops=10**5,
-        specs=[HBM] * len(small),
+        specs=[VMEM] + [HBM] * len(small),
         scratch=[pltpu.SemaphoreType.DMA((len(small),))],
     )
-    previous = lax.ppermute(tail, "sp", [(i, i + 1) for i in range(blocks - 1)])
-    following = lax.ppermute(head, "sp", [(i + 1, i) for i in range(blocks - 1)])
+    previous = lax.ppermute(tail, SP, [(i, i + 1) for i in range(blocks - 1)])
+    following = lax.ppermute(head, SP, [(i + 1, i) for i in range(blocks - 1)])
     (partial,) = call(
         attention_body,
         [shape((tokens, width), BF16)],
@@ -272,18 +299,29 @@
         scratch=[pltpu.VMEM(queries.shape, BF16)],
     )
     parts = lax.all_to_all(partial.reshape(members, own, width), "tp", 0, 0, tiled=True)
-    normed, sent = call(
+    normed, same, other = call(
         functools.partial(dispatch_body, experts),
-        [shape((own, width), BF16), shape((packed, LANES), BF16)],
+        [shape((own, width), BF16)] + [shape((packed // 2, LANES), BF16)] * 2,
         parts,
         resid,
         norm1_gain.reshape(1, -1),
         norm1_bias.reshape(1, -1),
         route_ids.T,
+        core,
         flops=10**9,
         scratch=[pltpu.VMEM((packed, LANES), F32)],
     )
-    arrived = lax.all_to_all(sent, "sp", 0, 0, tiled=True)
+    other = lax.ppermute(other, "core", [(0, 1), (1, 0)])
+    per_expert = capacity * tiles
+    (sent,) = call(
+        pair_body,
+        [shape((experts // 2, 2 * per_expert, LANES), BF16)],
+        same.reshape(-1, per_expert, LANES),
+        other.reshape(-1, per_expert, LANES),
+        core,
+        flops=10**6,
+    )
+    arrived = lax.all_to_all(sent.reshape(packed, LANES), "chip", 0, 0, tiled=True)
 
     def turned(array, by):
         return lax.ppermute(array, "tp", [(i, (i + by) % members) for i in range(members)])
@@ -328,14 +366,14 @@
         from_right_2,
         flops=10**7,
     )
-    back = lax.all_to_all(summed, "sp", 0, 0, tiled=True)
+    back = lax.all_to_all(summed, SP, 0, 0, tiled=True)
     (mixed,) = call(
         functools.partial(combine_body, experts),
         [shape((own, width), BF16)],
         back,
         normed,
-        route_ids,
-        route_weights,
+        route_ids.T,
+        route_weights.T,
         norm2_gain.reshape(1, -1),
         norm2_bias.reshape(1, -1),
         flops=10**9,
@@ -345,8 +383,12 @@
 
 
 def solution(mesh):
-    every = ("grp", "sp", "tp")
-    group = ("grp", "sp")
+    groups, cores = mesh.shape["grp"], 2
+    chips = mesh.shape["sp"] // cores
+    devices = mesh.devices.reshape(groups, chips, cores, mesh.shape["tp"])
+    mesh = Mesh(devices, ("grp", *SP, "tp"))
+    every = ("grp", *SP, "tp")
+    group = ("grp", *SP)
     placed = (
         P(every, None),
         P(group, "tp"),
@@ -359,9 +401,9 @@
         P(),
         P(every, None),
         P(every, None),
-        P("sp", None, "tp"),
-        P("sp", None, "tp"),
-        P("sp", "tp", None),
+        P(SP, None, "tp"),
+        P(SP, None, "tp"),
+        P(SP, "tp", None),
         P(),
         P(),
     )

time: 163 us -> 161 us (0.988)
  blocking collectives: 69.7 us -> 102 us
  waiting for transfers between devices: 48.6 us -> 19.5 us
  starting transfers between devices: 28.2 us -> 24.7 us
    all_to_all x1 -> x2, blocking collectives: 52.8 us -> 84.7 us  [the longest x1 47.7 us: per_device(): lax.all_to_all(sent.reshape(packed, LANES), 'chip', 0, 0, tiled=True)]
    all_to_all x1 -> x0, waiting for transfers between devices: 27.5 us -> none  [per_device(): back = lax.all_to_all(summed, 'sp', 0, 0, tiled=True)]
    all_to_all x1 -> x0, starting transfers between devices: 4.79 us -> none  [per_device(): back = lax.all_to_all(summed, 'sp', 0, 0, tiled=True)]
    ppermute x12, waiting for transfers between devices: 16.9 us -> 14.1 us  [turned(): lax.ppermute(array, 'tp', [(i, (i + by) % members) for i in range(members)])]
    ppermute x2 -> x3, starting transfers between devices: 3.15 us -> 4.52 us  [the longest x1 1.84 us: per_device(): previous = lax.ppermute(tail, SP, [(i, i + 1) for i in range(blocks - 1)])]
    ppermute x2 -> x3, waiting for transfers between devices: 4.31 us -> 5.38 us  [the longest x1 4.3 us: per_device(): following = lax.ppermute(head, SP, [(i + 1, i) for i in range(blocks - 1)])]
    pallas_call x8 -> x9, Pallas kernels: 14.6 us -> 14 us  [call(): pl.pallas_call(body, out_shape=out_shapes, in_specs=specs or [VMEM] * len...]
where the time goes in v1:
time: 161 us; the launch traced here: 160 us
  blocking collectives  102 us (63%)
  starting transfers between devices  24.7 us (15%)
  waiting for transfers between devices  19.5 us (12%)
  Pallas kernels  14 us (9%)
    all_to_all x1, blocking collectives, per_device(): lax.all_to_all(sent.reshape(packed, LANES), 'chip', 0, 0, tiled=True)  47.7 us
    all_to_all x1, blocking collectives, per_device(): back = lax.all_to_all(summed, SP, 0, 0, tiled=True)  37 us
    ppermute x12, starting transfers between devices, turned(): lax.ppermute(array, 'tp', [(i, (i + by) % members) for i in range(members)])  20.2 us
    all_to_all x1, blocking collectives, per_device(): lax.all_to_all(partial.reshape(members, own, width), 'tp', 0, 0, tiled=True)  16.9 us
    ppermute x12, waiting for transfers between devices, turned(): lax.ppermute(array, 'tp', [(i, (i + by) % members) for i in range(members)])  14.1 us
    pallas_call x9, Pallas kernels, call(): pl.pallas_call(body, out_shape=out_shapes, in_specs=specs or [VMEM] * len...  14 us
    ppermute x1, waiting for transfers between devices, per_device(): following = lax.ppermute(head, SP, [(i + 1, i) for i in range(blocks - 1)])  4.3 us
  transfers between devices with their start and end apart: 15, of which 6 were waited for; matrix products, arithmetic and copies ran while one was open for 0% of the time, Pallas kernels for 4%

profile of v1, /device:TPU:40, one launch (start us, length us, event | category | flops | bytes accessed | tf_op | source)
XLA Modules:
  0.0 160.2 jit_solution(1566617087543860967)
XLA Ops:
  0.0 1.4 shard_map.154
  1.5 1.8 %collective-permute-start = (bf16[144,128]{1,0:T(8,128)(2,1)S(1)}, bf16[144,128]{1,0:T(8,128)(2,1)S(1)}, u32[]{:S(2)}, u32[]{:S(2)}) collective-permute-start(bf16[144,128]{1,0:T(8,128)(2,1)S(1)} %get-tuple-element.29), channel_id=1, source_target_pairs={{0,4},{4,8},{8,12},{12,16},{16,20},{20,24},{24,28},{28,32},{32,36}... | collective-permute-start | bytes 110600 | tf_op jit(solution)/shard_map/ppermute | solution.py:285
  3.3 1.3 collective-permute-start.1
  4.6 4.3 %collective-permute-done.1.next_ref = bf16[144,128]{1,0:T(8,128)(2,1)S(1)} collective-permute-done((bf16[144,128]{1,0:T(8,128)(2,1)S(1)}, bf16[144,128]{1,0:T(8,128)(2,1)S(1)}, u32[]{:S(2)}, u32[]{:S(2)}) %collective-permute-start.1) | collective-permute-done | bytes 36896 | tf_op jit(solution)/shard_map/ppermute | solution.py:286
  8.9 2.9 %shard_map.155 = bf16[192,2048]{1,0:T(8,128)(2,1)S(1)} custom-call(f32[1,4]{1,0:T(1,128)S(1)} %get-tuple-element.24.sink_ref, bf16[192,256]{1,0:T(8,128)(2,1)S(1)} %get-tuple-element.25.query_ref, bf16[64,192]{1,0:T(8,128)(2,1)S(1)} %get-tuple-element.26.keys_ref, bf16[64,192]{1,0:T(8,128)(2,1)S(1)} %get-tuple-element.27.values_ref, ...), custom_call_target="tpu_custom_call" | custom-call | flops 1000000000 | bytes 2056976 | tf_op jit(solution)/shard_map/pallas_call | solution.py:42
  11.8 16.9 %all_to_all.24.parts_ref = bf16[4,48,2048]{2,1,0:T(8,128)(2,1)S(1)} all-to-all(bf16[4,48,2048]{2,1,0:T(8,128)(2,1)S(1)} %bitcast.32), channel_id=1, replica_groups=mesh['grp'=2,'chip'=16,'core'=2,'tp'=4] {'tp'}, dimensions={0} | all-to-all | bytes 1572864 | tf_op jit(solution)/shard_map/all_to_all | solution.py:301
  28.8 0.8 shard_map.156
  29.5 1.4 collective-permute-start.2
  30.9 1.1 collective-permute-done.2
  32.0 0.1 shard_map.157
  32.1 47.7 %all_to_all.25 = bf16[16,96,128]{2,1,0:T(8,128)(2,1)S(1)} all-to-all(bf16[16,96,128]{2,1,0:T(8,128)(2,1)S(1)} %shard_map.157), channel_id=1, replica_groups=mesh['grp'=2,'chip'=16,'core'=2,'tp'=4] {'chip'}, dimensions={0} | all-to-all | bytes 786432 | tf_op jit(solution)/shard_map/all_to_all | solution.py:324
  79.8 0.7 collective-permute-start.3
  80.5 2.7 %collective-permute-start.6 = (bf16[768,128]{1,0:T(8,128)(2,1)S(1)}, bf16[768,128]{1,0:T(8,128)(2,1)S(1)}, u32[]{:S(2)}, u32[]{:S(2)}) collective-permute-start(bf16[768,128]{1,0:T(8,128)(2,1)S(1)} %bitcast.45), channel_id=1, source_target_pairs={{0,3},{1,0},{2,1},{3,2},{4,7},{5,4},{6,5},{7,6},{8,11},{9,8},{10,9... | collective-permute-start | bytes 589832 | tf_op jit(solution)/shard_map/ppermute | solution.py:327
  83.1 5.4 %collective-permute-done.3.refs_0_ = bf16[768,128]{1,0:T(8,128)(2,1)S(1)} collective-permute-done((bf16[768,128]{1,0:T(8,128)(2,1)S(1)}, bf16[768,128]{1,0:T(8,128)(2,1)S(1)}, u32[]{:S(2)}, u32[]{:S(2)}) %collective-permute-start.3) | collective-permute-done | bytes 196640 | tf_op jit(solution)/shard_map/ppermute | solution.py:327
  88.6 3.2 %collective-permute-start.9 = (bf16[768,128]{1,0:T(8,128)(2,1)S(1)}, bf16[768,128]{1,0:T(8,128)(2,1)S(1)}, u32[]{:S(2)}, u32[]{:S(2)}) collective-permute-start(bf16[768,128]{1,0:T(8,128)(2,1)S(1)} %collective-permute-done.6.refs_3_), channel_id=1, source_target_pairs={{0,3},{1,0},{2,1},{3,2},{4,7},{5,4},{6,5},{7,6},{8,11},{9,8},{10,9... | collective-permute-start | bytes 589832 | tf_op jit(solution)/shard_map/ppermute | solution.py:327
  91.8 3.2 %collective-permute-start.5 = (bf16[768,128]{1,0:T(8,128)(2,1)S(1)}, bf16[768,128]{1,0:T(8,128)(2,1)S(1)}, u32[]{:S(2)}, u32[]{:S(2)}) collective-permute-start(bf16[768,128]{1,0:T(8,128)(2,1)S(1)} %bitcast.44), channel_id=1, source_target_pairs={{0,3},{1,0},{2,1},{3,2},{4,7},{5,4},{6,5},{7,6},{8,11},{9,8},{10,9... | collective-permute-start | bytes 589832 | tf_op jit(solution)/shard_map/ppermute | solution.py:327
  95.0 0.4 collective-permute-done.8.refs_0_
  95.5 2.0 %shard_map.160 = (bf16[768,128]{1,0:T(8,128)(2,1)S(1)}, bf16[768,128]{1,0:T(8,128)(2,1)S(1)}) custom-call(bf16[768,128]{1,0:T(8,128)(2,1)S(1)} %collective-permute-done.8.refs_0_, bf16[768,128]{1,0:T(8,128)(2,1)S(1)} %collective-permute-done.9.refs_1_, bf16[2048,768]{1,0:T(8,128)(2,1)S(1)} %bitcast.21, bf16[2048,768]{1,0:T(8,128)(2,1)S(1)} %bitcast.24, ...), custom_call_target="tpu_custom_call" | custom-call | flops 1536000000 | bytes 10223616 | tf_op jit(solution)/shard_map/pallas_call | solution.py:42
  97.4 3.5 %collective-permute-start.10 = (bf16[768,128]{1,0:T(8,128)(2,1)S(1)}, bf16[768,128]{1,0:T(8,128)(2,1)S(1)}, u32[]{:S(2)}, u32[]{:S(2)}) collective-permute-start(bf16[768,128]{1,0:T(8,128)(2,1)S(1)} %get-tuple-element.38), channel_id=1, source_target_pairs={{0,3},{1,0},{2,1},{3,2},{4,7},{5,4},{6,5},{7,6},{8,11},{9,8},{10,9... | collective-permute-start | bytes 589832 | tf_op jit(solution)/shard_map/ppermute | solution.py:327
  101.0 2.9 %shard_map.159 = (bf16[768,128]{1,0:T(8,128)(2,1)S(1)}, bf16[768,128]{1,0:T(8,128)(2,1)S(1)}, bf16[768,128]{1,0:T(8,128)(2,1)S(1)}, bf16[768,128]{1,0:T(8,128)(2,1)S(1)}) custom-call(bf16[768,128]{1,0:T(8,128)(2,1)S(1)} %collective-permute-done.3.refs_0_, bf16[768,128]{1,0:T(8,128)(2,1)S(1)} %collective-permute-done.4.refs_1_, ...), custom_call_target="tpu_custom_call" | custom-call | flops 3072000000 | bytes 11010048 | tf_op jit(solution)/shard_map/pallas_call | solution.py:42
  103.8 0.1 collective-permute-start.7
  104.0 3.2 %collective-permute-start.14 = (bf16[768,128]{1,0:T(8,128)(2,1)S(1)}, bf16[768,128]{1,0:T(8,128)(2,1)S(1)}, u32[]{:S(2)}, u32[]{:S(2)}) collective-permute-start(bf16[768,128]{1,0:T(8,128)(2,1)S(1)} %get-tuple-element.41), channel_id=1, source_target_pairs={{0,3},{1,0},{2,1},{3,2},{4,7},{5,4},{6,5},{7,6},{8,11},{9,8},{10,9... | collective-permute-start | bytes 589832 | tf_op jit(solution)/shard_map/ppermute | solution.py:327
  107.2 0.1 add_convert_fusion.1
  107.3 3.3 %collective-permute-start.11 = (bf16[768,128]{1,0:T(8,128)(2,1)S(1)}, bf16[768,128]{1,0:T(8,128)(2,1)S(1)}, u32[]{:S(2)}, u32[]{:S(2)}) collective-permute-start(bf16[768,128]{1,0:T(8,128)(2,1)S(1)} %add_convert_fusion.1), channel_id=1, source_target_pairs={{0,3},{1,0},{2,1},{3,2},{4,7},{5,4},{6,5},{7,6},{8,11},{9,8},{10,9... | collective-permute-start | bytes 589832 | tf_op jit(solution)/shard_map/ppermute | solution.py:327
  110.6 3.5 %collective-permute-done.12 = bf16[768,128]{1,0:T(8,128)(2,1)S(1)} collective-permute-done((bf16[768,128]{1,0:T(8,128)(2,1)S(1)}, bf16[768,128]{1,0:T(8,128)(2,1)S(1)}, u32[]{:S(2)}, u32[]{:S(2)}) %collective-permute-start.12) | collective-permute-done | bytes 196640 | tf_op jit(solution)/shard_map/ppermute | solution.py:327
  114.1 0.1 add_convert_fusion
  114.1 0.1 collective-permute-start.13
  114.3 2.0 %shard_map.158.kept_ref = bf16[1536,128]{1,0:T(8,128)(2,1)S(1)} custom-call(bf16[1536,128]{1,0:T(8,128)(2,1)S(1)} %bitcast.30, bf16[2048,768]{1,0:T(8,128)(2,1)S(1)} %bitcast.23, bf16[2048,768]{1,0:T(8,128)(2,1)S(1)} %bitcast.26, bf16[768,2048]{1,0:T(8,128)(2,1)S(1)} %bitcast.29), custom_call_target="tpu_custom_call" | custom-call | flops 1536000000 | bytes 10223616 | tf_op jit(solution)/shard_map/pallas_call | solution.py:42
  116.3 4.8 %collective-permute-done.13.left_2_ref = bf16[768,128]{1,0:T(8,128)(2,1)S(1)} collective-permute-done((bf16[768,128]{1,0:T(8,128)(2,1)S(1)}, bf16[768,128]{1,0:T(8,128)(2,1)S(1)}, u32[]{:S(2)}, u32[]{:S(2)}) %collective-permute-start.13) | collective-permute-done | bytes 196640 | tf_op jit(solution)/shard_map/ppermute | solution.py:327
  121.1 0.1 shard_map.161
  121.3 37.0 %all_to_all.26 = bf16[32,48,128]{2,1,0:T(8,128)(2,1)S(1)} all-to-all(bf16[32,48,128]{2,1,0:T(8,128)(2,1)S(1)} %bitcast.31), channel_id=1, replica_groups=mesh['grp'=2,'chip'=16,'core'=2,'tp'=4] {'chip','core'}, dimensions={0} | all-to-all | bytes 786432 | tf_op jit(solution)/shard_map/all_to_all | solution.py:369
  158.3 1.8 %shard_map.162 = bf16[48,2048]{1,0:T(8,128)(2,1)} custom-call(bf16[1536,128]{1,0:T(8,128)(2,1)S(1)} %bitcast.33, bf16[48,2048]{1,0:T(8,128)(2,1)S(1)} %get-tuple-element.42.normed_ref, s32[2,48]{1,0:T(2,128)S(1)} %bitcast.41, f32[2,48]{1,0:T(2,128)S(1)} %bitcast.42, f32[1,2048]{1,0:T(1,128)S(1)} %bitcast.38, f32[1,2048]{1,0:T(1,128)S(1)} %bitcast.39), custom_call_target="tpu_custom_call" | custom-call | flops 1000000000 | bytes 803584 | tf_op jit(solution)/shard_map/pallas_call | solution.py:42
  (32 shorter events, 0.1 us)
Async XLA Ops:
  0.0 28.8 %copy-start.3 = (f32[2048]{0:T(1024)S(1)}, f32[2048]{0:T(1024)}, u32[]{:S(2)}) copy-start(f32[2048]{0:T(1024)} %param.23) | copy-start | bytes 24580
  0.0 28.8 %copy-start.4 = (f32[2048]{0:T(1024)S(1)}, f32[2048]{0:T(1024)}, u32[]{:S(2)}) copy-start(f32[2048]{0:T(1024)} %param.24) | copy-start | bytes 24580
  0.0 28.8 %copy-start.7 = (s32[48,2]{0,1:T(2,128)S(1)}, s32[48,2]{0,1:T(2,128)}, u32[]{:S(2)}) copy-start(s32[48,2]{0,1:T(2,128)} %param.25) | copy-start | bytes 1156
  1.5 3.2 %collective-permute-start = (bf16[144,128]{1,0:T(8,128)(2,1)S(1)}, bf16[144,128]{1,0:T(8,128)(2,1)S(1)}, u32[]{:S(2)}, u32[]{:S(2)}) collective-permute-start(bf16[144,128]{1,0:T(8,128)(2,1)S(1)} %get-tuple-element.29), channel_id=1, source_target_pairs={{0,4},{4,8},{8,12},{12,16},{16,20},{20,24},{24,28},{28,32},{32,36}... | collective-permute-start | bytes 110600 | tf_op jit(solution)/shard_map/ppermute | solution.py:285
  3.3 5.6 %collective-permute-start.1 = (bf16[144,128]{1,0:T(8,128)(2,1)S(1)}, bf16[144,128]{1,0:T(8,128)(2,1)S(1)}, u32[]{:S(2)}, u32[]{:S(2)}) collective-permute-start(bf16[144,128]{1,0:T(8,128)(2,1)S(1)} %get-tuple-element.30), channel_id=1, source_target_pairs={{4,0},{8,4},{12,8},{16,12},{20,16},{24,20},{28,24},{32,28},{36,32}... | collective-permute-start | bytes 110600 | tf_op jit(solution)/shard_map/ppermute | solution.py:286
  8.9 86.5 %copy-start.2 = (bf16[1,768,2048]{2,1,0:T(8,128)(2,1)S(1)}, bf16[1,768,2048]{2,1,0:T(8,128)(2,1)}, u32[]{:S(2)}) copy-start(bf16[1,768,2048]{2,1,0:T(8,128)(2,1)} %param.29) | copy-start | bytes 9437188
  11.8 83.6 %copy-start.1 = (bf16[1,2048,768]{2,1,0:T(8,128)(2,1)S(1)}, bf16[1,2048,768]{2,1,0:T(8,128)(2,1)}, u32[]{:S(2)}) copy-start(bf16[1,2048,768]{2,1,0:T(8,128)(2,1)} %param.28) | copy-start | bytes 9437188
  28.8 66.7 %copy-start = (bf16[1,2048,768]{2,1,0:T(8,128)(2,1)S(1)}, bf16[1,2048,768]{2,1,0:T(8,128)(2,1)}, u32[]{:S(2)}) copy-start(bf16[1,2048,768]{2,1,0:T(8,128)(2,1)} %param.27) | copy-start | bytes 9437188
  29.5 2.4 %collective-permute-start.2 = (bf16[768,128]{1,0:T(8,128)(2,1)S(1)}, bf16[768,128]{1,0:T(8,128)(2,1)S(1)}, u32[]{:S(2)}, u32[]{:S(2)}) collective-permute-start(bf16[768,128]{1,0:T(8,128)(2,1)S(1)} %get-tuple-element.35), channel_id=1, source_target_pairs={{0,4},{4,0},{1,5},{5,1},{2,6},{6,2},{3,7},{7,3},{8,12},{12,8},{9,1... | collective-permute-start | bytes 589832 | tf_op jit(solution)/shard_map/ppermute | solution.py:314
  79.8 8.8 %collective-permute-start.3 = (bf16[768,128]{1,0:T(8,128)(2,1)S(1)}, bf16[768,128]{1,0:T(8,128)(2,1)S(1)}, u32[]{:S(2)}, u32[]{:S(2)}) collective-permute-start(bf16[768,128]{1,0:T(8,128)(2,1)S(1)} %bitcast.43), channel_id=1, source_target_pairs={{0,1},{1,2},{2,3},{3,0},{4,5},{5,6},{6,7},{7,4},{8,9},{9,10},{10,1... | collective-permute-start | bytes 589832 | tf_op jit(solution)/shard_map/ppermute | solution.py:327
  80.5 8.1 %collective-permute-start.6 = (bf16[768,128]{1,0:T(8,128)(2,1)S(1)}, bf16[768,128]{1,0:T(8,128)(2,1)S(1)}, u32[]{:S(2)}, u32[]{:S(2)}) collective-permute-start(bf16[768,128]{1,0:T(8,128)(2,1)S(1)} %bitcast.45), channel_id=1, source_target_pairs={{0,3},{1,0},{2,1},{3,2},{4,7},{5,4},{6,5},{7,6},{8,11},{9,8},{10,9... | collective-permute-start | bytes 589832 | tf_op jit(solution)/shard_map/ppermute | solution.py:327
  88.6 6.9 %collective-permute-start.8 = (bf16[768,128]{1,0:T(8,128)(2,1)S(1)}, bf16[768,128]{1,0:T(8,128)(2,1)S(1)}, u32[]{:S(2)}, u32[]{:S(2)}) collective-permute-start(bf16[768,128]{1,0:T(8,128)(2,1)S(1)} %collective-permute-done.3.refs_0_), channel_id=1, source_target_pairs={{0,1},{1,2},{2,3},{3,0},{4,5},{5,6},{6,7},{7,4},{8,9},{9,10},{10,1... | collective-permute-start | bytes 589832 | tf_op jit(solution)/shard_map/ppermute | solution.py:327
  88.6 6.9 %collective-permute-start.9 = (bf16[768,128]{1,0:T(8,128)(2,1)S(1)}, bf16[768,128]{1,0:T(8,128)(2,1)S(1)}, u32[]{:S(2)}, u32[]{:S(2)}) collective-permute-start(bf16[768,128]{1,0:T(8,128)(2,1)S(1)} %collective-permute-done.6.refs_3_), channel_id=1, source_target_pairs={{0,3},{1,0},{2,1},{3,2},{4,7},{5,4},{6,5},{7,6},{8,11},{9,8},{10,9... | collective-permute-start | bytes 589832 | tf_op jit(solution)/shard_map/ppermute | solution.py:327
  91.8 9.2 %collective-permute-start.4 = (bf16[768,128]{1,0:T(8,128)(2,1)S(1)}, bf16[768,128]{1,0:T(8,128)(2,1)S(1)}, u32[]{:S(2)}, u32[]{:S(2)}) collective-permute-start(bf16[768,128]{1,0:T(8,128)(2,1)S(1)} %bitcast.46), channel_id=1, source_target_pairs={{0,1},{1,2},{2,3},{3,0},{4,5},{5,6},{6,7},{7,4},{8,9},{9,10},{10,1... | collective-permute-start | bytes 589832 | tf_op jit(solution)/shard_map/ppermute | solution.py:327
  91.8 9.2 %collective-permute-start.5 = (bf16[768,128]{1,0:T(8,128)(2,1)S(1)}, bf16[768,128]{1,0:T(8,128)(2,1)S(1)}, u32[]{:S(2)}, u32[]{:S(2)}) collective-permute-start(bf16[768,128]{1,0:T(8,128)(2,1)S(1)} %bitcast.44), channel_id=1, source_target_pairs={{0,3},{1,0},{2,1},{3,2},{4,7},{5,4},{6,5},{7,6},{8,11},{9,8},{10,9... | collective-permute-start | bytes 589832 | tf_op jit(solution)/shard_map/ppermute | solution.py:327
  97.4 9.8 %collective-permute-start.10 = (bf16[768,128]{1,0:T(8,128)(2,1)S(1)}, bf16[768,128]{1,0:T(8,128)(2,1)S(1)}, u32[]{:S(2)}, u32[]{:S(2)}) collective-permute-start(bf16[768,128]{1,0:T(8,128)(2,1)S(1)} %get-tuple-element.38), channel_id=1, source_target_pairs={{0,3},{1,0},{2,1},{3,2},{4,7},{5,4},{6,5},{7,6},{8,11},{9,8},{10,9... | collective-permute-start | bytes 589832 | tf_op jit(solution)/shard_map/ppermute | solution.py:327
  103.8 12.4 %collective-permute-start.7 = (bf16[768,128]{1,0:T(8,128)(2,1)S(1)}, bf16[768,128]{1,0:T(8,128)(2,1)S(1)}, u32[]{:S(2)}, u32[]{:S(2)}) collective-permute-start(bf16[768,128]{1,0:T(8,128)(2,1)S(1)} %get-tuple-element.36), channel_id=1, source_target_pairs={{0,1},{1,2},{2,3},{3,0},{4,5},{5,6},{6,7},{7,4},{8,9},{9,10},{10,1... | collective-permute-start | bytes 589832 | tf_op jit(solution)/shard_map/ppermute | solution.py:327
  104.0 12.3 %collective-permute-start.14 = (bf16[768,128]{1,0:T(8,128)(2,1)S(1)}, bf16[768,128]{1,0:T(8,128)(2,1)S(1)}, u32[]{:S(2)}, u32[]{:S(2)}) collective-permute-start(bf16[768,128]{1,0:T(8,128)(2,1)S(1)} %get-tuple-element.41), channel_id=1, source_target_pairs={{0,3},{1,0},{2,1},{3,2},{4,7},{5,4},{6,5},{7,6},{8,11},{9,8},{10,9... | collective-permute-start | bytes 589832 | tf_op jit(solution)/shard_map/ppermute | solution.py:327
  107.2 6.9 %collective-permute-start.12 = (bf16[768,128]{1,0:T(8,128)(2,1)S(1)}, bf16[768,128]{1,0:T(8,128)(2,1)S(1)}, u32[]{:S(2)}, u32[]{:S(2)}) collective-permute-start(bf16[768,128]{1,0:T(8,128)(2,1)S(1)} %get-tuple-element.40), channel_id=1, source_target_pairs={{0,1},{1,2},{2,3},{3,0},{4,5},{5,6},{6,7},{7,4},{8,9},{9,10},{10,1... | collective-permute-start | bytes 589832 | tf_op jit(solution)/shard_map/ppermute | solution.py:327
  107.3 9.0 %collective-permute-start.11 = (bf16[768,128]{1,0:T(8,128)(2,1)S(1)}, bf16[768,128]{1,0:T(8,128)(2,1)S(1)}, u32[]{:S(2)}, u32[]{:S(2)}) collective-permute-start(bf16[768,128]{1,0:T(8,128)(2,1)S(1)} %add_convert_fusion.1), channel_id=1, source_target_pairs={{0,3},{1,0},{2,1},{3,2},{4,7},{5,4},{6,5},{7,6},{8,11},{9,8},{10,9... | collective-permute-start | bytes 589832 | tf_op jit(solution)/shard_map/ppermute | solution.py:327
  114.1 7.0 %collective-permute-start.13 = (bf16[768,128]{1,0:T(8,128)(2,1)S(1)}, bf16[768,128]{1,0:T(8,128)(2,1)S(1)}, u32[]{:S(2)}, u32[]{:S(2)}) collective-permute-start(bf16[768,128]{1,0:T(8,128)(2,1)S(1)} %add_convert_fusion), channel_id=1, source_target_pairs={{0,1},{1,2},{2,3},{3,0},{4,5},{5,6},{6,7},{7,4},{8,9},{9,10},{10,1... | collective-permute-start | bytes 589832 | tf_op jit(solution)/shard_map/ppermute | solution.py:327
  114.3 44.1 %copy-start.5 = (f32[2048]{0:T(1024)S(1)}, f32[2048]{0:T(1024)}, u32[]{:S(2)}) copy-start(f32[2048]{0:T(1024)} %param.30) | copy-start | bytes 24580
  114.3 44.0 %copy-start.6 = (f32[2048]{0:T(1024)S(1)}, f32[2048]{0:T(1024)}, u32[]{:S(2)}) copy-start(f32[2048]{0:T(1024)} %param.31) | copy-start | bytes 24580
  114.3 44.0 %copy-start.8 = (f32[48,2]{0,1:T(2,128)S(1)}, f32[48,2]{0,1:T(2,128)}, u32[]{:S(2)}) copy-start(f32[48,2]{0,1:T(2,128)} %param.26) | copy-start | bytes 1156

commit v2 on v1

--- a/solution.py
+++ b/solution.py
@@ -210,12 +210,19 @@
         out_refs[b][...] = wide[b].astype(BF16)
 
 
-def total_body(kept_ref, left_1_ref, right_1_ref, left_2_ref, right_2_ref, out_ref):
-    half = left_1_ref.shape[0]
+def total_body(
+    kept_ref, left_1_ref, right_1_ref, left_2_ref, right_2_ref, core_ref, same_ref, other_ref
+):
+    chips, per_expert, _ = same_ref.shape
+    half = chips // 2
+    first_core = jnp.broadcast_to(core_ref[...], (half, per_expert, LANES)) == 0
     for part, left_ref, right_ref in ((0, left_1_ref, right_1_ref), (1, left_2_ref, right_2_ref)):
         rows = slice(part * half, (part + 1) * half)
         sides = left_ref[...].astype(F32) + right_ref[...].astype(F32)
-        out_ref[rows, :] = (kept_ref[rows, :].astype(F32) + sides).astype(BF16)
+        result = kept_ref[rows].astype(F32) + sides
+        zero, one = result[:, 0:per_expert, :], result[:, per_expert:, :]
+        same_ref[rows] = jnp.where(first_core, zero, one).astype(BF16)
+        other_ref[rows] = jnp.where(first_core, one, zero).astype(BF16)
 
 
 def combine_body(
@@ -311,17 +318,22 @@
         flops=10**9,
         scratch=[pltpu.VMEM((packed, LANES), F32)],
     )
-    other = lax.ppermute(other, "core", [(0, 1), (1, 0)])
     per_expert = capacity * tiles
-    (sent,) = call(
-        pair_body,
-        [shape((experts // 2, 2 * per_expert, LANES), BF16)],
-        same.reshape(-1, per_expert, LANES),
-        other.reshape(-1, per_expert, LANES),
-        core,
-        flops=10**6,
-    )
-    arrived = lax.all_to_all(sent.reshape(packed, LANES), "chip", 0, 0, tiled=True)
+    chips = experts // 2
+
+    def exchanged(same, other):
+        other = lax.ppermute(other, "core", [(0, 1), (1, 0)])
+        (sent,) = call(
+            pair_body,
+            [shape((chips, 2 * per_expert, LANES), BF16)],
+            same.reshape(chips, per_expert, LANES),
+            other.reshape(chips, per_expert, LANES),
+            core,
+            flops=10**6,
+        )
+        return lax.all_to_all(sent.reshape(packed, LANES), "chip", 0, 0, tiled=True)
+
+    arrived = exchanged(same, other)
 
     def turned(array, by):
         return lax.ppermute(array, "tp", [(i, (i + by) % members) for i in range(members)])
@@ -356,17 +368,16 @@
     for_right_2 = for_right_2.astype(F32) + turned(for_far_2, 1).astype(F32)
     from_right_1 = turned(for_left_1.astype(BF16), -1)
     from_left_2 = turned(for_right_2.astype(BF16), 1)
-    (summed,) = call(
+    sides = [from_left_1, from_right_1, from_left_2, from_right_2]
+    same, other = call(
         total_body,
-        [shape((packed, LANES), BF16)],
-        kept,
-        from_left_1,
-        from_right_1,
-        from_left_2,
-        from_right_2,
+        [shape((chips, per_expert, LANES), BF16)] * 2,
+        kept.reshape(chips, 2 * per_expert, LANES),
+        *[side.reshape(chips // 2, 2 * per_expert, LANES) for side in sides],
+        core,
         flops=10**7,
     )
-    back = lax.all_to_all(summed, SP, 0, 0, tiled=True)
+    back = exchanged(same, other)
     (mixed,) = call(
         functools.partial(combine_body, experts),
         [shape((own, width), BF16)],
@@ -408,6 +419,4 @@
         P(),
     )
 
-    return jax.shard_map(
-        per_device, mesh=mesh, in_specs=placed, out_specs=P(every, None), check_vma=False
-    )
+    return jax.shard_map(per_device, mesh=mesh, in_specs=placed, out_specs=P(every, None), check_vma=False)

time: 161 us -> 158 us (0.981)
  blocking collectives: 102 us -> 97.4 us
    all_to_all x2, blocking collectives: 84.7 us -> 80.5 us  [exchanged(): return lax.all_to_all(sent.reshape(packed, LANES), 'chip', 0, 0, tiled=True)]
    pallas_call x9 -> x10, Pallas kernels: 14 us -> 14.1 us  [call(): pl.pallas_call(body, out_shape=out_shapes, in_specs=specs or [VMEM] * len...]
  transfers between devices with their start and end apart: 15 -> 16, of which waited for: 6 -> 7; matrix products, arithmetic and copies ran while one was open for 0% -> 0% of each run, Pallas kernels for 4% -> 4%
where the time goes in v2:
time: 158 us
  blocking collectives  97.4 us (62%)
  starting transfers between devices  24.8 us (16%)
  waiting for transfers between devices  20.9 us (13%)
  Pallas kernels  14.1 us (9%)
    all_to_all x2, blocking collectives, exchanged(): return lax.all_to_all(sent.reshape(packed, LANES), 'chip', 0, 0, tiled=True)  80.5 us
    ppermute x12, starting transfers between devices, turned(): lax.ppermute(array, 'tp', [(i, (i + by) % members) for i in range(members)])  20.2 us
    all_to_all x1, blocking collectives, per_device(): lax.all_to_all(partial.reshape(members, own, width), 'tp', 0, 0, tiled=True)  16.9 us
    ppermute x12, waiting for transfers between devices, turned(): lax.ppermute(array, 'tp', [(i, (i + by) % members) for i in range(members)])  14.1 us
    pallas_call x10, Pallas kernels, call(): pl.pallas_call(body, out_shape=out_shapes, in_specs=specs or [VMEM] * len...  14.1 us
    ppermute x1, waiting for transfers between devices, per_device(): following = lax.ppermute(head, SP, [(i + 1, i) for i in range(blocks - 1)])  4.3 us
  transfers between devices with their start and end apart: 16, of which 7 were waited for; matrix products, arithmetic and copies ran while one was open for 0% of the time, Pallas kernels for 4%

profile of v2, /device:TPU:40, one launch (start us, length us, event | category | flops | bytes accessed | tf_op | source)
XLA Modules:
  0.0 157.7 jit_solution(6726935260285601160)
XLA Ops:
  0.0 1.4 shard_map.154
  1.5 1.8 %collective-permute-start = (bf16[144,128]{1,0:T(8,128)(2,1)S(1)}, bf16[144,128]{1,0:T(8,128)(2,1)S(1)}, u32[]{:S(2)}, u32[]{:S(2)}) collective-permute-start(bf16[144,128]{1,0:T(8,128)(2,1)S(1)} %get-tuple-element.31), channel_id=1, source_target_pairs={{0,4},{4,8},{8,12},{12,16},{16,20},{20,24},{24,28},{28,32},{32,36}... | collective-permute-start | bytes 110600 | tf_op jit(solution)/shard_map/ppermute | solution.py:292
  3.3 1.3 collective-permute-start.1
  4.6 4.3 %collective-permute-done.1.next_ref = bf16[144,128]{1,0:T(8,128)(2,1)S(1)} collective-permute-done((bf16[144,128]{1,0:T(8,128)(2,1)S(1)}, bf16[144,128]{1,0:T(8,128)(2,1)S(1)}, u32[]{:S(2)}, u32[]{:S(2)}) %collective-permute-start.1) | collective-permute-done | bytes 36896 | tf_op jit(solution)/shard_map/ppermute | solution.py:293
  8.9 2.9 %shard_map.155 = bf16[192,2048]{1,0:T(8,128)(2,1)S(1)} custom-call(f32[1,4]{1,0:T(1,128)S(1)} %get-tuple-element.26.sink_ref, bf16[192,256]{1,0:T(8,128)(2,1)S(1)} %get-tuple-element.27.query_ref, bf16[64,192]{1,0:T(8,128)(2,1)S(1)} %get-tuple-element.28.keys_ref, bf16[64,192]{1,0:T(8,128)(2,1)S(1)} %get-tuple-element.29.values_ref, ...), custom_call_target="tpu_custom_call" | custom-call | flops 1000000000 | bytes 2056976 | tf_op jit(solution)/shard_map/pallas_call | solution.py:42
  11.8 16.9 %all_to_all.21.parts_ref = bf16[4,48,2048]{2,1,0:T(8,128)(2,1)S(1)} all-to-all(bf16[4,48,2048]{2,1,0:T(8,128)(2,1)S(1)} %bitcast.36), channel_id=1, replica_groups=mesh['grp'=2,'chip'=16,'core'=2,'tp'=4] {'tp'}, dimensions={0} | all-to-all | bytes 1572864 | tf_op jit(solution)/shard_map/all_to_all | solution.py:308
  28.8 0.8 shard_map.156
  29.5 1.4 collective-permute-start.2
  30.9 1.1 collective-permute-done.2
  32.0 0.1 shard_map.157
  32.1 47.7 %all_to_all.22 = bf16[16,96,128]{2,1,0:T(8,128)(2,1)S(1)} all-to-all(bf16[16,96,128]{2,1,0:T(8,128)(2,1)S(1)} %shard_map.157), channel_id=1, replica_groups=mesh['grp'=2,'chip'=16,'core'=2,'tp'=4] {'chip'}, dimensions={0} | all-to-all | bytes 786432 | tf_op jit(solution)/shard_map/all_to_all | solution.py:334
  79.8 0.7 collective-permute-start.3
  80.5 2.7 %collective-permute-start.6 = (bf16[768,128]{1,0:T(8,128)(2,1)S(1)}, bf16[768,128]{1,0:T(8,128)(2,1)S(1)}, u32[]{:S(2)}, u32[]{:S(2)}) collective-permute-start(bf16[768,128]{1,0:T(8,128)(2,1)S(1)} %bitcast.53), channel_id=1, source_target_pairs={{0,3},{1,0},{2,1},{3,2},{4,7},{5,4},{6,5},{7,6},{8,11},{9,8},{10,9... | collective-permute-start | bytes 589832 | tf_op jit(solution)/shard_map/ppermute | solution.py:339
  83.1 5.4 %collective-permute-done.3.refs_0_ = bf16[768,128]{1,0:T(8,128)(2,1)S(1)} collective-permute-done((bf16[768,128]{1,0:T(8,128)(2,1)S(1)}, bf16[768,128]{1,0:T(8,128)(2,1)S(1)}, u32[]{:S(2)}, u32[]{:S(2)}) %collective-permute-start.3) | collective-permute-done | bytes 196640 | tf_op jit(solution)/shard_map/ppermute | solution.py:339
  88.6 3.2 %collective-permute-start.9 = (bf16[768,128]{1,0:T(8,128)(2,1)S(1)}, bf16[768,128]{1,0:T(8,128)(2,1)S(1)}, u32[]{:S(2)}, u32[]{:S(2)}) collective-permute-start(bf16[768,128]{1,0:T(8,128)(2,1)S(1)} %collective-permute-done.6.refs_3_), channel_id=1, source_target_pairs={{0,3},{1,0},{2,1},{3,2},{4,7},{5,4},{6,5},{7,6},{8,11},{9,8},{10,9... | collective-permute-start | bytes 589832 | tf_op jit(solution)/shard_map/ppermute | solution.py:339
  91.8 3.2 %collective-permute-start.5 = (bf16[768,128]{1,0:T(8,128)(2,1)S(1)}, bf16[768,128]{1,0:T(8,128)(2,1)S(1)}, u32[]{:S(2)}, u32[]{:S(2)}) collective-permute-start(bf16[768,128]{1,0:T(8,128)(2,1)S(1)} %bitcast.52), channel_id=1, source_target_pairs={{0,3},{1,0},{2,1},{3,2},{4,7},{5,4},{6,5},{7,6},{8,11},{9,8},{10,9... | collective-permute-start | bytes 589832 | tf_op jit(solution)/shard_map/ppermute | solution.py:339
  95.0 0.4 collective-permute-done.8.refs_0_
  95.5 2.0 %shard_map.160 = (bf16[768,128]{1,0:T(8,128)(2,1)S(1)}, bf16[768,128]{1,0:T(8,128)(2,1)S(1)}) custom-call(bf16[768,128]{1,0:T(8,128)(2,1)S(1)} %collective-permute-done.8.refs_0_, bf16[768,128]{1,0:T(8,128)(2,1)S(1)} %collective-permute-done.9.refs_1_, bf16[2048,768]{1,0:T(8,128)(2,1)S(1)} %bitcast.25, bf16[2048,768]{1,0:T(8,128)(2,1)S(1)} %bitcast.28, ...), custom_call_target="tpu_custom_call" | custom-call | flops 1536000000 | bytes 10223616 | tf_op jit(solution)/shard_map/pallas_call | solution.py:42
  97.4 3.5 %collective-permute-start.10 = (bf16[768,128]{1,0:T(8,128)(2,1)S(1)}, bf16[768,128]{1,0:T(8,128)(2,1)S(1)}, u32[]{:S(2)}, u32[]{:S(2)}) collective-permute-start(bf16[768,128]{1,0:T(8,128)(2,1)S(1)} %get-tuple-element.40), channel_id=1, source_target_pairs={{0,3},{1,0},{2,1},{3,2},{4,7},{5,4},{6,5},{7,6},{8,11},{9,8},{10,9... | collective-permute-start | bytes 589832 | tf_op jit(solution)/shard_map/ppermute | solution.py:339
  101.0 2.9 %shard_map.159 = (bf16[768,128]{1,0:T(8,128)(2,1)S(1)}, bf16[768,128]{1,0:T(8,128)(2,1)S(1)}, bf16[768,128]{1,0:T(8,128)(2,1)S(1)}, bf16[768,128]{1,0:T(8,128)(2,1)S(1)}) custom-call(bf16[768,128]{1,0:T(8,128)(2,1)S(1)} %collective-permute-done.3.refs_0_, bf16[768,128]{1,0:T(8,128)(2,1)S(1)} %collective-permute-done.4.refs_1_, ...), custom_call_target="tpu_custom_call" | custom-call | flops 3072000000 | bytes 11010048 | tf_op jit(solution)/shard_map/pallas_call | solution.py:42
  103.8 0.1 collective-permute-start.7
  104.0 3.2 %collective-permute-start.14 = (bf16[768,128]{1,0:T(8,128)(2,1)S(1)}, bf16[768,128]{1,0:T(8,128)(2,1)S(1)}, u32[]{:S(2)}, u32[]{:S(2)}) collective-permute-start(bf16[768,128]{1,0:T(8,128)(2,1)S(1)} %get-tuple-element.43), channel_id=1, source_target_pairs={{0,3},{1,0},{2,1},{3,2},{4,7},{5,4},{6,5},{7,6},{8,11},{9,8},{10,9... | collective-permute-start | bytes 589832 | tf_op jit(solution)/shard_map/ppermute | solution.py:339
  107.3 3.3 %collective-permute-start.11 = (bf16[768,128]{1,0:T(8,128)(2,1)S(1)}, bf16[768,128]{1,0:T(8,128)(2,1)S(1)}, u32[]{:S(2)}, u32[]{:S(2)}) collective-permute-start(bf16[768,128]{1,0:T(8,128)(2,1)S(1)} %add_convert_fusion.1), channel_id=1, source_target_pairs={{0,3},{1,0},{2,1},{3,2},{4,7},{5,4},{6,5},{7,6},{8,11},{9,8},{10,9... | collective-permute-start | bytes 589832 | tf_op jit(solution)/shard_map/ppermute | solution.py:339
  110.6 3.5 %collective-permute-done.12 = bf16[768,128]{1,0:T(8,128)(2,1)S(1)} collective-permute-done((bf16[768,128]{1,0:T(8,128)(2,1)S(1)}, bf16[768,128]{1,0:T(8,128)(2,1)S(1)}, u32[]{:S(2)}, u32[]{:S(2)}) %collective-permute-start.12) | collective-permute-done | bytes 196640 | tf_op jit(solution)/shard_map/ppermute | solution.py:339
  114.1 0.1 collective-permute-start.13
  114.3 2.0 %shard_map.158 = bf16[1536,128]{1,0:T(8,128)(2,1)S(1)} custom-call(bf16[1536,128]{1,0:T(8,128)(2,1)S(1)} %bitcast.34, bf16[2048,768]{1,0:T(8,128)(2,1)S(1)} %bitcast.27, bf16[2048,768]{1,0:T(8,128)(2,1)S(1)} %bitcast.30, bf16[768,2048]{1,0:T(8,128)(2,1)S(1)} %bitcast.33), custom_call_target="tpu_custom_call" | custom-call | flops 1536000000 | bytes 10223616 | tf_op jit(solution)/shard_map/pallas_call | solution.py:42
  116.3 4.8 %collective-permute-done.13 = bf16[768,128]{1,0:T(8,128)(2,1)S(1)} collective-permute-done((bf16[768,128]{1,0:T(8,128)(2,1)S(1)}, bf16[768,128]{1,0:T(8,128)(2,1)S(1)}, u32[]{:S(2)}, u32[]{:S(2)}) %collective-permute-start.13) | collective-permute-done | bytes 196640 | tf_op jit(solution)/shard_map/ppermute | solution.py:339
  121.1 0.2 shard_map.161
  121.3 0.1 collective-permute-start.15
  121.5 1.4 collective-permute-done.15.other_ref
  123.0 32.8 %all_to_all.23 = bf16[16,96,128]{2,1,0:T(8,128)(2,1)S(1)} all-to-all(bf16[16,96,128]{2,1,0:T(8,128)(2,1)S(1)} %shard_map.162), channel_id=1, replica_groups=mesh['grp'=2,'chip'=16,'core'=2,'tp'=4] {'chip'}, dimensions={0} | all-to-all | bytes 786432 | tf_op jit(solution)/shard_map/all_to_all | solution.py:334
  155.8 1.8 %shard_map.163 = bf16[48,2048]{1,0:T(8,128)(2,1)} custom-call(bf16[1536,128]{1,0:T(8,128)(2,1)S(1)} %bitcast.37, bf16[48,2048]{1,0:T(8,128)(2,1)S(1)} %get-tuple-element.46.normed_ref, s32[2,48]{1,0:T(2,128)S(1)} %bitcast.49, f32[2,48]{1,0:T(2,128)S(1)} %bitcast.50, f32[1,2048]{1,0:T(1,128)S(1)} %bitcast.46, f32[1,2048]{1,0:T(1,128)S(1)} %bitcast.47), custom_call_target="tpu_custom_call" | custom-call | flops 1000000000 | bytes 803584 | tf_op jit(solution)/shard_map/pallas_call | solution.py:42
  (35 shorter events, 0.3 us)
Async XLA Ops:
  0.0 28.8 %copy-start.3 = (f32[2048]{0:T(1024)S(1)}, f32[2048]{0:T(1024)}, u32[]{:S(2)}) copy-start(f32[2048]{0:T(1024)} %param.23) | copy-start | bytes 24580
  0.0 28.8 %copy-start.4 = (f32[2048]{0:T(1024)S(1)}, f32[2048]{0:T(1024)}, u32[]{:S(2)}) copy-start(f32[2048]{0:T(1024)} %param.24) | copy-start | bytes 24580
  0.0 28.8 %copy-start.7 = (s32[48,2]{0,1:T(2,128)S(1)}, s32[48,2]{0,1:T(2,128)}, u32[]{:S(2)}) copy-start(s32[48,2]{0,1:T(2,128)} %param.25) | copy-start | bytes 1156
  1.5 3.2 %collective-permute-start = (bf16[144,128]{1,0:T(8,128)(2,1)S(1)}, bf16[144,128]{1,0:T(8,128)(2,1)S(1)}, u32[]{:S(2)}, u32[]{:S(2)}) collective-permute-start(bf16[144,128]{1,0:T(8,128)(2,1)S(1)} %get-tuple-element.31), channel_id=1, source_target_pairs={{0,4},{4,8},{8,12},{12,16},{16,20},{20,24},{24,28},{28,32},{32,36}... | collective-permute-start | bytes 110600 | tf_op jit(solution)/shard_map/ppermute | solution.py:292
  3.3 5.6 %collective-permute-start.1 = (bf16[144,128]{1,0:T(8,128)(2,1)S(1)}, bf16[144,128]{1,0:T(8,128)(2,1)S(1)}, u32[]{:S(2)}, u32[]{:S(2)}) collective-permute-start(bf16[144,128]{1,0:T(8,128)(2,1)S(1)} %get-tuple-element.32), channel_id=1, source_target_pairs={{4,0},{8,4},{12,8},{16,12},{20,16},{24,20},{28,24},{32,28},{36,32}... | collective-permute-start | bytes 110600 | tf_op jit(solution)/shard_map/ppermute | solution.py:293
  8.9 86.5 %copy-start.2 = (bf16[1,768,2048]{2,1,0:T(8,128)(2,1)S(1)}, bf16[1,768,2048]{2,1,0:T(8,128)(2,1)}, u32[]{:S(2)}) copy-start(bf16[1,768,2048]{2,1,0:T(8,128)(2,1)} %param.29) | copy-start | bytes 9437188
  11.8 83.6 %copy-start.1 = (bf16[1,2048,768]{2,1,0:T(8,128)(2,1)S(1)}, bf16[1,2048,768]{2,1,0:T(8,128)(2,1)}, u32[]{:S(2)}) copy-start(bf16[1,2048,768]{2,1,0:T(8,128)(2,1)} %param.28) | copy-start | bytes 9437188
  28.8 66.7 %copy-start = (bf16[1,2048,768]{2,1,0:T(8,128)(2,1)S(1)}, bf16[1,2048,768]{2,1,0:T(8,128)(2,1)}, u32[]{:S(2)}) copy-start(bf16[1,2048,768]{2,1,0:T(8,128)(2,1)} %param.27) | copy-start | bytes 9437188
  29.5 2.4 %collective-permute-start.2 = (bf16[768,128]{1,0:T(8,128)(2,1)S(1)}, bf16[768,128]{1,0:T(8,128)(2,1)S(1)}, u32[]{:S(2)}, u32[]{:S(2)}) collective-permute-start(bf16[768,128]{1,0:T(8,128)(2,1)S(1)} %get-tuple-element.37), channel_id=1, source_target_pairs={{0,4},{4,0},{1,5},{5,1},{2,6},{6,2},{3,7},{7,3},{8,12},{12,8},{9,1... | collective-permute-start | bytes 589832 | tf_op jit(solution)/shard_map/ppermute | solution.py:325
  79.8 8.8 %collective-permute-start.3 = (bf16[768,128]{1,0:T(8,128)(2,1)S(1)}, bf16[768,128]{1,0:T(8,128)(2,1)S(1)}, u32[]{:S(2)}, u32[]{:S(2)}) collective-permute-start(bf16[768,128]{1,0:T(8,128)(2,1)S(1)} %bitcast.51), channel_id=1, source_target_pairs={{0,1},{1,2},{2,3},{3,0},{4,5},{5,6},{6,7},{7,4},{8,9},{9,10},{10,1... | collective-permute-start | bytes 589832 | tf_op jit(solution)/shard_map/ppermute | solution.py:339
  80.5 8.1 %collective-permute-start.6 = (bf16[768,128]{1,0:T(8,128)(2,1)S(1)}, bf16[768,128]{1,0:T(8,128)(2,1)S(1)}, u32[]{:S(2)}, u32[]{:S(2)}) collective-permute-start(bf16[768,128]{1,0:T(8,128)(2,1)S(1)} %bitcast.53), channel_id=1, source_target_pairs={{0,3},{1,0},{2,1},{3,2},{4,7},{5,4},{6,5},{7,6},{8,11},{9,8},{10,9... | collective-permute-start | bytes 589832 | tf_op jit(solution)/shard_map/ppermute | solution.py:339
  88.6 6.9 %collective-permute-start.8 = (bf16[768,128]{1,0:T(8,128)(2,1)S(1)}, bf16[768,128]{1,0:T(8,128)(2,1)S(1)}, u32[]{:S(2)}, u32[]{:S(2)}) collective-permute-start(bf16[768,128]{1,0:T(8,128)(2,1)S(1)} %collective-permute-done.3.refs_0_), channel_id=1, source_target_pairs={{0,1},{1,2},{2,3},{3,0},{4,5},{5,6},{6,7},{7,4},{8,9},{9,10},{10,1... | collective-permute-start | bytes 589832 | tf_op jit(solution)/shard_map/ppermute | solution.py:339
  88.6 6.9 %collective-permute-start.9 = (bf16[768,128]{1,0:T(8,128)(2,1)S(1)}, bf16[768,128]{1,0:T(8,128)(2,1)S(1)}, u32[]{:S(2)}, u32[]{:S(2)}) collective-permute-start(bf16[768,128]{1,0:T(8,128)(2,1)S(1)} %collective-permute-done.6.refs_3_), channel_id=1, source_target_pairs={{0,3},{1,0},{2,1},{3,2},{4,7},{5,4},{6,5},{7,6},{8,11},{9,8},{10,9... | collective-permute-start | bytes 589832 | tf_op jit(solution)/shard_map/ppermute | solution.py:339
  91.8 9.2 %collective-permute-start.4 = (bf16[768,128]{1,0:T(8,128)(2,1)S(1)}, bf16[768,128]{1,0:T(8,128)(2,1)S(1)}, u32[]{:S(2)}, u32[]{:S(2)}) collective-permute-start(bf16[768,128]{1,0:T(8,128)(2,1)S(1)} %bitcast.54), channel_id=1, source_target_pairs={{0,1},{1,2},{2,3},{3,0},{4,5},{5,6},{6,7},{7,4},{8,9},{9,10},{10,1... | collective-permute-start | bytes 589832 | tf_op jit(solution)/shard_map/ppermute | solution.py:339
  91.8 9.2 %collective-permute-start.5 = (bf16[768,128]{1,0:T(8,128)(2,1)S(1)}, bf16[768,128]{1,0:T(8,128)(2,1)S(1)}, u32[]{:S(2)}, u32[]{:S(2)}) collective-permute-start(bf16[768,128]{1,0:T(8,128)(2,1)S(1)} %bitcast.52), channel_id=1, source_target_pairs={{0,3},{1,0},{2,1},{3,2},{4,7},{5,4},{6,5},{7,6},{8,11},{9,8},{10,9... | collective-permute-start | bytes 589832 | tf_op jit(solution)/shard_map/ppermute | solution.py:339
  97.4 9.8 %collective-permute-start.10 = (bf16[768,128]{1,0:T(8,128)(2,1)S(1)}, bf16[768,128]{1,0:T(8,128)(2,1)S(1)}, u32[]{:S(2)}, u32[]{:S(2)}) collective-permute-start(bf16[768,128]{1,0:T(8,128)(2,1)S(1)} %get-tuple-element.40), channel_id=1, source_target_pairs={{0,3},{1,0},{2,1},{3,2},{4,7},{5,4},{6,5},{7,6},{8,11},{9,8},{10,9... | collective-permute-start | bytes 589832 | tf_op jit(solution)/shard_map/ppermute | solution.py:339
  103.8 12.4 %collective-permute-start.7 = (bf16[768,128]{1,0:T(8,128)(2,1)S(1)}, bf16[768,128]{1,0:T(8,128)(2,1)S(1)}, u32[]{:S(2)}, u32[]{:S(2)}) collective-permute-start(bf16[768,128]{1,0:T(8,128)(2,1)S(1)} %get-tuple-element.38), channel_id=1, source_target_pairs={{0,1},{1,2},{2,3},{3,0},{4,5},{5,6},{6,7},{7,4},{8,9},{9,10},{10,1... | collective-permute-start | bytes 589832 | tf_op jit(solution)/shard_map/ppermute | solution.py:339
  104.0 12.3 %collective-permute-start.14 = (bf16[768,128]{1,0:T(8,128)(2,1)S(1)}, bf16[768,128]{1,0:T(8,128)(2,1)S(1)}, u32[]{:S(2)}, u32[]{:S(2)}) collective-permute-start(bf16[768,128]{1,0:T(8,128)(2,1)S(1)} %get-tuple-element.43), channel_id=1, source_target_pairs={{0,3},{1,0},{2,1},{3,2},{4,7},{5,4},{6,5},{7,6},{8,11},{9,8},{10,9... | collective-permute-start | bytes 589832 | tf_op jit(solution)/shard_map/ppermute | solution.py:339
  107.2 6.9 %collective-permute-start.12 = (bf16[768,128]{1,0:T(8,128)(2,1)S(1)}, bf16[768,128]{1,0:T(8,128)(2,1)S(1)}, u32[]{:S(2)}, u32[]{:S(2)}) collective-permute-start(bf16[768,128]{1,0:T(8,128)(2,1)S(1)} %get-tuple-element.42), channel_id=1, source_target_pairs={{0,1},{1,2},{2,3},{3,0},{4,5},{5,6},{6,7},{7,4},{8,9},{9,10},{10,1... | collective-permute-start | bytes 589832 | tf_op jit(solution)/shard_map/ppermute | solution.py:339
  107.3 9.0 %collective-permute-start.11 = (bf16[768,128]{1,0:T(8,128)(2,1)S(1)}, bf16[768,128]{1,0:T(8,128)(2,1)S(1)}, u32[]{:S(2)}, u32[]{:S(2)}) collective-permute-start(bf16[768,128]{1,0:T(8,128)(2,1)S(1)} %add_convert_fusion.1), channel_id=1, source_target_pairs={{0,3},{1,0},{2,1},{3,2},{4,7},{5,4},{6,5},{7,6},{8,11},{9,8},{10,9... | collective-permute-start | bytes 589832 | tf_op jit(solution)/shard_map/ppermute | solution.py:339
  114.1 7.0 %collective-permute-start.13 = (bf16[768,128]{1,0:T(8,128)(2,1)S(1)}, bf16[768,128]{1,0:T(8,128)(2,1)S(1)}, u32[]{:S(2)}, u32[]{:S(2)}) collective-permute-start(bf16[768,128]{1,0:T(8,128)(2,1)S(1)} %add_convert_fusion), channel_id=1, source_target_pairs={{0,1},{1,2},{2,3},{3,0},{4,5},{5,6},{6,7},{7,4},{8,9},{9,10},{10,1... | collective-permute-start | bytes 589832 | tf_op jit(solution)/shard_map/ppermute | solution.py:339
  114.3 41.5 %copy-start.5 = (f32[2048]{0:T(1024)S(1)}, f32[2048]{0:T(1024)}, u32[]{:S(2)}) copy-start(f32[2048]{0:T(1024)} %param.30) | copy-start | bytes 24580
  114.3 41.5 %copy-start.6 = (f32[2048]{0:T(1024)S(1)}, f32[2048]{0:T(1024)}, u32[]{:S(2)}) copy-start(f32[2048]{0:T(1024)} %param.31) | copy-start | bytes 24580
  114.3 41.5 %copy-start.8 = (f32[48,2]{0,1:T(2,128)S(1)}, f32[48,2]{0,1:T(2,128)}, u32[]{:S(2)}) copy-start(f32[48,2]{0,1:T(2,128)} %param.26) | copy-start | bytes 1156
  121.3 1.6 collective-permute-start.15

commit v3 on v2

--- a/solution.py
+++ b/solution.py
@@ -48,6 +48,10 @@
         compiler_params=pltpu.CompilerParams(vmem_limit_bytes=vmem or 12 * 2**20),
         cost_estimate=pl.CostEstimate(flops=flops, bytes_accessed=size, transcendentals=0),
     )(*args)
+
+
+def in_hbm(array):
+    return pltpu.with_memory_space_constraint(array, pltpu.HBM)
 
 
 def shape(dims, dtype):
@@ -81,8 +85,25 @@
 
 
 def attention_body(
-    sink_ref, query_ref, keys_ref, values_ref, docs_ref, prev_ref, next_ref, proj_ref, out_ref, att_ref
+    sink_ref,
+    query_ref,
+    keys_ref,
+    values_ref,
+    docs_ref,
+    prev_ref,
+    next_ref,
+    proj_hbm,
+    resid_hbm,
+    out_ref,
+    resid_ref,
+    att_ref,
+    proj_ref,
+    sems,
 ):
+    proj_copy = pltpu.make_async_copy(proj_hbm, proj_ref, sems.at[0])
+    resid_copy = pltpu.make_async_copy(resid_hbm, resid_ref, sems.at[1])
+    proj_copy.start()
+    resid_copy.start()
     tokens = query_ref.shape[0]
     heads = query_ref.shape[1] // HEAD_DIM
     own_docs = docs_ref[...].astype(F32) + 1.0
@@ -100,27 +121,26 @@
         width = key.shape[1]
         place = first + lax.broadcasted_iota(jnp.int32, (1, width), 1)
         allowed = (jnp.abs(row - place) <= WINDOW) & (query_docs == docs)
-        blocks.append((key, value, allowed))
+        blocks.append((key, value, jnp.where(allowed, 0.0, MASKED)))
     for h in range(heads):
         cols = slice(h * HEAD_DIM, (h + 1) * HEAD_DIM)
         query = query_ref[:, cols]
         sink = sink_ref[:, h : h + 1]
         scores = [
-            jnp.where(allowed, mm(query, key) * HEAD_DIM ** (-0.5), MASKED)
-            for key, _, allowed in blocks
+            mm(query, key) * HEAD_DIM ** (-0.5) + hidden for key, _, hidden in blocks
         ]
         top = functools.reduce(jnp.maximum, [jnp.max(s, -1, keepdims=True) for s in scores])
         top = jnp.maximum(top, sink)
-        raised = [
-            jnp.where(allowed, jnp.exp(s - top), 0.0) for s, (_, _, allowed) in zip(scores, blocks)
-        ]
+        raised = [jnp.exp(s - top) for s in scores]
         total = jnp.exp(sink - top) + sum(jnp.sum(r, -1, keepdims=True) for r in raised)
         scale = 1.0 / total
         result = sum(
             mm_nt((r * scale).astype(BF16), value) for r, (_, value, _) in zip(raised, blocks)
         )
         att_ref[:, cols] = result.astype(BF16)
+    proj_copy.wait()
     out_ref[...] = mm(att_ref[...], proj_ref[...]).astype(BF16)
+    resid_copy.wait()
 
 
 def routing_rows(ids, expert, weights=None):
@@ -234,19 +254,20 @@
     wide_ref[...] = back_ref[...].astype(F32)
     expert = lax.broadcasted_iota(jnp.int32, (experts, tokens), 0)
     weighted, rank = routing_rows(ids_ref[...], expert, weights_ref[...])
-    moe_sum = 0.0
+    picks = []
     for j in range(capacity):
-        pick = jnp.where(jnp.abs(rank - j) < 0.5, weighted, 0.0)
+        picks.append(jnp.where(jnp.abs(rank - j) < 0.5, weighted, 0.0))
         for c in range(tiles):
-            rows_ref[:, c * LANES : (c + 1) * LANES] = wide_ref[
+            rows_ref[j * experts : (j + 1) * experts, c * LANES : (c + 1) * LANES] = wide_ref[
                 pl.ds(j * tiles + c, experts, stride=capacity * tiles), :
             ].astype(BF16)
-        high = pick.astype(BF16)
-        low = pick - high.astype(F32)
-        middle = low.astype(BF16)
-        last = (low - middle.astype(F32)).astype(BF16)
-        rows = rows_ref[...]
-        moe_sum = moe_sum + (mm_tn(high, rows) + (mm_tn(middle, rows) + mm_tn(last, rows)))
+    pick = jnp.concatenate(picks, axis=0)
+    high = pick.astype(BF16)
+    low = pick - high.astype(F32)
+    middle = low.astype(BF16)
+    last = (low - middle.astype(F32)).astype(BF16)
+    rows = rows_ref[...]
+    moe_sum = mm_tn(high, rows) + (mm_tn(middle, rows) + mm_tn(last, rows))
     pre_final = RESIDUAL_SCALE * normed_ref[...].astype(F32) + moe_sum
     out_ref[...] = layer_norm(pre_final, gain_ref[...], bias_ref[...]).astype(BF16)
 
@@ -277,23 +298,23 @@
     tiles = width // LANES
     packed = experts * capacity * tiles
 
-    small = (keys.T, values.T, doc_ids.reshape(1, tokens), queries, out_proj, resid, sink_logits.reshape(1, -1))
+    small = (keys.T, values.T, doc_ids.reshape(1, tokens), queries, sink_logits.reshape(1, -1))
     pack = shape((2 * HEAD_DIM + 16, WINDOW), BF16)
     core = jnp.full((1, LANES), lax.axis_index("core"), jnp.int32)
-    keys_t, values_t, docs, queries, out_proj, resid, sinks, head, tail, core = call(
+    keys_t, values_t, docs, queries, sinks, head, tail, core = call(
         functools.partial(first_body, len(small)),
         [shape(a.shape, a.dtype) for a in small] + [pack, pack, shape(core.shape, core.dtype)],
         core,
-        *[pltpu.with_memory_space_constraint(a, pltpu.HBM) for a in small],
+        *[in_hbm(a) for a in small],
         flops=10**5,
         specs=[VMEM] + [HBM] * len(small),
         scratch=[pltpu.SemaphoreType.DMA((len(small),))],
     )
     previous = lax.ppermute(tail, SP, [(i, i + 1) for i in range(blocks - 1)])
     following = lax.ppermute(head, SP, [(i + 1, i) for i in range(blocks - 1)])
-    (partial,) = call(
+    partial, resid = call(
         attention_body,
-        [shape((tokens, width), BF16)],
+        [shape((tokens, width), BF16), shape(resid.shape, BF16)],
         sinks,
         queries,
         keys_t,
@@ -301,9 +322,15 @@
         docs,
         previous,
         following,
-        out_proj,
+        in_hbm(out_proj),
+        in_hbm(resid),
         flops=10**9,
-        scratch=[pltpu.VMEM(queries.shape, BF16)],
+        specs=[VMEM] * 7 + [HBM] * 2,
+        scratch=[
+            pltpu.VMEM(queries.shape, BF16),
+            pltpu.VMEM(out_proj.shape, BF16),
+            pltpu.SemaphoreType.DMA((2,)),
+        ],
     )
     parts = lax.all_to_all(partial.reshape(members, own, width), "tp", 0, 0, tiled=True)
     normed, same, other = call(
@@ -388,7 +415,7 @@
         norm2_gain.reshape(1, -1),
         norm2_bias.reshape(1, -1),
         flops=10**9,
-        scratch=[pltpu.VMEM((packed, LANES), F32), pltpu.VMEM((experts, width), BF16)],
+        scratch=[pltpu.VMEM((packed, LANES), F32), pltpu.VMEM((capacity * experts, width), BF16)],
     )
     return mixed
 
@@ -419,4 +446,6 @@
         P(),
     )
 
-    return jax.shard_map(per_device, mesh=mesh, in_specs=placed, out_specs=P(every, None), check_vma=False)
+    return jax.shard_map(
+        per_device, mesh=mesh, in_specs=placed, out_specs=P(every, None), check_vma=False
+    )

time: 158 us -> 158 us (level)
  no operation moved by 1% of the time
where the time goes in v3:
time: 158 us
  blocking collectives  97.5 us (62%)
  starting transfers between devices  24.8 us (16%)
  waiting for transfers between devices  20.9 us (13%)
  Pallas kernels  14.5 us (9%)
    all_to_all x2, blocking collectives, exchanged(): return lax.all_to_all(sent.reshape(packed, LANES), 'chip', 0, 0, tiled=True)  80.5 us
    ppermute x12, starting transfers between devices, turned(): lax.ppermute(array, 'tp', [(i, (i + by) % members) for i in range(members)])  20.2 us
    all_to_all x1, blocking collectives, per_device(): lax.all_to_all(partial.reshape(members, own, width), 'tp', 0, 0, tiled=True)  16.9 us
    pallas_call x10, Pallas kernels, call(): pl.pallas_call(body, out_shape=out_shapes, in_specs=specs or [VMEM] * len...  14.5 us
    ppermute x12, waiting for transfers between devices, turned(): lax.ppermute(array, 'tp', [(i, (i + by) % members) for i in range(members)])  14.1 us
    ppermute x1, waiting for transfers between devices, per_device(): following = lax.ppermute(head, SP, [(i + 1, i) for i in range(blocks - 1)])  4.3 us
  transfers between devices with their start and end apart: 16, of which 7 were waited for; matrix products, arithmetic and copies ran while one was open for 0% of the time, Pallas kernels for 4%

profile of v3, /device:TPU:40, one launch (start us, length us, event | category | flops | bytes accessed | tf_op | source)
XLA Modules:
  0.0 158.1 jit_solution(8451430300399315362)
XLA Ops:
  0.0 1.0 shard_map.154
  1.0 1.8 %collective-permute-start = (bf16[144,128]{1,0:T(8,128)(2,1)S(1)}, bf16[144,128]{1,0:T(8,128)(2,1)S(1)}, u32[]{:S(2)}, u32[]{:S(2)}) collective-permute-start(bf16[144,128]{1,0:T(8,128)(2,1)S(1)} %get-tuple-element.31), channel_id=1, source_target_pairs={{0,4},{4,8},{8,12},{12,16},{16,20},{20,24},{24,28},{28,32},{32,36}... | collective-permute-start | bytes 110600 | tf_op jit(solution)/shard_map/ppermute | solution.py:313
  2.9 1.3 collective-permute-start.1
  4.2 4.3 %collective-permute-done.1.next_ref = bf16[144,128]{1,0:T(8,128)(2,1)S(1)} collective-permute-done((bf16[144,128]{1,0:T(8,128)(2,1)S(1)}, bf16[144,128]{1,0:T(8,128)(2,1)S(1)}, u32[]{:S(2)}, u32[]{:S(2)}) %collective-permute-start.1) | collective-permute-done | bytes 36896 | tf_op jit(solution)/shard_map/ppermute | solution.py:314
  8.5 3.9 %shard_map.155 = (bf16[192,2048]{1,0:T(8,128)(2,1)S(1)}, bf16[48,2048]{1,0:T(8,128)(2,1)S(1)}) custom-call(f32[1,4]{1,0:T(1,128)S(1)} %get-tuple-element.26.sink_ref, bf16[192,256]{1,0:T(8,128)(2,1)S(1)} %get-tuple-element.27.query_ref, bf16[64,192]{1,0:T(8,128)(2,1)S(1)} %get-tuple-element.28.keys_ref, bf16[64,192]{1,0:T(8,128)(2,1)S(1)} %get-tuple-element.29.values_ref, ...), custom_call_target="tpu_custom_call" | custom-call | flops 1000000000 | bytes 2450192 | tf_op jit(solution)/shard_map/pallas_call | solution.py:42
  12.4 16.9 %all_to_all.21.parts_ref = bf16[4,48,2048]{2,1,0:T(8,128)(2,1)S(1)} all-to-all(bf16[4,48,2048]{2,1,0:T(8,128)(2,1)S(1)} %bitcast.36), channel_id=1, replica_groups=mesh['grp'=2,'chip'=16,'core'=2,'tp'=4] {'tp'}, dimensions={0} | all-to-all | bytes 1572864 | tf_op jit(solution)/shard_map/all_to_all | solution.py:335
  29.4 0.8 shard_map.156
  30.1 1.4 collective-permute-start.2
  31.5 1.1 collective-permute-done.2
  32.6 0.1 shard_map.157
  32.7 47.7 %all_to_all.22 = bf16[16,96,128]{2,1,0:T(8,128)(2,1)S(1)} all-to-all(bf16[16,96,128]{2,1,0:T(8,128)(2,1)S(1)} %shard_map.157), channel_id=1, replica_groups=mesh['grp'=2,'chip'=16,'core'=2,'tp'=4] {'chip'}, dimensions={0} | all-to-all | bytes 786432 | tf_op jit(solution)/shard_map/all_to_all | solution.py:361
  80.4 0.7 collective-permute-start.3
  81.1 2.7 %collective-permute-start.6 = (bf16[768,128]{1,0:T(8,128)(2,1)S(1)}, bf16[768,128]{1,0:T(8,128)(2,1)S(1)}, u32[]{:S(2)}, u32[]{:S(2)}) collective-permute-start(bf16[768,128]{1,0:T(8,128)(2,1)S(1)} %bitcast.53), channel_id=1, source_target_pairs={{0,3},{1,0},{2,1},{3,2},{4,7},{5,4},{6,5},{7,6},{8,11},{9,8},{10,9... | collective-permute-start | bytes 589832 | tf_op jit(solution)/shard_map/ppermute | solution.py:366
  83.7 5.4 %collective-permute-done.3.refs_0_ = bf16[768,128]{1,0:T(8,128)(2,1)S(1)} collective-permute-done((bf16[768,128]{1,0:T(8,128)(2,1)S(1)}, bf16[768,128]{1,0:T(8,128)(2,1)S(1)}, u32[]{:S(2)}, u32[]{:S(2)}) %collective-permute-start.3) | collective-permute-done | bytes 196640 | tf_op jit(solution)/shard_map/ppermute | solution.py:366
  89.1 3.2 %collective-permute-start.9 = (bf16[768,128]{1,0:T(8,128)(2,1)S(1)}, bf16[768,128]{1,0:T(8,128)(2,1)S(1)}, u32[]{:S(2)}, u32[]{:S(2)}) collective-permute-start(bf16[768,128]{1,0:T(8,128)(2,1)S(1)} %collective-permute-done.6.refs_3_), channel_id=1, source_target_pairs={{0,3},{1,0},{2,1},{3,2},{4,7},{5,4},{6,5},{7,6},{8,11},{9,8},{10,9... | collective-permute-start | bytes 589832 | tf_op jit(solution)/shard_map/ppermute | solution.py:366
  92.4 3.2 %collective-permute-start.5 = (bf16[768,128]{1,0:T(8,128)(2,1)S(1)}, bf16[768,128]{1,0:T(8,128)(2,1)S(1)}, u32[]{:S(2)}, u32[]{:S(2)}) collective-permute-start(bf16[768,128]{1,0:T(8,128)(2,1)S(1)} %bitcast.52), channel_id=1, source_target_pairs={{0,3},{1,0},{2,1},{3,2},{4,7},{5,4},{6,5},{7,6},{8,11},{9,8},{10,9... | collective-permute-start | bytes 589832 | tf_op jit(solution)/shard_map/ppermute | solution.py:366
  95.6 0.4 collective-permute-done.8.refs_0_
  96.0 2.0 %shard_map.160 = (bf16[768,128]{1,0:T(8,128)(2,1)S(1)}, bf16[768,128]{1,0:T(8,128)(2,1)S(1)}) custom-call(bf16[768,128]{1,0:T(8,128)(2,1)S(1)} %collective-permute-done.8.refs_0_, bf16[768,128]{1,0:T(8,128)(2,1)S(1)} %collective-permute-done.9.refs_1_, bf16[2048,768]{1,0:T(8,128)(2,1)S(1)} %bitcast.25, bf16[2048,768]{1,0:T(8,128)(2,1)S(1)} %bitcast.28, ...), custom_call_target="tpu_custom_call" | custom-call | flops 1536000000 | bytes 10223616 | tf_op jit(solution)/shard_map/pallas_call | solution.py:42
  98.0 3.5 %collective-permute-start.10 = (bf16[768,128]{1,0:T(8,128)(2,1)S(1)}, bf16[768,128]{1,0:T(8,128)(2,1)S(1)}, u32[]{:S(2)}, u32[]{:S(2)}) collective-permute-start(bf16[768,128]{1,0:T(8,128)(2,1)S(1)} %get-tuple-element.40), channel_id=1, source_target_pairs={{0,3},{1,0},{2,1},{3,2},{4,7},{5,4},{6,5},{7,6},{8,11},{9,8},{10,9... | collective-permute-start | bytes 589832 | tf_op jit(solution)/shard_map/ppermute | solution.py:366
  101.6 2.9 %shard_map.159 = (bf16[768,128]{1,0:T(8,128)(2,1)S(1)}, bf16[768,128]{1,0:T(8,128)(2,1)S(1)}, bf16[768,128]{1,0:T(8,128)(2,1)S(1)}, bf16[768,128]{1,0:T(8,128)(2,1)S(1)}) custom-call(bf16[768,128]{1,0:T(8,128)(2,1)S(1)} %collective-permute-done.3.refs_0_, bf16[768,128]{1,0:T(8,128)(2,1)S(1)} %collective-permute-done.4.refs_1_, ...), custom_call_target="tpu_custom_call" | custom-call | flops 3072000000 | bytes 11010048 | tf_op jit(solution)/shard_map/pallas_call | solution.py:42
  104.5 0.1 collective-permute-start.7
  104.6 3.2 %collective-permute-start.14 = (bf16[768,128]{1,0:T(8,128)(2,1)S(1)}, bf16[768,128]{1,0:T(8,128)(2,1)S(1)}, u32[]{:S(2)}, u32[]{:S(2)}) collective-permute-start(bf16[768,128]{1,0:T(8,128)(2,1)S(1)} %get-tuple-element.43), channel_id=1, source_target_pairs={{0,3},{1,0},{2,1},{3,2},{4,7},{5,4},{6,5},{7,6},{8,11},{9,8},{10,9... | collective-permute-start | bytes 589832 | tf_op jit(solution)/shard_map/ppermute | solution.py:366
  107.9 3.3 %collective-permute-start.11 = (bf16[768,128]{1,0:T(8,128)(2,1)S(1)}, bf16[768,128]{1,0:T(8,128)(2,1)S(1)}, u32[]{:S(2)}, u32[]{:S(2)}) collective-permute-start(bf16[768,128]{1,0:T(8,128)(2,1)S(1)} %add_convert_fusion.1), channel_id=1, source_target_pairs={{0,3},{1,0},{2,1},{3,2},{4,7},{5,4},{6,5},{7,6},{8,11},{9,8},{10,9... | collective-permute-start | bytes 589832 | tf_op jit(solution)/shard_map/ppermute | solution.py:366
  111.2 3.5 %collective-permute-done.12 = bf16[768,128]{1,0:T(8,128)(2,1)S(1)} collective-permute-done((bf16[768,128]{1,0:T(8,128)(2,1)S(1)}, bf16[768,128]{1,0:T(8,128)(2,1)S(1)}, u32[]{:S(2)}, u32[]{:S(2)}) %collective-permute-start.12) | collective-permute-done | bytes 196640 | tf_op jit(solution)/shard_map/ppermute | solution.py:366
  114.8 0.1 collective-permute-start.13
  114.9 2.0 %shard_map.158 = bf16[1536,128]{1,0:T(8,128)(2,1)S(1)} custom-call(bf16[1536,128]{1,0:T(8,128)(2,1)S(1)} %bitcast.34, bf16[2048,768]{1,0:T(8,128)(2,1)S(1)} %bitcast.27, bf16[2048,768]{1,0:T(8,128)(2,1)S(1)} %bitcast.30, bf16[768,2048]{1,0:T(8,128)(2,1)S(1)} %bitcast.33), custom_call_target="tpu_custom_call" | custom-call | flops 1536000000 | bytes 10223616 | tf_op jit(solution)/shard_map/pallas_call | solution.py:42
  116.9 4.8 %collective-permute-done.13 = bf16[768,128]{1,0:T(8,128)(2,1)S(1)} collective-permute-done((bf16[768,128]{1,0:T(8,128)(2,1)S(1)}, bf16[768,128]{1,0:T(8,128)(2,1)S(1)}, u32[]{:S(2)}, u32[]{:S(2)}) %collective-permute-start.13) | collective-permute-done | bytes 196640 | tf_op jit(solution)/shard_map/ppermute | solution.py:366
  121.7 0.2 shard_map.161
  121.9 0.1 collective-permute-start.15
  122.1 1.4 collective-permute-done.15.other_ref
  123.6 32.9 %all_to_all.23 = bf16[16,96,128]{2,1,0:T(8,128)(2,1)S(1)} all-to-all(bf16[16,96,128]{2,1,0:T(8,128)(2,1)S(1)} %shard_map.162), channel_id=1, replica_groups=mesh['grp'=2,'chip'=16,'core'=2,'tp'=4] {'chip'}, dimensions={0} | all-to-all | bytes 786432 | tf_op jit(solution)/shard_map/all_to_all | solution.py:361
  156.5 1.7 %shard_map.163 = bf16[48,2048]{1,0:T(8,128)(2,1)} custom-call(bf16[1536,128]{1,0:T(8,128)(2,1)S(1)} %bitcast.37, bf16[48,2048]{1,0:T(8,128)(2,1)S(1)} %get-tuple-element.46.normed_ref, s32[2,48]{1,0:T(2,128)S(1)} %bitcast.49, f32[2,48]{1,0:T(2,128)S(1)} %bitcast.50, f32[1,2048]{1,0:T(1,128)S(1)} %bitcast.46, f32[1,2048]{1,0:T(1,128)S(1)} %bitcast.47), custom_call_target="tpu_custom_call" | custom-call | flops 1000000000 | bytes 803584 | tf_op jit(solution)/shard_map/pallas_call | solution.py:42
  (35 shorter events, 0.3 us)
Async XLA Ops:
  0.0 29.4 %copy-start.3 = (f32[2048]{0:T(1024)S(1)}, f32[2048]{0:T(1024)}, u32[]{:S(2)}) copy-start(f32[2048]{0:T(1024)} %param.23) | copy-start | bytes 24580
  0.0 29.4 %copy-start.4 = (f32[2048]{0:T(1024)S(1)}, f32[2048]{0:T(1024)}, u32[]{:S(2)}) copy-start(f32[2048]{0:T(1024)} %param.24) | copy-start | bytes 24580
  0.0 29.4 %copy-start.7 = (s32[48,2]{0,1:T(2,128)S(1)}, s32[48,2]{0,1:T(2,128)}, u32[]{:S(2)}) copy-start(s32[48,2]{0,1:T(2,128)} %param.25) | copy-start | bytes 1156
  1.0 3.2 %collective-permute-start = (bf16[144,128]{1,0:T(8,128)(2,1)S(1)}, bf16[144,128]{1,0:T(8,128)(2,1)S(1)}, u32[]{:S(2)}, u32[]{:S(2)}) collective-permute-start(bf16[144,128]{1,0:T(8,128)(2,1)S(1)} %get-tuple-element.31), channel_id=1, source_target_pairs={{0,4},{4,8},{8,12},{12,16},{16,20},{20,24},{24,28},{28,32},{32,36}... | collective-permute-start | bytes 110600 | tf_op jit(solution)/shard_map/ppermute | solution.py:313
  2.9 5.6 %collective-permute-start.1 = (bf16[144,128]{1,0:T(8,128)(2,1)S(1)}, bf16[144,128]{1,0:T(8,128)(2,1)S(1)}, u32[]{:S(2)}, u32[]{:S(2)}) collective-permute-start(bf16[144,128]{1,0:T(8,128)(2,1)S(1)} %get-tuple-element.32), channel_id=1, source_target_pairs={{4,0},{8,4},{12,8},{16,12},{20,16},{24,20},{28,24},{32,28},{36,32}... | collective-permute-start | bytes 110600 | tf_op jit(solution)/shard_map/ppermute | solution.py:314
  8.5 87.5 %copy-start.2 = (bf16[1,768,2048]{2,1,0:T(8,128)(2,1)S(1)}, bf16[1,768,2048]{2,1,0:T(8,128)(2,1)}, u32[]{:S(2)}) copy-start(bf16[1,768,2048]{2,1,0:T(8,128)(2,1)} %param.29) | copy-start | bytes 9437188
  12.4 83.6 %copy-start.1 = (bf16[1,2048,768]{2,1,0:T(8,128)(2,1)S(1)}, bf16[1,2048,768]{2,1,0:T(8,128)(2,1)}, u32[]{:S(2)}) copy-start(bf16[1,2048,768]{2,1,0:T(8,128)(2,1)} %param.28) | copy-start | bytes 9437188
  29.3 66.7 %copy-start = (bf16[1,2048,768]{2,1,0:T(8,128)(2,1)S(1)}, bf16[1,2048,768]{2,1,0:T(8,128)(2,1)}, u32[]{:S(2)}) copy-start(bf16[1,2048,768]{2,1,0:T(8,128)(2,1)} %param.27) | copy-start | bytes 9437188
  30.1 2.4 %collective-permute-start.2 = (bf16[768,128]{1,0:T(8,128)(2,1)S(1)}, bf16[768,128]{1,0:T(8,128)(2,1)S(1)}, u32[]{:S(2)}, u32[]{:S(2)}) collective-permute-start(bf16[768,128]{1,0:T(8,128)(2,1)S(1)} %get-tuple-element.37), channel_id=1, source_target_pairs={{0,4},{4,0},{1,5},{5,1},{2,6},{6,2},{3,7},{7,3},{8,12},{12,8},{9,1... | collective-permute-start | bytes 589832 | tf_op jit(solution)/shard_map/ppermute | solution.py:352
  80.4 8.8 %collective-permute-start.3 = (bf16[768,128]{1,0:T(8,128)(2,1)S(1)}, bf16[768,128]{1,0:T(8,128)(2,1)S(1)}, u32[]{:S(2)}, u32[]{:S(2)}) collective-permute-start(bf16[768,128]{1,0:T(8,128)(2,1)S(1)} %bitcast.51), channel_id=1, source_target_pairs={{0,1},{1,2},{2,3},{3,0},{4,5},{5,6},{6,7},{7,4},{8,9},{9,10},{10,1... | collective-permute-start | bytes 589832 | tf_op jit(solution)/shard_map/ppermute | solution.py:366
  81.1 8.1 %collective-permute-start.6 = (bf16[768,128]{1,0:T(8,128)(2,1)S(1)}, bf16[768,128]{1,0:T(8,128)(2,1)S(1)}, u32[]{:S(2)}, u32[]{:S(2)}) collective-permute-start(bf16[768,128]{1,0:T(8,128)(2,1)S(1)} %bitcast.53), channel_id=1, source_target_pairs={{0,3},{1,0},{2,1},{3,2},{4,7},{5,4},{6,5},{7,6},{8,11},{9,8},{10,9... | collective-permute-start | bytes 589832 | tf_op jit(solution)/shard_map/ppermute | solution.py:366
  89.1 6.9 %collective-permute-start.8 = (bf16[768,128]{1,0:T(8,128)(2,1)S(1)}, bf16[768,128]{1,0:T(8,128)(2,1)S(1)}, u32[]{:S(2)}, u32[]{:S(2)}) collective-permute-start(bf16[768,128]{1,0:T(8,128)(2,1)S(1)} %collective-permute-done.3.refs_0_), channel_id=1, source_target_pairs={{0,1},{1,2},{2,3},{3,0},{4,5},{5,6},{6,7},{7,4},{8,9},{9,10},{10,1... | collective-permute-start | bytes 589832 | tf_op jit(solution)/shard_map/ppermute | solution.py:366
  89.1 6.9 %collective-permute-start.9 = (bf16[768,128]{1,0:T(8,128)(2,1)S(1)}, bf16[768,128]{1,0:T(8,128)(2,1)S(1)}, u32[]{:S(2)}, u32[]{:S(2)}) collective-permute-start(bf16[768,128]{1,0:T(8,128)(2,1)S(1)} %collective-permute-done.6.refs_3_), channel_id=1, source_target_pairs={{0,3},{1,0},{2,1},{3,2},{4,7},{5,4},{6,5},{7,6},{8,11},{9,8},{10,9... | collective-permute-start | bytes 589832 | tf_op jit(solution)/shard_map/ppermute | solution.py:366
  92.4 9.2 %collective-permute-start.4 = (bf16[768,128]{1,0:T(8,128)(2,1)S(1)}, bf16[768,128]{1,0:T(8,128)(2,1)S(1)}, u32[]{:S(2)}, u32[]{:S(2)}) collective-permute-start(bf16[768,128]{1,0:T(8,128)(2,1)S(1)} %bitcast.54), channel_id=1, source_target_pairs={{0,1},{1,2},{2,3},{3,0},{4,5},{5,6},{6,7},{7,4},{8,9},{9,10},{10,1... | collective-permute-start | bytes 589832 | tf_op jit(solution)/shard_map/ppermute | solution.py:366
  92.4 9.2 %collective-permute-start.5 = (bf16[768,128]{1,0:T(8,128)(2,1)S(1)}, bf16[768,128]{1,0:T(8,128)(2,1)S(1)}, u32[]{:S(2)}, u32[]{:S(2)}) collective-permute-start(bf16[768,128]{1,0:T(8,128)(2,1)S(1)} %bitcast.52), channel_id=1, source_target_pairs={{0,3},{1,0},{2,1},{3,2},{4,7},{5,4},{6,5},{7,6},{8,11},{9,8},{10,9... | collective-permute-start | bytes 589832 | tf_op jit(solution)/shard_map/ppermute | solution.py:366
  98.0 9.8 %collective-permute-start.10 = (bf16[768,128]{1,0:T(8,128)(2,1)S(1)}, bf16[768,128]{1,0:T(8,128)(2,1)S(1)}, u32[]{:S(2)}, u32[]{:S(2)}) collective-permute-start(bf16[768,128]{1,0:T(8,128)(2,1)S(1)} %get-tuple-element.40), channel_id=1, source_target_pairs={{0,3},{1,0},{2,1},{3,2},{4,7},{5,4},{6,5},{7,6},{8,11},{9,8},{10,9... | collective-permute-start | bytes 589832 | tf_op jit(solution)/shard_map/ppermute | solution.py:366
  104.5 12.5 %collective-permute-start.7 = (bf16[768,128]{1,0:T(8,128)(2,1)S(1)}, bf16[768,128]{1,0:T(8,128)(2,1)S(1)}, u32[]{:S(2)}, u32[]{:S(2)}) collective-permute-start(bf16[768,128]{1,0:T(8,128)(2,1)S(1)} %get-tuple-element.38), channel_id=1, source_target_pairs={{0,1},{1,2},{2,3},{3,0},{4,5},{5,6},{6,7},{7,4},{8,9},{9,10},{10,1... | collective-permute-start | bytes 589832 | tf_op jit(solution)/shard_map/ppermute | solution.py:366
  104.6 12.3 %collective-permute-start.14 = (bf16[768,128]{1,0:T(8,128)(2,1)S(1)}, bf16[768,128]{1,0:T(8,128)(2,1)S(1)}, u32[]{:S(2)}, u32[]{:S(2)}) collective-permute-start(bf16[768,128]{1,0:T(8,128)(2,1)S(1)} %get-tuple-element.43), channel_id=1, source_target_pairs={{0,3},{1,0},{2,1},{3,2},{4,7},{5,4},{6,5},{7,6},{8,11},{9,8},{10,9... | collective-permute-start | bytes 589832 | tf_op jit(solution)/shard_map/ppermute | solution.py:366
  107.8 6.9 %collective-permute-start.12 = (bf16[768,128]{1,0:T(8,128)(2,1)S(1)}, bf16[768,128]{1,0:T(8,128)(2,1)S(1)}, u32[]{:S(2)}, u32[]{:S(2)}) collective-permute-start(bf16[768,128]{1,0:T(8,128)(2,1)S(1)} %get-tuple-element.42), channel_id=1, source_target_pairs={{0,1},{1,2},{2,3},{3,0},{4,5},{5,6},{6,7},{7,4},{8,9},{9,10},{10,1... | collective-permute-start | bytes 589832 | tf_op jit(solution)/shard_map/ppermute | solution.py:366
  107.9 9.1 %collective-permute-start.11 = (bf16[768,128]{1,0:T(8,128)(2,1)S(1)}, bf16[768,128]{1,0:T(8,128)(2,1)S(1)}, u32[]{:S(2)}, u32[]{:S(2)}) collective-permute-start(bf16[768,128]{1,0:T(8,128)(2,1)S(1)} %add_convert_fusion.1), channel_id=1, source_target_pairs={{0,3},{1,0},{2,1},{3,2},{4,7},{5,4},{6,5},{7,6},{8,11},{9,8},{10,9... | collective-permute-start | bytes 589832 | tf_op jit(solution)/shard_map/ppermute | solution.py:366
  114.8 7.0 %collective-permute-start.13 = (bf16[768,128]{1,0:T(8,128)(2,1)S(1)}, bf16[768,128]{1,0:T(8,128)(2,1)S(1)}, u32[]{:S(2)}, u32[]{:S(2)}) collective-permute-start(bf16[768,128]{1,0:T(8,128)(2,1)S(1)} %add_convert_fusion), channel_id=1, source_target_pairs={{0,1},{1,2},{2,3},{3,0},{4,5},{5,6},{6,7},{7,4},{8,9},{9,10},{10,1... | collective-permute-start | bytes 589832 | tf_op jit(solution)/shard_map/ppermute | solution.py:366
  114.9 41.6 %copy-start.5 = (f32[2048]{0:T(1024)S(1)}, f32[2048]{0:T(1024)}, u32[]{:S(2)}) copy-start(f32[2048]{0:T(1024)} %param.30) | copy-start | bytes 24580
  114.9 41.6 %copy-start.6 = (f32[2048]{0:T(1024)S(1)}, f32[2048]{0:T(1024)}, u32[]{:S(2)}) copy-start(f32[2048]{0:T(1024)} %param.31) | copy-start | bytes 24580
  114.9 41.5 %copy-start.8 = (f32[48,2]{0,1:T(2,128)S(1)}, f32[48,2]{0,1:T(2,128)}, u32[]{:S(2)}) copy-start(f32[48,2]{0,1:T(2,128)} %param.26) | copy-start | bytes 1156
  121.9 1.6 collective-permute-start.15

commit v4 on v3

--- a/solution.py
+++ b/solution.py
@@ -74,7 +74,7 @@
         copy.wait()
     keys_ref, values_ref, docs_ref = held[:3]
     tokens = keys_ref.shape[1]
-    docs = (docs_ref[...].astype(F32) + 1.0).astype(BF16)
+    docs = docs_ref[...].astype(F32).astype(BF16)
     for ref, lo in ((head_ref, 0), (tail_ref, tokens - WINDOW)):
         cols = slice(lo, lo + WINDOW)
         ref[0:HEAD_DIM, :] = keys_ref[:, cols]
@@ -92,21 +92,14 @@
     docs_ref,
     prev_ref,
     next_ref,
-    proj_hbm,
-    resid_hbm,
-    out_ref,
-    resid_ref,
-    att_ref,
     proj_ref,
-    sems,
+    member_ref,
+    *refs,
 ):
-    proj_copy = pltpu.make_async_copy(proj_hbm, proj_ref, sems.at[0])
-    resid_copy = pltpu.make_async_copy(resid_hbm, resid_ref, sems.at[1])
-    proj_copy.start()
-    resid_copy.start()
+    out_refs, att_ref = refs[:-1], refs[-1]
     tokens = query_ref.shape[0]
     heads = query_ref.shape[1] // HEAD_DIM
-    own_docs = docs_ref[...].astype(F32) + 1.0
+    own_docs = docs_ref[...].astype(F32)
     query_docs = jnp.broadcast_to(own_docs, (LANES, tokens)).T[:, 0:1]
     row = lax.broadcasted_iota(jnp.int32, (tokens, 1), 0)
     blocks = []
@@ -138,9 +131,11 @@
             mm_nt((r * scale).astype(BF16), value) for r, (_, value, _) in zip(raised, blocks)
         )
         att_ref[:, cols] = result.astype(BF16)
-    proj_copy.wait()
-    out_ref[...] = mm(att_ref[...], proj_ref[...]).astype(BF16)
-    resid_copy.wait()
+    members = len(out_refs)
+    own = tokens // members
+    for by, out_ref in enumerate(out_refs):
+        start = pl.multiple_of(lax.rem(member_ref[0] + by, members) * own, own)
+        out_ref[...] = mm(att_ref[pl.ds(start, own), :], proj_ref[...]).astype(BF16)
 
 
 def routing_rows(ids, expert, weights=None):
@@ -159,23 +154,13 @@
     return (named if weights is None else weighted), rank
 
 
-def dispatch_body(
-    experts,
-    parts_ref,
-    resid_ref,
-    gain_ref,
-    bias_ref,
-    ids_ref,
-    core_ref,
-    normed_ref,
-    same_ref,
-    other_ref,
-    wide_ref,
-):
+def dispatch_body(experts, members, *refs):
+    part_refs, (resid_ref, gain_ref, bias_ref, ids_ref, core_ref) = refs[:members], refs[members : members + 5]
+    normed_ref, same_ref, other_ref, wide_ref = refs[members + 5 :]
     tokens, width = resid_ref.shape
     tiles = width // LANES
     capacity = ids_ref.shape[0] * tokens // experts
-    projected = sum(parts_ref[i].astype(F32) for i in range(parts_ref.shape[0]))
+    projected = sum(ref[...].astype(F32) for ref in part_refs)
     pre_norm = RESIDUAL_SCALE * resid_ref[...].astype(F32) + projected.astype(BF16).astype(F32)
     normed = layer_norm(pre_norm, gain_ref[...], bias_ref[...]).astype(BF16)
     normed_ref[...] = normed
@@ -298,10 +283,10 @@
     tiles = width // LANES
     packed = experts * capacity * tiles
 
-    small = (keys.T, values.T, doc_ids.reshape(1, tokens), queries, sink_logits.reshape(1, -1))
+    small = (keys.T, values.T, doc_ids.reshape(1, tokens), queries, out_proj, resid, sink_logits.reshape(1, -1))
     pack = shape((2 * HEAD_DIM + 16, WINDOW), BF16)
     core = jnp.full((1, LANES), lax.axis_index("core"), jnp.int32)
-    keys_t, values_t, docs, queries, sinks, head, tail, core = call(
+    keys_t, values_t, docs, queries, out_proj, resid, sinks, head, tail, core = call(
         functools.partial(first_body, len(small)),
         [shape(a.shape, a.dtype) for a in small] + [pack, pack, shape(core.shape, core.dtype)],
         core,
@@ -310,11 +295,11 @@
         specs=[VMEM] + [HBM] * len(small),
         scratch=[pltpu.SemaphoreType.DMA((len(small),))],
     )
-    previous = lax.ppermute(tail, SP, [(i, i + 1) for i in range(blocks - 1)])
-    following = lax.ppermute(head, SP, [(i + 1, i) for i in range(blocks - 1)])
-    partial, resid = call(
+    previous = lax.ppermute(tail, SP, [(i, (i + 1) % blocks) for i in range(blocks)])
+    following = lax.ppermute(head, SP, [((i + 1) % blocks, i) for i in range(blocks)])
+    shares = call(
         attention_body,
-        [shape((tokens, width), BF16), shape(resid.shape, BF16)],
+        [shape((own, width), BF16)] * members,
         sinks,
         queries,
         keys_t,
@@ -322,21 +307,21 @@
         docs,
         previous,
         following,
-        in_hbm(out_proj),
-        in_hbm(resid),
+        out_proj,
+        lax.axis_index("tp").astype(jnp.int32).reshape(1),
         flops=10**9,
-        specs=[VMEM] * 7 + [HBM] * 2,
-        scratch=[
-            pltpu.VMEM(queries.shape, BF16),
-            pltpu.VMEM(out_proj.shape, BF16),
-            pltpu.SemaphoreType.DMA((2,)),
-        ],
-    )
-    parts = lax.all_to_all(partial.reshape(members, own, width), "tp", 0, 0, tiled=True)
+        specs=[VMEM] * 8 + [pl.BlockSpec(memory_space=pltpu.SMEM)],
+        scratch=[pltpu.VMEM(queries.shape, BF16)],
+    )
+
+    def turned(array, by):
+        return lax.ppermute(array, "tp", [(i, (i + by) % members) for i in range(members)])
+
+    parts = [shares[0]] + [turned(shares[by], by) for by in range(1, members)]
     normed, same, other = call(
-        functools.partial(dispatch_body, experts),
+        functools.partial(dispatch_body, experts, members),
         [shape((own, width), BF16)] + [shape((packed // 2, LANES), BF16)] * 2,
-        parts,
+        *parts,
         resid,
         norm1_gain.reshape(1, -1),
         norm1_bias.reshape(1, -1),
@@ -361,9 +346,6 @@
         return lax.all_to_all(sent.reshape(packed, LANES), "chip", 0, 0, tiled=True)
 
     arrived = exchanged(same, other)
-
-    def turned(array, by):
-        return lax.ppermute(array, "tp", [(i, (i + by) % members) for i in range(members)])
 
     def expert_call(*row_sets):
         count, rows = len(row_sets), row_sets[0].shape[0]
@@ -446,6 +428,4 @@
         P(),
     )
 
-    return jax.shard_map(
-        per_device, mesh=mesh, in_specs=placed, out_specs=P(every, None), check_vma=False
-    )
+    return jax.shard_map(per_device, mesh=mesh, in_specs=placed, out_specs=P(every, None), check_vma=False)

time: 158 us -> 151 us (0.956)
  blocking collectives: 97.5 us -> 64.2 us
  starting transfers between devices: 24.8 us -> 48.4 us
  waiting for transfers between devices: 20.9 us -> 23 us
    ppermute x2, starting transfers between devices: 3.15 us -> 22 us  [the longest x1 21.9 us: per_device(): lax.ppermute(head, SP, [((i + 1) % blocks, i) for i in range(blocks)])]
    all_to_all x1 -> x0, blocking collectives: 16.9 us -> none  [per_device(): lax.all_to_all(partial.reshape(members, own, width), 'tp', 0, 0, tiled=True)]
    all_to_all x2, blocking collectives: 80.5 us -> 64.2 us  [exchanged(): return lax.all_to_all(sent.reshape(packed, LANES), 'chip', 0, 0, tiled=True)]
    ppermute x12 -> x15, starting transfers between devices: 20.2 us -> 26.2 us  [turned(): lax.ppermute(array, 'tp', [(i, (i + by) % members) for i in range(members)])]
    ppermute x12 -> x15, waiting for transfers between devices: 14.1 us -> 18.6 us  [turned(): lax.ppermute(array, 'tp', [(i, (i + by) % members) for i in range(members)])]
    ppermute x2, waiting for transfers between devices: 4.31 us -> 1.64 us  [the longest x1 1.58 us: per_device(): lax.ppermute(tail, SP, [(i, (i + 1) % blocks) for i in range(blocks)])]
  transfers between devices with their start and end apart: 16 -> 19, of which waited for: 7 -> 10; matrix products, arithmetic and copies ran while one was open for 0% -> 0% of each run, Pallas kernels for 4% -> 5%
where the time goes in v4:
time: 151 us
  blocking collectives  64.2 us (43%)
  starting transfers between devices  48.4 us (32%)
  waiting for transfers between devices  23 us (15%)
  Pallas kernels  14.4 us (10%)
    all_to_all x2, blocking collectives, exchanged(): return lax.all_to_all(sent.reshape(packed, LANES), 'chip', 0, 0, tiled=True)  64.2 us
    ppermute x15, starting transfers between devices, turned(): lax.ppermute(array, 'tp', [(i, (i + by) % members) for i in range(members)])  26.2 us
    ppermute x1, starting transfers between devices, per_device(): lax.ppermute(head, SP, [((i + 1) % blocks, i) for i in range(blocks)])  21.9 us
    ppermute x15, waiting for transfers between devices, turned(): lax.ppermute(array, 'tp', [(i, (i + by) % members) for i in range(members)])  18.6 us
    pallas_call x10, Pallas kernels, call(): pl.pallas_call(body, out_shape=out_shapes, in_specs=specs or [VMEM] * len...  14.4 us
  transfers between devices with their start and end apart: 19, of which 10 were waited for; matrix products, arithmetic and copies ran while one was open for 0% of the time, Pallas kernels for 5%

profile of v4, /device:TPU:40, one launch (start us, length us, event | category | flops | bytes accessed | tf_op | source)
XLA Modules:
  0.0 150.5 jit_solution(16642572899541125200)
XLA Ops:
  0.0 1.4 shard_map.154
  1.5 21.9 %collective-permute-start.1 = (bf16[144,128]{1,0:T(8,128)(2,1)S(1)}, bf16[144,128]{1,0:T(8,128)(2,1)S(1)}, u32[]{:S(2)}, u32[]{:S(2)}) collective-permute-start(bf16[144,128]{1,0:T(8,128)(2,1)S(1)} %get-tuple-element.36), channel_id=1, source_target_pairs={{4,0},{8,4},{12,8},{16,12},{20,16},{24,20},{28,24},{32,28},{36,32}... | collective-permute-start | bytes 110600 | tf_op jit(solution)/shard_map/ppermute | solution.py:299
  23.5 1.6 %collective-permute-done.prev_ref = bf16[144,128]{1,0:T(8,128)(2,1)S(1)} collective-permute-done((bf16[144,128]{1,0:T(8,128)(2,1)S(1)}, bf16[144,128]{1,0:T(8,128)(2,1)S(1)}, u32[]{:S(2)}, u32[]{:S(2)}) %collective-permute-start) | collective-permute-done | bytes 36896 | tf_op jit(solution)/shard_map/ppermute | solution.py:298
  25.1 3.3 %shard_map.155 = (bf16[48,2048]{1,0:T(8,128)(2,1)S(1)}, bf16[48,2048]{1,0:T(8,128)(2,1)S(1)}, bf16[48,2048]{1,0:T(8,128)(2,1)S(1)}, bf16[48,2048]{1,0:T(8,128)(2,1)S(1)}) custom-call(f32[1,4]{1,0:T(1,128)S(1)} %get-tuple-element.30.sink_ref, bf16[192,256]{1,0:T(8,128)(2,1)S(1)} %get-tuple-element.31.query_ref, ...), custom_call_target="tpu_custom_call" | custom-call | flops 1000000000 | bytes 2056980 | tf_op jit(solution)/shard_map/pallas_call | solution.py:42
  28.4 1.7 %collective-permute-start.2 = (bf16[48,2048]{1,0:T(8,128)(2,1)S(1)}, bf16[48,2048]{1,0:T(8,128)(2,1)S(1)}, u32[]{:S(2)}, u32[]{:S(2)}) collective-permute-start(bf16[48,2048]{1,0:T(8,128)(2,1)S(1)} %get-tuple-element.39), channel_id=1, source_target_pairs={{0,1},{1,2},{2,3},{3,0},{4,5},{5,6},{6,7},{7,4},{8,9},{9,10},{10,1... | collective-permute-start | bytes 589832 | tf_op jit(solution)/shard_map/ppermute | solution.py:318
  30.2 3.0 %collective-permute-start.3 = (bf16[48,2048]{1,0:T(8,128)(2,1)S(1)}, bf16[48,2048]{1,0:T(8,128)(2,1)S(1)}, u32[]{:S(2)}, u32[]{:S(2)}) collective-permute-start(bf16[48,2048]{1,0:T(8,128)(2,1)S(1)} %get-tuple-element.40), channel_id=1, source_target_pairs={{0,2},{1,3},{2,0},{3,1},{4,6},{5,7},{6,4},{7,5},{8,10},{9,11},{10,... | collective-permute-start | bytes 589832 | tf_op jit(solution)/shard_map/ppermute | solution.py:318
  33.2 1.3 collective-permute-start.4
  34.5 1.0 collective-permute-done.2.refs_1_
  35.4 3.5 %collective-permute-done.3.refs_2_ = bf16[48,2048]{1,0:T(8,128)(2,1)S(1)} collective-permute-done((bf16[48,2048]{1,0:T(8,128)(2,1)S(1)}, bf16[48,2048]{1,0:T(8,128)(2,1)S(1)}, u32[]{:S(2)}, u32[]{:S(2)}) %collective-permute-start.3) | collective-permute-done | bytes 196640 | tf_op jit(solution)/shard_map/ppermute | solution.py:318
  39.0 0.8 shard_map.156
  39.7 0.1 collective-permute-start.5
  39.9 1.4 collective-permute-done.5
  41.4 31.6 %all_to_all.16 = bf16[16,96,128]{2,1,0:T(8,128)(2,1)S(1)} all-to-all(bf16[16,96,128]{2,1,0:T(8,128)(2,1)S(1)} %shard_map.157), channel_id=1, replica_groups=mesh['grp'=2,'chip'=16,'core'=2,'tp'=4] {'chip'}, dimensions={0} | all-to-all | bytes 786432 | tf_op jit(solution)/shard_map/all_to_all | solution.py:346
  73.1 1.8 %collective-permute-start.6 = (bf16[768,128]{1,0:T(8,128)(2,1)S(1)}, bf16[768,128]{1,0:T(8,128)(2,1)S(1)}, u32[]{:S(2)}, u32[]{:S(2)}) collective-permute-start(bf16[768,128]{1,0:T(8,128)(2,1)S(1)} %bitcast.50), channel_id=1, source_target_pairs={{0,1},{1,2},{2,3},{3,0},{4,5},{5,6},{6,7},{7,4},{8,9},{9,10},{10,1... | collective-permute-start | bytes 589832 | tf_op jit(solution)/shard_map/ppermute | solution.py:318
  74.9 1.5 %collective-permute-start.9 = (bf16[768,128]{1,0:T(8,128)(2,1)S(1)}, bf16[768,128]{1,0:T(8,128)(2,1)S(1)}, u32[]{:S(2)}, u32[]{:S(2)}) collective-permute-start(bf16[768,128]{1,0:T(8,128)(2,1)S(1)} %bitcast.52), channel_id=1, source_target_pairs={{0,3},{1,0},{2,1},{3,2},{4,7},{5,4},{6,5},{7,6},{8,11},{9,8},{10,9... | collective-permute-start | bytes 589832 | tf_op jit(solution)/shard_map/ppermute | solution.py:318
  76.4 5.4 %collective-permute-done.6.refs_0_ = bf16[768,128]{1,0:T(8,128)(2,1)S(1)} collective-permute-done((bf16[768,128]{1,0:T(8,128)(2,1)S(1)}, bf16[768,128]{1,0:T(8,128)(2,1)S(1)}, u32[]{:S(2)}, u32[]{:S(2)}) %collective-permute-start.6) | collective-permute-done | bytes 196640 | tf_op jit(solution)/shard_map/ppermute | solution.py:318
  81.8 0.2 collective-permute-start.11
  82.1 3.0 %collective-permute-start.12 = (bf16[768,128]{1,0:T(8,128)(2,1)S(1)}, bf16[768,128]{1,0:T(8,128)(2,1)S(1)}, u32[]{:S(2)}, u32[]{:S(2)}) collective-permute-start(bf16[768,128]{1,0:T(8,128)(2,1)S(1)} %collective-permute-done.9.refs_3_), channel_id=1, source_target_pairs={{0,3},{1,0},{2,1},{3,2},{4,7},{5,4},{6,5},{7,6},{8,11},{9,8},{10,9... | collective-permute-start | bytes 589832 | tf_op jit(solution)/shard_map/ppermute | solution.py:318
  85.1 3.2 %collective-permute-start.8 = (bf16[768,128]{1,0:T(8,128)(2,1)S(1)}, bf16[768,128]{1,0:T(8,128)(2,1)S(1)}, u32[]{:S(2)}, u32[]{:S(2)}) collective-permute-start(bf16[768,128]{1,0:T(8,128)(2,1)S(1)} %bitcast.51), channel_id=1, source_target_pairs={{0,3},{1,0},{2,1},{3,2},{4,7},{5,4},{6,5},{7,6},{8,11},{9,8},{10,9... | collective-permute-start | bytes 589832 | tf_op jit(solution)/shard_map/ppermute | solution.py:318
  88.3 0.4 collective-permute-done.11.refs_0_
  88.7 2.0 %shard_map.160 = (bf16[768,128]{1,0:T(8,128)(2,1)S(1)}, bf16[768,128]{1,0:T(8,128)(2,1)S(1)}) custom-call(bf16[768,128]{1,0:T(8,128)(2,1)S(1)} %collective-permute-done.11.refs_0_, bf16[768,128]{1,0:T(8,128)(2,1)S(1)} %collective-permute-done.12.refs_1_, bf16[2048,768]{1,0:T(8,128)(2,1)S(1)} %bitcast.25, bf16[2048,768]{1,0:T(8,128)(2,1)S(1)} %bitcast.28, ...), custom_call_target="tpu_custom_call" | custom-call | flops 1536000000 | bytes 10223616 | tf_op jit(solution)/shard_map/pallas_call | solution.py:42
  90.7 3.3 %collective-permute-start.13 = (bf16[768,128]{1,0:T(8,128)(2,1)S(1)}, bf16[768,128]{1,0:T(8,128)(2,1)S(1)}, u32[]{:S(2)}, u32[]{:S(2)}) collective-permute-start(bf16[768,128]{1,0:T(8,128)(2,1)S(1)} %get-tuple-element.48), channel_id=1, source_target_pairs={{0,3},{1,0},{2,1},{3,2},{4,7},{5,4},{6,5},{7,6},{8,11},{9,8},{10,9... | collective-permute-start | bytes 589832 | tf_op jit(solution)/shard_map/ppermute | solution.py:318
  94.1 2.9 %shard_map.159 = (bf16[768,128]{1,0:T(8,128)(2,1)S(1)}, bf16[768,128]{1,0:T(8,128)(2,1)S(1)}, bf16[768,128]{1,0:T(8,128)(2,1)S(1)}, bf16[768,128]{1,0:T(8,128)(2,1)S(1)}) custom-call(bf16[768,128]{1,0:T(8,128)(2,1)S(1)} %collective-permute-done.6.refs_0_, bf16[768,128]{1,0:T(8,128)(2,1)S(1)} %collective-permute-done.7.refs_1_, ...), custom_call_target="tpu_custom_call" | custom-call | flops 3072000000 | bytes 11010048 | tf_op jit(solution)/shard_map/pallas_call | solution.py:42
  97.1 3.4 %collective-permute-start.17 = (bf16[768,128]{1,0:T(8,128)(2,1)S(1)}, bf16[768,128]{1,0:T(8,128)(2,1)S(1)}, u32[]{:S(2)}, u32[]{:S(2)}) collective-permute-start(bf16[768,128]{1,0:T(8,128)(2,1)S(1)} %get-tuple-element.51), channel_id=1, source_target_pairs={{0,3},{1,0},{2,1},{3,2},{4,7},{5,4},{6,5},{7,6},{8,11},{9,8},{10,9... | collective-permute-start | bytes 589832 | tf_op jit(solution)/shard_map/ppermute | solution.py:318
  100.5 3.3 %collective-permute-start.14 = (bf16[768,128]{1,0:T(8,128)(2,1)S(1)}, bf16[768,128]{1,0:T(8,128)(2,1)S(1)}, u32[]{:S(2)}, u32[]{:S(2)}) collective-permute-start(bf16[768,128]{1,0:T(8,128)(2,1)S(1)} %add_convert_fusion.1), channel_id=1, source_target_pairs={{0,3},{1,0},{2,1},{3,2},{4,7},{5,4},{6,5},{7,6},{8,11},{9,8},{10,9... | collective-permute-start | bytes 589832 | tf_op jit(solution)/shard_map/ppermute | solution.py:318
  103.9 3.5 %collective-permute-done.15 = bf16[768,128]{1,0:T(8,128)(2,1)S(1)} collective-permute-done((bf16[768,128]{1,0:T(8,128)(2,1)S(1)}, bf16[768,128]{1,0:T(8,128)(2,1)S(1)}, u32[]{:S(2)}, u32[]{:S(2)}) %collective-permute-start.15) | collective-permute-done | bytes 196640 | tf_op jit(solution)/shard_map/ppermute | solution.py:318
  107.6 2.0 %shard_map.158 = bf16[1536,128]{1,0:T(8,128)(2,1)S(1)} custom-call(bf16[1536,128]{1,0:T(8,128)(2,1)S(1)} %bitcast.34, bf16[2048,768]{1,0:T(8,128)(2,1)S(1)} %bitcast.27, bf16[2048,768]{1,0:T(8,128)(2,1)S(1)} %bitcast.30, bf16[768,2048]{1,0:T(8,128)(2,1)S(1)} %bitcast.33), custom_call_target="tpu_custom_call" | custom-call | flops 1536000000 | bytes 10223616 | tf_op jit(solution)/shard_map/pallas_call | solution.py:42
  109.6 4.8 %collective-permute-done.16 = bf16[768,128]{1,0:T(8,128)(2,1)S(1)} collective-permute-done((bf16[768,128]{1,0:T(8,128)(2,1)S(1)}, bf16[768,128]{1,0:T(8,128)(2,1)S(1)}, u32[]{:S(2)}, u32[]{:S(2)}) %collective-permute-start.16) | collective-permute-done | bytes 196640 | tf_op jit(solution)/shard_map/ppermute | solution.py:318
  114.4 0.2 shard_map.161
  114.7 1.4 collective-permute-done.18.other_ref
  116.2 32.6 %all_to_all.17 = bf16[16,96,128]{2,1,0:T(8,128)(2,1)S(1)} all-to-all(bf16[16,96,128]{2,1,0:T(8,128)(2,1)S(1)} %shard_map.162), channel_id=1, replica_groups=mesh['grp'=2,'chip'=16,'core'=2,'tp'=4] {'chip'}, dimensions={0} | all-to-all | bytes 786432 | tf_op jit(solution)/shard_map/all_to_all | solution.py:346
  148.8 1.7 %shard_map.163 = bf16[48,2048]{1,0:T(8,128)(2,1)} custom-call(bf16[1536,128]{1,0:T(8,128)(2,1)S(1)} %bitcast.36, bf16[48,2048]{1,0:T(8,128)(2,1)S(1)} %get-tuple-element.54.normed_ref, s32[2,48]{1,0:T(2,128)S(1)} %bitcast.48, f32[2,48]{1,0:T(2,128)S(1)} %bitcast.49, f32[1,2048]{1,0:T(1,128)S(1)} %bitcast.45, f32[1,2048]{1,0:T(1,128)S(1)} %bitcast.46), custom_call_target="tpu_custom_call" | custom-call | flops 1000000000 | bytes 803584 | tf_op jit(solution)/shard_map/pallas_call | solution.py:42
  (40 shorter events, 0.9 us)
Async XLA Ops:
  0.0 38.9 %copy-start.3 = (f32[2048]{0:T(1024)S(1)}, f32[2048]{0:T(1024)}, u32[]{:S(2)}) copy-start(f32[2048]{0:T(1024)} %param.23) | copy-start | bytes 24580
  0.0 38.9 %copy-start.4 = (f32[2048]{0:T(1024)S(1)}, f32[2048]{0:T(1024)}, u32[]{:S(2)}) copy-start(f32[2048]{0:T(1024)} %param.24) | copy-start | bytes 24580
  0.0 38.9 %copy-start.7 = (s32[48,2]{0,1:T(2,128)S(1)}, s32[48,2]{0,1:T(2,128)}, u32[]{:S(2)}) copy-start(s32[48,2]{0,1:T(2,128)} %param.25) | copy-start | bytes 1156
  1.5 23.6 %collective-permute-start = (bf16[144,128]{1,0:T(8,128)(2,1)S(1)}, bf16[144,128]{1,0:T(8,128)(2,1)S(1)}, u32[]{:S(2)}, u32[]{:S(2)}) collective-permute-start(bf16[144,128]{1,0:T(8,128)(2,1)S(1)} %get-tuple-element.35), channel_id=1, source_target_pairs={{0,4},{4,8},{8,12},{12,16},{16,20},{20,24},{24,28},{28,32},{32,36}... | collective-permute-start | bytes 110600 | tf_op jit(solution)/shard_map/ppermute | solution.py:298
  1.5 23.6 %collective-permute-start.1 = (bf16[144,128]{1,0:T(8,128)(2,1)S(1)}, bf16[144,128]{1,0:T(8,128)(2,1)S(1)}, u32[]{:S(2)}, u32[]{:S(2)}) collective-permute-start(bf16[144,128]{1,0:T(8,128)(2,1)S(1)} %get-tuple-element.36), channel_id=1, source_target_pairs={{4,0},{8,4},{12,8},{16,12},{20,16},{24,20},{28,24},{32,28},{36,32}... | collective-permute-start | bytes 110600 | tf_op jit(solution)/shard_map/ppermute | solution.py:299
  25.1 63.6 %copy-start.1 = (bf16[1,2048,768]{2,1,0:T(8,128)(2,1)S(1)}, bf16[1,2048,768]{2,1,0:T(8,128)(2,1)}, u32[]{:S(2)}) copy-start(bf16[1,2048,768]{2,1,0:T(8,128)(2,1)} %param.28) | copy-start | bytes 9437188
  25.1 63.6 %copy-start.2 = (bf16[1,768,2048]{2,1,0:T(8,128)(2,1)S(1)}, bf16[1,768,2048]{2,1,0:T(8,128)(2,1)}, u32[]{:S(2)}) copy-start(bf16[1,768,2048]{2,1,0:T(8,128)(2,1)} %param.29) | copy-start | bytes 9437188
  28.4 60.3 %copy-start = (bf16[1,2048,768]{2,1,0:T(8,128)(2,1)S(1)}, bf16[1,2048,768]{2,1,0:T(8,128)(2,1)}, u32[]{:S(2)}) copy-start(bf16[1,2048,768]{2,1,0:T(8,128)(2,1)} %param.27) | copy-start | bytes 9437188
  28.4 7.0 %collective-permute-start.2 = (bf16[48,2048]{1,0:T(8,128)(2,1)S(1)}, bf16[48,2048]{1,0:T(8,128)(2,1)S(1)}, u32[]{:S(2)}, u32[]{:S(2)}) collective-permute-start(bf16[48,2048]{1,0:T(8,128)(2,1)S(1)} %get-tuple-element.39), channel_id=1, source_target_pairs={{0,1},{1,2},{2,3},{3,0},{4,5},{5,6},{6,7},{7,4},{8,9},{9,10},{10,1... | collective-permute-start | bytes 589832 | tf_op jit(solution)/shard_map/ppermute | solution.py:318
  30.2 8.8 %collective-permute-start.3 = (bf16[48,2048]{1,0:T(8,128)(2,1)S(1)}, bf16[48,2048]{1,0:T(8,128)(2,1)S(1)}, u32[]{:S(2)}, u32[]{:S(2)}) collective-permute-start(bf16[48,2048]{1,0:T(8,128)(2,1)S(1)} %get-tuple-element.40), channel_id=1, source_target_pairs={{0,2},{1,3},{2,0},{3,1},{4,6},{5,7},{6,4},{7,5},{8,10},{9,11},{10,... | collective-permute-start | bytes 589832 | tf_op jit(solution)/shard_map/ppermute | solution.py:318
  33.2 5.8 %collective-permute-start.4 = (bf16[48,2048]{1,0:T(8,128)(2,1)S(1)}, bf16[48,2048]{1,0:T(8,128)(2,1)S(1)}, u32[]{:S(2)}, u32[]{:S(2)}) collective-permute-start(bf16[48,2048]{1,0:T(8,128)(2,1)S(1)} %get-tuple-element.41), channel_id=1, source_target_pairs={{0,3},{1,0},{2,1},{3,2},{4,7},{5,4},{6,5},{7,6},{8,11},{9,8},{10,9... | collective-permute-start | bytes 589832 | tf_op jit(solution)/shard_map/ppermute | solution.py:318
  39.7 1.6 %collective-permute-start.5 = (bf16[768,128]{1,0:T(8,128)(2,1)S(1)}, bf16[768,128]{1,0:T(8,128)(2,1)S(1)}, u32[]{:S(2)}, u32[]{:S(2)}) collective-permute-start(bf16[768,128]{1,0:T(8,128)(2,1)S(1)} %get-tuple-element.45), channel_id=1, source_target_pairs={{0,4},{4,0},{1,5},{5,1},{2,6},{6,2},{3,7},{7,3},{8,12},{12,8},{9,1... | collective-permute-start | bytes 589832 | tf_op jit(solution)/shard_map/ppermute | solution.py:337
  73.1 8.8 %collective-permute-start.6 = (bf16[768,128]{1,0:T(8,128)(2,1)S(1)}, bf16[768,128]{1,0:T(8,128)(2,1)S(1)}, u32[]{:S(2)}, u32[]{:S(2)}) collective-permute-start(bf16[768,128]{1,0:T(8,128)(2,1)S(1)} %bitcast.50), channel_id=1, source_target_pairs={{0,1},{1,2},{2,3},{3,0},{4,5},{5,6},{6,7},{7,4},{8,9},{9,10},{10,1... | collective-permute-start | bytes 589832 | tf_op jit(solution)/shard_map/ppermute | solution.py:318
  74.9 7.2 %collective-permute-start.9 = (bf16[768,128]{1,0:T(8,128)(2,1)S(1)}, bf16[768,128]{1,0:T(8,128)(2,1)S(1)}, u32[]{:S(2)}, u32[]{:S(2)}) collective-permute-start(bf16[768,128]{1,0:T(8,128)(2,1)S(1)} %bitcast.52), channel_id=1, source_target_pairs={{0,3},{1,0},{2,1},{3,2},{4,7},{5,4},{6,5},{7,6},{8,11},{9,8},{10,9... | collective-permute-start | bytes 589832 | tf_op jit(solution)/shard_map/ppermute | solution.py:318
  81.8 6.9 %collective-permute-start.11 = (bf16[768,128]{1,0:T(8,128)(2,1)S(1)}, bf16[768,128]{1,0:T(8,128)(2,1)S(1)}, u32[]{:S(2)}, u32[]{:S(2)}) collective-permute-start(bf16[768,128]{1,0:T(8,128)(2,1)S(1)} %collective-permute-done.6.refs_0_), channel_id=1, source_target_pairs={{0,1},{1,2},{2,3},{3,0},{4,5},{5,6},{6,7},{7,4},{8,9},{9,10},{10,1... | collective-permute-start | bytes 589832 | tf_op jit(solution)/shard_map/ppermute | solution.py:318
  82.1 6.7 %collective-permute-start.12 = (bf16[768,128]{1,0:T(8,128)(2,1)S(1)}, bf16[768,128]{1,0:T(8,128)(2,1)S(1)}, u32[]{:S(2)}, u32[]{:S(2)}) collective-permute-start(bf16[768,128]{1,0:T(8,128)(2,1)S(1)} %collective-permute-done.9.refs_3_), channel_id=1, source_target_pairs={{0,3},{1,0},{2,1},{3,2},{4,7},{5,4},{6,5},{7,6},{8,11},{9,8},{10,9... | collective-permute-start | bytes 589832 | tf_op jit(solution)/shard_map/ppermute | solution.py:318
  85.1 9.0 %collective-permute-start.7 = (bf16[768,128]{1,0:T(8,128)(2,1)S(1)}, bf16[768,128]{1,0:T(8,128)(2,1)S(1)}, u32[]{:S(2)}, u32[]{:S(2)}) collective-permute-start(bf16[768,128]{1,0:T(8,128)(2,1)S(1)} %bitcast.53), channel_id=1, source_target_pairs={{0,1},{1,2},{2,3},{3,0},{4,5},{5,6},{6,7},{7,4},{8,9},{9,10},{10,1... | collective-permute-start | bytes 589832 | tf_op jit(solution)/shard_map/ppermute | solution.py:318
  85.1 9.0 %collective-permute-start.8 = (bf16[768,128]{1,0:T(8,128)(2,1)S(1)}, bf16[768,128]{1,0:T(8,128)(2,1)S(1)}, u32[]{:S(2)}, u32[]{:S(2)}) collective-permute-start(bf16[768,128]{1,0:T(8,128)(2,1)S(1)} %bitcast.51), channel_id=1, source_target_pairs={{0,3},{1,0},{2,1},{3,2},{4,7},{5,4},{6,5},{7,6},{8,11},{9,8},{10,9... | collective-permute-start | bytes 589832 | tf_op jit(solution)/shard_map/ppermute | solution.py:318
  90.7 9.7 %collective-permute-start.13 = (bf16[768,128]{1,0:T(8,128)(2,1)S(1)}, bf16[768,128]{1,0:T(8,128)(2,1)S(1)}, u32[]{:S(2)}, u32[]{:S(2)}) collective-permute-start(bf16[768,128]{1,0:T(8,128)(2,1)S(1)} %get-tuple-element.48), channel_id=1, source_target_pairs={{0,3},{1,0},{2,1},{3,2},{4,7},{5,4},{6,5},{7,6},{8,11},{9,8},{10,9... | collective-permute-start | bytes 589832 | tf_op jit(solution)/shard_map/ppermute | solution.py:318
  97.0 12.6 %collective-permute-start.10 = (bf16[768,128]{1,0:T(8,128)(2,1)S(1)}, bf16[768,128]{1,0:T(8,128)(2,1)S(1)}, u32[]{:S(2)}, u32[]{:S(2)}) collective-permute-start(bf16[768,128]{1,0:T(8,128)(2,1)S(1)} %get-tuple-element.46), channel_id=1, source_target_pairs={{0,1},{1,2},{2,3},{3,0},{4,5},{5,6},{6,7},{7,4},{8,9},{9,10},{10,1... | collective-permute-start | bytes 589832 | tf_op jit(solution)/shard_map/ppermute | solution.py:318
  97.1 12.5 %collective-permute-start.17 = (bf16[768,128]{1,0:T(8,128)(2,1)S(1)}, bf16[768,128]{1,0:T(8,128)(2,1)S(1)}, u32[]{:S(2)}, u32[]{:S(2)}) collective-permute-start(bf16[768,128]{1,0:T(8,128)(2,1)S(1)} %get-tuple-element.51), channel_id=1, source_target_pairs={{0,3},{1,0},{2,1},{3,2},{4,7},{5,4},{6,5},{7,6},{8,11},{9,8},{10,9... | collective-permute-start | bytes 589832 | tf_op jit(solution)/shard_map/ppermute | solution.py:318
  100.4 6.9 %collective-permute-start.15 = (bf16[768,128]{1,0:T(8,128)(2,1)S(1)}, bf16[768,128]{1,0:T(8,128)(2,1)S(1)}, u32[]{:S(2)}, u32[]{:S(2)}) collective-permute-start(bf16[768,128]{1,0:T(8,128)(2,1)S(1)} %get-tuple-element.50), channel_id=1, source_target_pairs={{0,1},{1,2},{2,3},{3,0},{4,5},{5,6},{6,7},{7,4},{8,9},{9,10},{10,1... | collective-permute-start | bytes 589832 | tf_op jit(solution)/shard_map/ppermute | solution.py:318
  100.5 9.1 %collective-permute-start.14 = (bf16[768,128]{1,0:T(8,128)(2,1)S(1)}, bf16[768,128]{1,0:T(8,128)(2,1)S(1)}, u32[]{:S(2)}, u32[]{:S(2)}) collective-permute-start(bf16[768,128]{1,0:T(8,128)(2,1)S(1)} %add_convert_fusion.1), channel_id=1, source_target_pairs={{0,3},{1,0},{2,1},{3,2},{4,7},{5,4},{6,5},{7,6},{8,11},{9,8},{10,9... | collective-permute-start | bytes 589832 | tf_op jit(solution)/shard_map/ppermute | solution.py:318
  107.4 7.0 %collective-permute-start.16 = (bf16[768,128]{1,0:T(8,128)(2,1)S(1)}, bf16[768,128]{1,0:T(8,128)(2,1)S(1)}, u32[]{:S(2)}, u32[]{:S(2)}) collective-permute-start(bf16[768,128]{1,0:T(8,128)(2,1)S(1)} %add_convert_fusion), channel_id=1, source_target_pairs={{0,1},{1,2},{2,3},{3,0},{4,5},{5,6},{6,7},{7,4},{8,9},{9,10},{10,1... | collective-permute-start | bytes 589832 | tf_op jit(solution)/shard_map/ppermute | solution.py:318
  107.5 41.3 %copy-start.5 = (f32[2048]{0:T(1024)S(1)}, f32[2048]{0:T(1024)}, u32[]{:S(2)}) copy-start(f32[2048]{0:T(1024)} %param.30) | copy-start | bytes 24580
  107.5 41.3 %copy-start.6 = (f32[2048]{0:T(1024)S(1)}, f32[2048]{0:T(1024)}, u32[]{:S(2)}) copy-start(f32[2048]{0:T(1024)} %param.31) | copy-start | bytes 24580
  107.5 41.3 %copy-start.8 = (f32[48,2]{0,1:T(2,128)S(1)}, f32[48,2]{0,1:T(2,128)}, u32[]{:S(2)}) copy-start(f32[48,2]{0,1:T(2,128)} %param.26) | copy-start | bytes 1156
  114.6 1.6 %collective-permute-start.18 = (bf16[16,48,128]{2,1,0:T(8,128)(2,1)S(1)}, bf16[16,48,128]{2,1,0:T(8,128)(2,1)S(1)}, u32[]{:S(2)}, u32[]{:S(2)}) collective-permute-start(bf16[16,48,128]{2,1,0:T(8,128)(2,1)S(1)} %get-tuple-element.53), channel_id=1, source_target_pairs={{0,4},{4,0},{1,5},{5,1},{2,6},{6,2},{3,7},{7,3},{8,12},{12,8},{9,1... | collective-permute-start | bytes 589832 | tf_op jit(solution)/shard_map/ppermute | solution.py:337

commit v5 on v4

--- a/solution.py
+++ b/solution.py
@@ -81,6 +81,15 @@
         ref[HEAD_DIM : 2 * HEAD_DIM, :] = values_ref[:, cols]
         ref[2 * HEAD_DIM :, :] = jnp.broadcast_to(docs[:, cols], (16, WINDOW))
     for copy in copies[3:]:
+        copy.wait()
+
+
+def fetch_body(count, *refs):
+    sources, held, sems = refs[:count], refs[count : 2 * count], refs[2 * count]
+    copies = [pltpu.make_async_copy(a, b, sems.at[i]) for i, (a, b) in enumerate(zip(sources, held))]
+    for copy in copies:
+        copy.start()
+    for copy in copies:
         copy.wait()
 
 
@@ -133,9 +142,13 @@
         att_ref[:, cols] = result.astype(BF16)
     members = len(out_refs)
     own = tokens // members
+    ordered = []
+    for by in range(members):
+        start = pl.multiple_of(lax.rem(member_ref[0] + by, members) * own, own)
+        ordered.append(att_ref[pl.ds(start, own), :])
+    shares = mm(jnp.concatenate(ordered, axis=0), proj_ref[...])
     for by, out_ref in enumerate(out_refs):
-        start = pl.multiple_of(lax.rem(member_ref[0] + by, members) * own, own)
-        out_ref[...] = mm(att_ref[pl.ds(start, own), :], proj_ref[...]).astype(BF16)
+        out_ref[...] = shares[by * own : (by + 1) * own].astype(BF16)
 
 
 def routing_rows(ids, expert, weights=None):
@@ -283,10 +296,10 @@
     tiles = width // LANES
     packed = experts * capacity * tiles
 
-    small = (keys.T, values.T, doc_ids.reshape(1, tokens), queries, out_proj, resid, sink_logits.reshape(1, -1))
+    small = (keys.T, values.T, doc_ids.reshape(1, tokens), queries, sink_logits.reshape(1, -1))
     pack = shape((2 * HEAD_DIM + 16, WINDOW), BF16)
     core = jnp.full((1, LANES), lax.axis_index("core"), jnp.int32)
-    keys_t, values_t, docs, queries, out_proj, resid, sinks, head, tail, core = call(
+    keys_t, values_t, docs, queries, sinks, head, tail, core = call(
         functools.partial(first_body, len(small)),
         [shape(a.shape, a.dtype) for a in small] + [pack, pack, shape(core.shape, core.dtype)],
         core,
@@ -297,6 +310,15 @@
     )
     previous = lax.ppermute(tail, SP, [(i, (i + 1) % blocks) for i in range(blocks)])
     following = lax.ppermute(head, SP, [((i + 1) % blocks, i) for i in range(blocks)])
+    later = (out_proj, resid)
+    out_proj, resid = call(
+        functools.partial(fetch_body, len(later)),
+        [shape(a.shape, a.dtype) for a in later],
+        *[in_hbm(a) for a in later],
+        flops=10**5,
+        specs=[HBM] * len(later),
+        scratch=[pltpu.SemaphoreType.DMA((len(later),))],
+    )
     shares = call(
         attention_body,
         [shape((own, width), BF16)] * members,

time: 151 us -> 150 us (level)
    pallas_call x10 -> x11, Pallas kernels: 14.4 us -> 14.8 us  [call(): pl.pallas_call(body, out_shape=out_shapes, in_specs=specs or [VMEM] * len...]
where the time goes in v5:
time: 150 us
  blocking collectives  64.2 us (43%)
  starting transfers between devices  48.4 us (32%)
  waiting for transfers between devices  21.8 us (15%)
  Pallas kernels  14.8 us (10%)
    all_to_all x2, blocking collectives, exchanged(): return lax.all_to_all(sent.reshape(packed, LANES), 'chip', 0, 0, tiled=True)  64.2 us
    ppermute x15, starting transfers between devices, turned(): lax.ppermute(array, 'tp', [(i, (i + by) % members) for i in range(members)])  26.2 us
    ppermute x1, starting transfers between devices, per_device(): lax.ppermute(head, SP, [((i + 1) % blocks, i) for i in range(blocks)])  21.9 us
    ppermute x15, waiting for transfers between devices, turned(): lax.ppermute(array, 'tp', [(i, (i + by) % members) for i in range(members)])  18.6 us
    pallas_call x11, Pallas kernels, call(): pl.pallas_call(body, out_shape=out_shapes, in_specs=specs or [VMEM] * len...  14.8 us
  transfers between devices with their start and end apart: 19, of which 10 were waited for; matrix products, arithmetic and copies ran while one was open for 0% of the time, Pallas kernels for 5%

profile of v5, /device:TPU:40, one launch (start us, length us, event | category | flops | bytes accessed | tf_op | source)
XLA Modules:
  0.0 149.7 jit_solution(4958787030834678247)
XLA Ops:
  0.0 1.0 shard_map.154
  1.1 21.9 %collective-permute-start.1 = (bf16[144,128]{1,0:T(8,128)(2,1)S(1)}, bf16[144,128]{1,0:T(8,128)(2,1)S(1)}, u32[]{:S(2)}, u32[]{:S(2)}) collective-permute-start(bf16[144,128]{1,0:T(8,128)(2,1)S(1)} %get-tuple-element.36), channel_id=1, source_target_pairs={{4,0},{8,4},{12,8},{16,12},{20,16},{24,20},{28,24},{32,28},{36,32}... | collective-permute-start | bytes 110600 | tf_op jit(solution)/shard_map/ppermute | solution.py:312
  23.1 1.3 shard_map.155
  24.3 0.3 collective-permute-done.prev_ref
  24.7 2.9 %shard_map.156 = (bf16[48,2048]{1,0:T(8,128)(2,1)S(1)}, bf16[48,2048]{1,0:T(8,128)(2,1)S(1)}, bf16[48,2048]{1,0:T(8,128)(2,1)S(1)}, bf16[48,2048]{1,0:T(8,128)(2,1)S(1)}) custom-call(f32[1,4]{1,0:T(1,128)S(1)} %get-tuple-element.30.sink_ref, bf16[192,256]{1,0:T(8,128)(2,1)S(1)} %get-tuple-element.31.query_ref, ...), custom_call_target="tpu_custom_call" | custom-call | flops 1000000000 | bytes 2056980 | tf_op jit(solution)/shard_map/pallas_call | solution.py:42
  27.6 1.7 %collective-permute-start.2 = (bf16[48,2048]{1,0:T(8,128)(2,1)S(1)}, bf16[48,2048]{1,0:T(8,128)(2,1)S(1)}, u32[]{:S(2)}, u32[]{:S(2)}) collective-permute-start(bf16[48,2048]{1,0:T(8,128)(2,1)S(1)} %get-tuple-element.39), channel_id=1, source_target_pairs={{0,1},{1,2},{2,3},{3,0},{4,5},{5,6},{6,7},{7,4},{8,9},{9,10},{10,1... | collective-permute-start | bytes 589832 | tf_op jit(solution)/shard_map/ppermute | solution.py:340
  29.3 3.0 %collective-permute-start.3 = (bf16[48,2048]{1,0:T(8,128)(2,1)S(1)}, bf16[48,2048]{1,0:T(8,128)(2,1)S(1)}, u32[]{:S(2)}, u32[]{:S(2)}) collective-permute-start(bf16[48,2048]{1,0:T(8,128)(2,1)S(1)} %get-tuple-element.40), channel_id=1, source_target_pairs={{0,2},{1,3},{2,0},{3,1},{4,6},{5,7},{6,4},{7,5},{8,10},{9,11},{10,... | collective-permute-start | bytes 589832 | tf_op jit(solution)/shard_map/ppermute | solution.py:340
  32.3 1.3 collective-permute-start.4
  33.6 1.0 collective-permute-done.2.refs_1_
  34.6 3.5 %collective-permute-done.3.refs_2_ = bf16[48,2048]{1,0:T(8,128)(2,1)S(1)} collective-permute-done((bf16[48,2048]{1,0:T(8,128)(2,1)S(1)}, bf16[48,2048]{1,0:T(8,128)(2,1)S(1)}, u32[]{:S(2)}, u32[]{:S(2)}) %collective-permute-start.3) | collective-permute-done | bytes 196640 | tf_op jit(solution)/shard_map/ppermute | solution.py:340
  38.1 0.8 shard_map.157
  39.0 1.4 collective-permute-done.5
  40.6 31.6 %all_to_all.16 = bf16[16,96,128]{2,1,0:T(8,128)(2,1)S(1)} all-to-all(bf16[16,96,128]{2,1,0:T(8,128)(2,1)S(1)} %shard_map.158), channel_id=1, replica_groups=mesh['grp'=2,'chip'=16,'core'=2,'tp'=4] {'chip'}, dimensions={0} | all-to-all | bytes 786432 | tf_op jit(solution)/shard_map/all_to_all | solution.py:368
  72.2 1.8 %collective-permute-start.6 = (bf16[768,128]{1,0:T(8,128)(2,1)S(1)}, bf16[768,128]{1,0:T(8,128)(2,1)S(1)}, u32[]{:S(2)}, u32[]{:S(2)}) collective-permute-start(bf16[768,128]{1,0:T(8,128)(2,1)S(1)} %bitcast.50), channel_id=1, source_target_pairs={{0,1},{1,2},{2,3},{3,0},{4,5},{5,6},{6,7},{7,4},{8,9},{9,10},{10,1... | collective-permute-start | bytes 589832 | tf_op jit(solution)/shard_map/ppermute | solution.py:340
  74.0 1.5 %collective-permute-start.9 = (bf16[768,128]{1,0:T(8,128)(2,1)S(1)}, bf16[768,128]{1,0:T(8,128)(2,1)S(1)}, u32[]{:S(2)}, u32[]{:S(2)}) collective-permute-start(bf16[768,128]{1,0:T(8,128)(2,1)S(1)} %bitcast.52), channel_id=1, source_target_pairs={{0,3},{1,0},{2,1},{3,2},{4,7},{5,4},{6,5},{7,6},{8,11},{9,8},{10,9... | collective-permute-start | bytes 589832 | tf_op jit(solution)/shard_map/ppermute | solution.py:340
  75.6 5.4 %collective-permute-done.6.refs_0_ = bf16[768,128]{1,0:T(8,128)(2,1)S(1)} collective-permute-done((bf16[768,128]{1,0:T(8,128)(2,1)S(1)}, bf16[768,128]{1,0:T(8,128)(2,1)S(1)}, u32[]{:S(2)}, u32[]{:S(2)}) %collective-permute-start.6) | collective-permute-done | bytes 196640 | tf_op jit(solution)/shard_map/ppermute | solution.py:340
  81.0 0.2 collective-permute-start.11
  81.2 3.0 %collective-permute-start.12 = (bf16[768,128]{1,0:T(8,128)(2,1)S(1)}, bf16[768,128]{1,0:T(8,128)(2,1)S(1)}, u32[]{:S(2)}, u32[]{:S(2)}) collective-permute-start(bf16[768,128]{1,0:T(8,128)(2,1)S(1)} %collective-permute-done.9.refs_3_), channel_id=1, source_target_pairs={{0,3},{1,0},{2,1},{3,2},{4,7},{5,4},{6,5},{7,6},{8,11},{9,8},{10,9... | collective-permute-start | bytes 589832 | tf_op jit(solution)/shard_map/ppermute | solution.py:340
  84.2 3.2 %collective-permute-start.8 = (bf16[768,128]{1,0:T(8,128)(2,1)S(1)}, bf16[768,128]{1,0:T(8,128)(2,1)S(1)}, u32[]{:S(2)}, u32[]{:S(2)}) collective-permute-start(bf16[768,128]{1,0:T(8,128)(2,1)S(1)} %bitcast.51), channel_id=1, source_target_pairs={{0,3},{1,0},{2,1},{3,2},{4,7},{5,4},{6,5},{7,6},{8,11},{9,8},{10,9... | collective-permute-start | bytes 589832 | tf_op jit(solution)/shard_map/ppermute | solution.py:340
  87.5 0.4 collective-permute-done.11.refs_0_
  87.9 2.0 %shard_map.161 = (bf16[768,128]{1,0:T(8,128)(2,1)S(1)}, bf16[768,128]{1,0:T(8,128)(2,1)S(1)}) custom-call(bf16[768,128]{1,0:T(8,128)(2,1)S(1)} %collective-permute-done.11.refs_0_, bf16[768,128]{1,0:T(8,128)(2,1)S(1)} %collective-permute-done.12.refs_1_, bf16[2048,768]{1,0:T(8,128)(2,1)S(1)} %bitcast.25, bf16[2048,768]{1,0:T(8,128)(2,1)S(1)} %bitcast.28, ...), custom_call_target="tpu_custom_call" | custom-call | flops 1536000000 | bytes 10223616 | tf_op jit(solution)/shard_map/pallas_call | solution.py:42
  89.9 3.3 %collective-permute-start.13 = (bf16[768,128]{1,0:T(8,128)(2,1)S(1)}, bf16[768,128]{1,0:T(8,128)(2,1)S(1)}, u32[]{:S(2)}, u32[]{:S(2)}) collective-permute-start(bf16[768,128]{1,0:T(8,128)(2,1)S(1)} %get-tuple-element.48), channel_id=1, source_target_pairs={{0,3},{1,0},{2,1},{3,2},{4,7},{5,4},{6,5},{7,6},{8,11},{9,8},{10,9... | collective-permute-start | bytes 589832 | tf_op jit(solution)/shard_map/ppermute | solution.py:340
  93.2 2.9 %shard_map.160 = (bf16[768,128]{1,0:T(8,128)(2,1)S(1)}, bf16[768,128]{1,0:T(8,128)(2,1)S(1)}, bf16[768,128]{1,0:T(8,128)(2,1)S(1)}, bf16[768,128]{1,0:T(8,128)(2,1)S(1)}) custom-call(bf16[768,128]{1,0:T(8,128)(2,1)S(1)} %collective-permute-done.6.refs_0_, bf16[768,128]{1,0:T(8,128)(2,1)S(1)} %collective-permute-done.7.refs_1_, ...), custom_call_target="tpu_custom_call" | custom-call | flops 3072000000 | bytes 11010048 | tf_op jit(solution)/shard_map/pallas_call | solution.py:42
  96.2 3.3 %collective-permute-start.17 = (bf16[768,128]{1,0:T(8,128)(2,1)S(1)}, bf16[768,128]{1,0:T(8,128)(2,1)S(1)}, u32[]{:S(2)}, u32[]{:S(2)}) collective-permute-start(bf16[768,128]{1,0:T(8,128)(2,1)S(1)} %get-tuple-element.51), channel_id=1, source_target_pairs={{0,3},{1,0},{2,1},{3,2},{4,7},{5,4},{6,5},{7,6},{8,11},{9,8},{10,9... | collective-permute-start | bytes 589832 | tf_op jit(solution)/shard_map/ppermute | solution.py:340
  99.7 3.3 %collective-permute-start.14 = (bf16[768,128]{1,0:T(8,128)(2,1)S(1)}, bf16[768,128]{1,0:T(8,128)(2,1)S(1)}, u32[]{:S(2)}, u32[]{:S(2)}) collective-permute-start(bf16[768,128]{1,0:T(8,128)(2,1)S(1)} %add_convert_fusion.1), channel_id=1, source_target_pairs={{0,3},{1,0},{2,1},{3,2},{4,7},{5,4},{6,5},{7,6},{8,11},{9,8},{10,9... | collective-permute-start | bytes 589832 | tf_op jit(solution)/shard_map/ppermute | solution.py:340
  103.0 3.5 %collective-permute-done.15 = bf16[768,128]{1,0:T(8,128)(2,1)S(1)} collective-permute-done((bf16[768,128]{1,0:T(8,128)(2,1)S(1)}, bf16[768,128]{1,0:T(8,128)(2,1)S(1)}, u32[]{:S(2)}, u32[]{:S(2)}) %collective-permute-start.15) | collective-permute-done | bytes 196640 | tf_op jit(solution)/shard_map/ppermute | solution.py:340
  106.7 2.0 %shard_map.159 = bf16[1536,128]{1,0:T(8,128)(2,1)S(1)} custom-call(bf16[1536,128]{1,0:T(8,128)(2,1)S(1)} %bitcast.34, bf16[2048,768]{1,0:T(8,128)(2,1)S(1)} %bitcast.27, bf16[2048,768]{1,0:T(8,128)(2,1)S(1)} %bitcast.30, bf16[768,2048]{1,0:T(8,128)(2,1)S(1)} %bitcast.33), custom_call_target="tpu_custom_call" | custom-call | flops 1536000000 | bytes 10223616 | tf_op jit(solution)/shard_map/pallas_call | solution.py:42
  108.7 4.8 %collective-permute-done.16 = bf16[768,128]{1,0:T(8,128)(2,1)S(1)} collective-permute-done((bf16[768,128]{1,0:T(8,128)(2,1)S(1)}, bf16[768,128]{1,0:T(8,128)(2,1)S(1)}, u32[]{:S(2)}, u32[]{:S(2)}) %collective-permute-start.16) | collective-permute-done | bytes 196640 | tf_op jit(solution)/shard_map/ppermute | solution.py:340
  113.5 0.2 shard_map.162
  113.8 1.4 collective-permute-done.18.other_ref
  115.4 32.6 %all_to_all.17 = bf16[16,96,128]{2,1,0:T(8,128)(2,1)S(1)} all-to-all(bf16[16,96,128]{2,1,0:T(8,128)(2,1)S(1)} %shard_map.163), channel_id=1, replica_groups=mesh['grp'=2,'chip'=16,'core'=2,'tp'=4] {'chip'}, dimensions={0} | all-to-all | bytes 786432 | tf_op jit(solution)/shard_map/all_to_all | solution.py:368
  148.0 1.7 %shard_map.164 = bf16[48,2048]{1,0:T(8,128)(2,1)} custom-call(bf16[1536,128]{1,0:T(8,128)(2,1)S(1)} %bitcast.36, bf16[48,2048]{1,0:T(8,128)(2,1)S(1)} %get-tuple-element.54.normed_ref, s32[2,48]{1,0:T(2,128)S(1)} %bitcast.48, f32[2,48]{1,0:T(2,128)S(1)} %bitcast.49, f32[1,2048]{1,0:T(1,128)S(1)} %bitcast.45, f32[1,2048]{1,0:T(1,128)S(1)} %bitcast.46), custom_call_target="tpu_custom_call" | custom-call | flops 1000000000 | bytes 803584 | tf_op jit(solution)/shard_map/pallas_call | solution.py:42
  (41 shorter events, 1.1 us)
Async XLA Ops:
  0.0 38.1 %copy-start.3 = (f32[2048]{0:T(1024)S(1)}, f32[2048]{0:T(1024)}, u32[]{:S(2)}) copy-start(f32[2048]{0:T(1024)} %param.23) | copy-start | bytes 24580
  0.0 38.1 %copy-start.4 = (f32[2048]{0:T(1024)S(1)}, f32[2048]{0:T(1024)}, u32[]{:S(2)}) copy-start(f32[2048]{0:T(1024)} %param.24) | copy-start | bytes 24580
  0.0 38.1 %copy-start.7 = (s32[48,2]{0,1:T(2,128)S(1)}, s32[48,2]{0,1:T(2,128)}, u32[]{:S(2)}) copy-start(s32[48,2]{0,1:T(2,128)} %param.25) | copy-start | bytes 1156
  1.0 23.6 %collective-permute-start = (bf16[144,128]{1,0:T(8,128)(2,1)S(1)}, bf16[144,128]{1,0:T(8,128)(2,1)S(1)}, u32[]{:S(2)}, u32[]{:S(2)}) collective-permute-start(bf16[144,128]{1,0:T(8,128)(2,1)S(1)} %get-tuple-element.35), channel_id=1, source_target_pairs={{0,4},{4,8},{8,12},{12,16},{16,20},{20,24},{24,28},{28,32},{32,36}... | collective-permute-start | bytes 110600 | tf_op jit(solution)/shard_map/ppermute | solution.py:311
  1.1 23.6 %collective-permute-start.1 = (bf16[144,128]{1,0:T(8,128)(2,1)S(1)}, bf16[144,128]{1,0:T(8,128)(2,1)S(1)}, u32[]{:S(2)}, u32[]{:S(2)}) collective-permute-start(bf16[144,128]{1,0:T(8,128)(2,1)S(1)} %get-tuple-element.36), channel_id=1, source_target_pairs={{4,0},{8,4},{12,8},{16,12},{20,16},{24,20},{28,24},{32,28},{36,32}... | collective-permute-start | bytes 110600 | tf_op jit(solution)/shard_map/ppermute | solution.py:312
  24.7 63.2 %copy-start.1 = (bf16[1,2048,768]{2,1,0:T(8,128)(2,1)S(1)}, bf16[1,2048,768]{2,1,0:T(8,128)(2,1)}, u32[]{:S(2)}) copy-start(bf16[1,2048,768]{2,1,0:T(8,128)(2,1)} %param.28) | copy-start | bytes 9437188
  24.7 63.2 %copy-start.2 = (bf16[1,768,2048]{2,1,0:T(8,128)(2,1)S(1)}, bf16[1,768,2048]{2,1,0:T(8,128)(2,1)}, u32[]{:S(2)}) copy-start(bf16[1,768,2048]{2,1,0:T(8,128)(2,1)} %param.29) | copy-start | bytes 9437188
  27.6 60.3 %copy-start = (bf16[1,2048,768]{2,1,0:T(8,128)(2,1)S(1)}, bf16[1,2048,768]{2,1,0:T(8,128)(2,1)}, u32[]{:S(2)}) copy-start(bf16[1,2048,768]{2,1,0:T(8,128)(2,1)} %param.27) | copy-start | bytes 9437188
  27.6 7.0 %collective-permute-start.2 = (bf16[48,2048]{1,0:T(8,128)(2,1)S(1)}, bf16[48,2048]{1,0:T(8,128)(2,1)S(1)}, u32[]{:S(2)}, u32[]{:S(2)}) collective-permute-start(bf16[48,2048]{1,0:T(8,128)(2,1)S(1)} %get-tuple-element.39), channel_id=1, source_target_pairs={{0,1},{1,2},{2,3},{3,0},{4,5},{5,6},{6,7},{7,4},{8,9},{9,10},{10,1... | collective-permute-start | bytes 589832 | tf_op jit(solution)/shard_map/ppermute | solution.py:340
  29.3 8.8 %collective-permute-start.3 = (bf16[48,2048]{1,0:T(8,128)(2,1)S(1)}, bf16[48,2048]{1,0:T(8,128)(2,1)S(1)}, u32[]{:S(2)}, u32[]{:S(2)}) collective-permute-start(bf16[48,2048]{1,0:T(8,128)(2,1)S(1)} %get-tuple-element.40), channel_id=1, source_target_pairs={{0,2},{1,3},{2,0},{3,1},{4,6},{5,7},{6,4},{7,5},{8,10},{9,11},{10,... | collective-permute-start | bytes 589832 | tf_op jit(solution)/shard_map/ppermute | solution.py:340
  32.3 5.8 %collective-permute-start.4 = (bf16[48,2048]{1,0:T(8,128)(2,1)S(1)}, bf16[48,2048]{1,0:T(8,128)(2,1)S(1)}, u32[]{:S(2)}, u32[]{:S(2)}) collective-permute-start(bf16[48,2048]{1,0:T(8,128)(2,1)S(1)} %get-tuple-element.41), channel_id=1, source_target_pairs={{0,3},{1,0},{2,1},{3,2},{4,7},{5,4},{6,5},{7,6},{8,11},{9,8},{10,9... | collective-permute-start | bytes 589832 | tf_op jit(solution)/shard_map/ppermute | solution.py:340
  38.9 1.6 %collective-permute-start.5 = (bf16[768,128]{1,0:T(8,128)(2,1)S(1)}, bf16[768,128]{1,0:T(8,128)(2,1)S(1)}, u32[]{:S(2)}, u32[]{:S(2)}) collective-permute-start(bf16[768,128]{1,0:T(8,128)(2,1)S(1)} %get-tuple-element.45), channel_id=1, source_target_pairs={{0,4},{4,0},{1,5},{5,1},{2,6},{6,2},{3,7},{7,3},{8,12},{12,8},{9,1... | collective-permute-start | bytes 589832 | tf_op jit(solution)/shard_map/ppermute | solution.py:359
  72.2 8.8 %collective-permute-start.6 = (bf16[768,128]{1,0:T(8,128)(2,1)S(1)}, bf16[768,128]{1,0:T(8,128)(2,1)S(1)}, u32[]{:S(2)}, u32[]{:S(2)}) collective-permute-start(bf16[768,128]{1,0:T(8,128)(2,1)S(1)} %bitcast.50), channel_id=1, source_target_pairs={{0,1},{1,2},{2,3},{3,0},{4,5},{5,6},{6,7},{7,4},{8,9},{9,10},{10,1... | collective-permute-start | bytes 589832 | tf_op jit(solution)/shard_map/ppermute | solution.py:340
  74.0 7.2 %collective-permute-start.9 = (bf16[768,128]{1,0:T(8,128)(2,1)S(1)}, bf16[768,128]{1,0:T(8,128)(2,1)S(1)}, u32[]{:S(2)}, u32[]{:S(2)}) collective-permute-start(bf16[768,128]{1,0:T(8,128)(2,1)S(1)} %bitcast.52), channel_id=1, source_target_pairs={{0,3},{1,0},{2,1},{3,2},{4,7},{5,4},{6,5},{7,6},{8,11},{9,8},{10,9... | collective-permute-start | bytes 589832 | tf_op jit(solution)/shard_map/ppermute | solution.py:340
  81.0 6.9 %collective-permute-start.11 = (bf16[768,128]{1,0:T(8,128)(2,1)S(1)}, bf16[768,128]{1,0:T(8,128)(2,1)S(1)}, u32[]{:S(2)}, u32[]{:S(2)}) collective-permute-start(bf16[768,128]{1,0:T(8,128)(2,1)S(1)} %collective-permute-done.6.refs_0_), channel_id=1, source_target_pairs={{0,1},{1,2},{2,3},{3,0},{4,5},{5,6},{6,7},{7,4},{8,9},{9,10},{10,1... | collective-permute-start | bytes 589832 | tf_op jit(solution)/shard_map/ppermute | solution.py:340
  81.2 6.7 %collective-permute-start.12 = (bf16[768,128]{1,0:T(8,128)(2,1)S(1)}, bf16[768,128]{1,0:T(8,128)(2,1)S(1)}, u32[]{:S(2)}, u32[]{:S(2)}) collective-permute-start(bf16[768,128]{1,0:T(8,128)(2,1)S(1)} %collective-permute-done.9.refs_3_), channel_id=1, source_target_pairs={{0,3},{1,0},{2,1},{3,2},{4,7},{5,4},{6,5},{7,6},{8,11},{9,8},{10,9... | collective-permute-start | bytes 589832 | tf_op jit(solution)/shard_map/ppermute | solution.py:340
  84.2 9.0 %collective-permute-start.7 = (bf16[768,128]{1,0:T(8,128)(2,1)S(1)}, bf16[768,128]{1,0:T(8,128)(2,1)S(1)}, u32[]{:S(2)}, u32[]{:S(2)}) collective-permute-start(bf16[768,128]{1,0:T(8,128)(2,1)S(1)} %bitcast.53), channel_id=1, source_target_pairs={{0,1},{1,2},{2,3},{3,0},{4,5},{5,6},{6,7},{7,4},{8,9},{9,10},{10,1... | collective-permute-start | bytes 589832 | tf_op jit(solution)/shard_map/ppermute | solution.py:340
  84.2 9.0 %collective-permute-start.8 = (bf16[768,128]{1,0:T(8,128)(2,1)S(1)}, bf16[768,128]{1,0:T(8,128)(2,1)S(1)}, u32[]{:S(2)}, u32[]{:S(2)}) collective-permute-start(bf16[768,128]{1,0:T(8,128)(2,1)S(1)} %bitcast.51), channel_id=1, source_target_pairs={{0,3},{1,0},{2,1},{3,2},{4,7},{5,4},{6,5},{7,6},{8,11},{9,8},{10,9... | collective-permute-start | bytes 589832 | tf_op jit(solution)/shard_map/ppermute | solution.py:340
  89.9 9.7 %collective-permute-start.13 = (bf16[768,128]{1,0:T(8,128)(2,1)S(1)}, bf16[768,128]{1,0:T(8,128)(2,1)S(1)}, u32[]{:S(2)}, u32[]{:S(2)}) collective-permute-start(bf16[768,128]{1,0:T(8,128)(2,1)S(1)} %get-tuple-element.48), channel_id=1, source_target_pairs={{0,3},{1,0},{2,1},{3,2},{4,7},{5,4},{6,5},{7,6},{8,11},{9,8},{10,9... | collective-permute-start | bytes 589832 | tf_op jit(solution)/shard_map/ppermute | solution.py:340
  96.1 12.6 %collective-permute-start.10 = (bf16[768,128]{1,0:T(8,128)(2,1)S(1)}, bf16[768,128]{1,0:T(8,128)(2,1)S(1)}, u32[]{:S(2)}, u32[]{:S(2)}) collective-permute-start(bf16[768,128]{1,0:T(8,128)(2,1)S(1)} %get-tuple-element.46), channel_id=1, source_target_pairs={{0,1},{1,2},{2,3},{3,0},{4,5},{5,6},{6,7},{7,4},{8,9},{9,10},{10,1... | collective-permute-start | bytes 589832 | tf_op jit(solution)/shard_map/ppermute | solution.py:340
  96.2 12.5 %collective-permute-start.17 = (bf16[768,128]{1,0:T(8,128)(2,1)S(1)}, bf16[768,128]{1,0:T(8,128)(2,1)S(1)}, u32[]{:S(2)}, u32[]{:S(2)}) collective-permute-start(bf16[768,128]{1,0:T(8,128)(2,1)S(1)} %get-tuple-element.51), channel_id=1, source_target_pairs={{0,3},{1,0},{2,1},{3,2},{4,7},{5,4},{6,5},{7,6},{8,11},{9,8},{10,9... | collective-permute-start | bytes 589832 | tf_op jit(solution)/shard_map/ppermute | solution.py:340
  99.6 6.9 %collective-permute-start.15 = (bf16[768,128]{1,0:T(8,128)(2,1)S(1)}, bf16[768,128]{1,0:T(8,128)(2,1)S(1)}, u32[]{:S(2)}, u32[]{:S(2)}) collective-permute-start(bf16[768,128]{1,0:T(8,128)(2,1)S(1)} %get-tuple-element.50), channel_id=1, source_target_pairs={{0,1},{1,2},{2,3},{3,0},{4,5},{5,6},{6,7},{7,4},{8,9},{9,10},{10,1... | collective-permute-start | bytes 589832 | tf_op jit(solution)/shard_map/ppermute | solution.py:340
  99.7 9.1 %collective-permute-start.14 = (bf16[768,128]{1,0:T(8,128)(2,1)S(1)}, bf16[768,128]{1,0:T(8,128)(2,1)S(1)}, u32[]{:S(2)}, u32[]{:S(2)}) collective-permute-start(bf16[768,128]{1,0:T(8,128)(2,1)S(1)} %add_convert_fusion.1), channel_id=1, source_target_pairs={{0,3},{1,0},{2,1},{3,2},{4,7},{5,4},{6,5},{7,6},{8,11},{9,8},{10,9... | collective-permute-start | bytes 589832 | tf_op jit(solution)/shard_map/ppermute | solution.py:340
  106.5 7.0 %collective-permute-start.16 = (bf16[768,128]{1,0:T(8,128)(2,1)S(1)}, bf16[768,128]{1,0:T(8,128)(2,1)S(1)}, u32[]{:S(2)}, u32[]{:S(2)}) collective-permute-start(bf16[768,128]{1,0:T(8,128)(2,1)S(1)} %add_convert_fusion), channel_id=1, source_target_pairs={{0,1},{1,2},{2,3},{3,0},{4,5},{5,6},{6,7},{7,4},{8,9},{9,10},{10,1... | collective-permute-start | bytes 589832 | tf_op jit(solution)/shard_map/ppermute | solution.py:340
  106.7 41.3 %copy-start.5 = (f32[2048]{0:T(1024)S(1)}, f32[2048]{0:T(1024)}, u32[]{:S(2)}) copy-start(f32[2048]{0:T(1024)} %param.30) | copy-start | bytes 24580
  106.7 41.3 %copy-start.6 = (f32[2048]{0:T(1024)S(1)}, f32[2048]{0:T(1024)}, u32[]{:S(2)}) copy-start(f32[2048]{0:T(1024)} %param.31) | copy-start | bytes 24580
  106.7 41.3 %copy-start.8 = (f32[48,2]{0,1:T(2,128)S(1)}, f32[48,2]{0,1:T(2,128)}, u32[]{:S(2)}) copy-start(f32[48,2]{0,1:T(2,128)} %param.26) | copy-start | bytes 1156
  113.7 1.6 %collective-permute-start.18 = (bf16[16,48,128]{2,1,0:T(8,128)(2,1)S(1)}, bf16[16,48,128]{2,1,0:T(8,128)(2,1)S(1)}, u32[]{:S(2)}, u32[]{:S(2)}) collective-permute-start(bf16[16,48,128]{2,1,0:T(8,128)(2,1)S(1)} %get-tuple-element.53), channel_id=1, source_target_pairs={{0,4},{4,0},{1,5},{5,1},{2,6},{6,2},{3,7},{7,3},{8,12},{12,8},{9,1... | collective-permute-start | bytes 589832 | tf_op jit(solution)/shard_map/ppermute | solution.py:359
